TPU v7x, 256 devices: a 4x2x16 block of a 4x16x16 slice. The times are simulated.
256 devices in a mesh: grp: 2 (over y), fs: 16 (over z), tp: 8 (over x, core).
Axes of the slice: x: 4, y: 2, z: 16, core: 2. Of those that a mesh axis runs over, the one named last changes fastest.
The devices are a block of a 4x16x16 slice.
Arguments:
- prompt_rows: bfloat16 [32768, 2048], P(('grp', 'fs')), parts along dimension 0, may hold values from -6 to 6
- up_master: float32 [2048, 8192], P('fs', 'tp'), may hold values from -0.125 to 0.125
- down_master: float32 [8192, 2048], P('fs', 'tp'), may hold values from -0.0625 to 0.0625
- norm_gain: float32 [2048], P('fs'), may hold values from 0.1 to 1.9
Outputs:
- up_sampler: bfloat16 [16, 2048, 1024], P(('grp', 'tp')), parts along dimension 0
- down_sampler: bfloat16 [16, 1024, 2048], P(('grp', 'tp')), parts along dimension 0
- layer_out: bfloat16 [32768, 2048], P(('grp', 'fs', 'tp')), parts along dimension 0
There are 2 independent parts, one for each index of `grp`. A program takes and returns all parts, laid end to end along the dimension named above; an argument that names none is the same for every part. Nothing has to cross between parts.
All inputs are finite; a program needn't handle non-finite values.
Results may differ from a plain program's by a relative error of at most 0.014.
Values may be sent and summed in bfloat16 or wider, within the bound.
No kernel may reach another device: no remote copies, remote signals or barrier semaphores. Data moves between devices by JAX's collectives and lax.ppermute only.
A program may use at most 64 MiB of HBM per device.

v0:
```python
import jax
import jax.numpy as jnp
from jax import lax
from jax.experimental import pallas as pl
from jax.experimental.pallas import tpu as pltpu
from jax.sharding import PartitionSpec as P


eps = 1e-06


def place(z, moves, outs, n_fs, earlier=None):
    pieces = []
    for move in moves:
        if not any(move[0] is piece for piece in pieces):
            pieces.append(move[0])
    at = [next(k for k, piece in enumerate(pieces) if piece is move[0]) for move in moves]
    n_old = 0 if earlier is None else len(earlier)

    def body(z_ref, *refs):
        ins = refs[: len(pieces)]
        out_refs = refs[len(pieces) + n_old : len(pieces) + n_old + len(outs)]
        sems = refs[-1]
        copies = []
        for k, (_, row, rows, out, offset, block, within, col) in enumerate(moves):
            home = lax.rem(z_ref[0] + (offset + n_fs), n_fs)
            start = pl.multiple_of(home * block + within, 16)
            src = ins[at[k]]
            dst = out_refs[out].at[pl.ds(start, rows), pl.ds(col, src.shape[1])]
            copies.append(pltpu.make_async_copy(src.at[pl.ds(row, rows)], dst, sems.at[k]))
        for copy in copies:
            copy.start()
        for copy in copies:
            copy.wait()

    anywhere = pl.BlockSpec(memory_space=pl.ANY)
    old = [] if earlier is None else list(earlier)
    return pl.pallas_call(
        body,
        out_shape=outs,
        in_specs=[pl.BlockSpec(memory_space=pltpu.SMEM)]
        + [pl.BlockSpec(memory_space=pltpu.VMEM)] * len(pieces)
        + [anywhere] * n_old,
        out_specs=[anywhere] * len(outs),
        scratch_shapes=[pltpu.SemaphoreType.DMA((len(moves),))],
        input_output_aliases={1 + len(pieces) + k: k for k in range(n_old)},
    )(z.reshape(1), *pieces, *old)


def on_device(prompt_rows, up_master, down_master, norm_gain):
    n_fs = lax.axis_size("fs")
    n_tp = lax.axis_size("tp")
    n_x = n_tp // 2
    half = n_fs // 2
    z = lax.axis_index("fs")
    tp = lax.axis_index("tp")
    x = tp // 2
    core = tp % 2

    up_rows, width = up_master.shape
    span = width // n_fs
    per_tp = n_fs // n_tp
    piece = per_tp * span
    down_cols = down_master.shape[1]
    full = down_cols * n_tp
    folds = down_cols // piece
    sides = full // width

    up_cast = (up_master * norm_gain[:, None]).astype(jnp.bfloat16)
    down_cast = down_master.astype(jnp.bfloat16)
    up_parts = up_cast.reshape(up_rows, per_tp, n_tp, span).transpose(2, 0, 1, 3)
    up_parts = up_parts.reshape(n_tp, 1, up_rows, piece)
    down_parts = down_cast.reshape(n_tp, span, folds, piece).transpose(0, 2, 1, 3)
    down_parts = down_parts.reshape(n_tp, 1, folds * span, piece)
    parts = jnp.concatenate([up_parts, down_parts], axis=1)
    parts = lax.all_to_all(parts, "tp", split_axis=0, concat_axis=0, tiled=True)
    up_own = parts[:, 0].transpose(1, 0, 2).reshape(up_rows, width)
    down_own = parts[:, 1].reshape(sides, n_tp // sides, folds, span, piece)
    down_own = down_own.transpose(0, 3, 1, 2, 4).reshape(sides * span, width)

    own = jnp.concatenate([up_own, down_own], axis=0)

    fore = [(k, (k + 1) % n_fs) for k in range(n_fs)]
    back = [(k, (k - 1) % n_fs) for k in range(n_fs)]
    held = {0: own}
    for step in range(1, half):
        held[-step] = lax.ppermute(held[1 - step], "fs", fore)
        held[step] = lax.ppermute(held[step - 1], "fs", back)
    up_far = lax.ppermute(held[1 - half][:up_rows], "fs", fore)
    down_far = lax.ppermute(held[half - 1][up_rows:], "fs", back)

    def up_moves(keys):
        return [(held[k], 0, up_rows, 0, k, up_rows, 0, 0) for k in keys]

    def down_moves(keys):
        return [
            (held[k], up_rows + s * span, span, 0, k, span, 0, s * width)
            for k in keys
            for s in range(sides)
        ]

    near = half - 3
    early = [k for k in held if abs(k) <= near]
    late = [k for k in held if abs(k) > near]
    up_shape = [jax.ShapeDtypeStruct((n_fs * up_rows, width), jnp.bfloat16)]
    down_shape = [jax.ShapeDtypeStruct((n_fs * span, full), jnp.bfloat16)]
    blank = jnp.zeros((up_rows, width), jnp.bfloat16)
    moves = up_moves(early)
    moves += [(blank, 0, up_rows, 0, k, up_rows, 0, 0) for k in late + [half]]
    up_sampler = place(z, moves, up_shape, n_fs)
    down_sampler = place(z, down_moves(early), down_shape, n_fs)

    tokens = prompt_rows.shape[0]
    block = tokens // n_tp
    order = [(dx % n_x, dc) for dc in (1, 0) for dx in range(1, n_x + 1)]
    rows = [
        lax.dynamic_slice_in_dim(
            prompt_rows, ((x + dx) % n_x * 2 + (core + dc) % 2) * block, block, axis=0
        )
        for dx, dc in order
    ]
    values = lax.optimization_barrier(jnp.concatenate(rows, axis=0)).astype(jnp.float32)
    normed = (values * lax.rsqrt(jnp.mean(values * values, axis=-1, keepdims=True) + eps)).astype(
        jnp.bfloat16
    )
    normed = lax.optimization_barrier(normed)
    pre_act = jnp.dot(normed, up_sampler[0], preferred_element_type=jnp.float32)
    pre_act = lax.optimization_barrier(pre_act)

    rest = [held[k][:up_rows] for k in late] + [up_far]
    rest = jnp.concatenate(rest, axis=0)
    features = [
        lax.dynamic_slice_in_dim(normed, (z + n_fs + k) % n_fs * up_rows, up_rows, axis=1)
        for k in late + [half]
    ]
    features = lax.optimization_barrier(jnp.concatenate(features, axis=1))
    pre_act = pre_act + jnp.dot(features, rest, preferred_element_type=jnp.float32)
    hidden = jnp.square(jax.nn.relu(pre_act)).astype(jnp.bfloat16)

    moves = down_moves(late)
    moves += [(down_far, k * span, span, 0, half, span, 0, k * width) for k in range(sides)]
    down_sampler = place(z, moves, down_shape, n_fs, down_sampler)[0]
    moves = up_moves(late)
    moves += [(up_far, 0, up_rows, 0, half, up_rows, 0, 0)]
    up_sampler = place(z, moves, up_shape, n_fs, up_sampler)[0]

    pair = [(k, k ^ 1) for k in range(n_tp)]
    hops = [[(j, (j + 2 * dx) % n_tp) for j in range(n_tp)] for dx in range(1, n_x)]
    bounds = [0, 3 * full // 8, full]
    sums = []
    for lo, hi in zip(bounds[:-1], bounds[1:]):
        weights = lax.slice_in_dim(down_sampler, lo, hi, axis=1)
        partial = jnp.dot(hidden, weights, preferred_element_type=jnp.float32).astype(jnp.bfloat16)
        theirs = lax.ppermute(partial[: tokens // 2], "tp", pair)
        chip = partial[tokens // 2 :].astype(jnp.float32) + theirs.astype(jnp.float32)
        total = chip[(n_x - 1) * block :]
        chip = chip[: (n_x - 1) * block].astype(jnp.bfloat16)
        for k, hop in enumerate(hops):
            sent = chip[k * block : (k + 1) * block]
            total = total + lax.ppermute(sent, "tp", hop).astype(jnp.float32)
        sums.append(total.astype(jnp.bfloat16))
    return (up_sampler[None], down_sampler[None], jnp.concatenate(sums, axis=1))


def solution(mesh):
    in_specs = (P(("grp", "fs"), None), P("fs", "tp"), P("fs", "tp"), P("fs"))
    out_specs = (
        P(("grp", "tp"), None, None),
        P(("grp", "tp"), None, None),
        P(("grp", "fs", "tp"), None),
    )

    return jax.shard_map(
        on_device, mesh=mesh, in_specs=in_specs, out_specs=out_specs, check_vma=False
    )
```

profile of v0, /device:TPU:40, one launch (start us, length us, event | category | flops | bytes accessed | tf_op | source)
XLA Modules:
  0.0 199.5 jit_solution(17846369218981634382)
XLA Ops:
  0.6 1.1 convert_element_type.60
  2.0 1.2 copy.34
  3.3 0.7 multiply_convert_fusion.1
  4.1 14.7 %all_to_all.5 = bf16[8,2,128,128]{2,3,1,0:T(8,128)(2,1)S(1)} all-to-all(bf16[8,2,128,128]{2,3,1,0:T(8,128)(2,1)S(1)} %copy.38), channel_id=1, replica_groups=mesh['grp'=2,'fs'=16,'tp'=8] {'tp'}, dimensions={0} | all-to-all | bytes 1048576 | tf_op jit(solution)/shard_map/all_to_all | solution.py:76
  19.2 0.3 copy.41
  19.7 2.9 %collective-permute-start = (bf16[256,1024]{1,0:T(8,128)(2,1)S(1)}, bf16[256,1024]{1,0:T(8,128)(2,1)S(1)}, u32[]{:S(2)}, u32[]{:S(2)}) collective-permute-start(bf16[256,1024]{1,0:T(8,128)(2,1)S(1)} %pad_maximum_fusion.1.refs_0_), channel_id=1, source_target_pairs={{0,8},{8,16},{16,24},{24,32},{32,40},{40,48},{48,56},{56,64},{64,7... | collective-permute-start | bytes 1572872 | tf_op jit(solution)/shard_map/ppermute | solution.py:87
  22.6 19.7 %collective-permute-start.6 = (bf16[256,1024]{1,0:T(8,128)(2,1)S(1)}, bf16[256,1024]{1,0:T(8,128)(2,1)S(1)}, u32[]{:S(2)}, u32[]{:S(2)}) collective-permute-start(bf16[256,1024]{1,0:T(8,128)(2,1)S(1)} %pad_maximum_fusion.1.refs_0_), channel_id=1, source_target_pairs={{0,120},{8,0},{16,8},{24,16},{32,24},{40,32},{48,40},{56,48},{64,5... | collective-permute-start | bytes 1572872 | tf_op jit(solution)/shard_map/ppermute | solution.py:88
  42.3 11.4 %collective-permute-done.refs_1_ = bf16[256,1024]{1,0:T(8,128)(2,1)S(1)} collective-permute-done((bf16[256,1024]{1,0:T(8,128)(2,1)S(1)}, bf16[256,1024]{1,0:T(8,128)(2,1)S(1)}, u32[]{:S(2)}, u32[]{:S(2)}) %collective-permute-start) | collective-permute-done | bytes 524320 | tf_op jit(solution)/shard_map/ppermute | solution.py:87
  53.8 2.1 %dynamic-slice_dynamic-update-slice_fusion.7 = bf16[1024,2048]{1,0:T(8,128)(2,1)} fusion(bf16[1024,2048]{1,0:T(8,128)(2,1)} %param.4, s32[]{:T(128)S(6)} %select_n.118), kind=kLoop, calls=%fused_computation.25 | loop fusion | bytes 1048580
  55.8 1.9 dynamic-slice_dynamic-update-slice_fusion.6
  57.7 3.0 %collective-permute-start.7 = (bf16[256,1024]{1,0:T(8,128)(2,1)S(1)}, bf16[256,1024]{1,0:T(8,128)(2,1)S(1)}, u32[]{:S(2)}, u32[]{:S(2)}) collective-permute-start(bf16[256,1024]{1,0:T(8,128)(2,1)S(1)} %collective-permute-done.6.refs_2_), channel_id=1, source_target_pairs={{0,120},{8,0},{16,8},{24,16},{32,24},{40,32},{48,40},{56,48},{64,5... | collective-permute-start | bytes 1572872 | tf_op jit(solution)/shard_map/ppermute | solution.py:88
  60.8 6.9 %collective-permute-done.1.refs_3_ = bf16[256,1024]{1,0:T(8,128)(2,1)S(1)} collective-permute-done((bf16[256,1024]{1,0:T(8,128)(2,1)S(1)}, bf16[256,1024]{1,0:T(8,128)(2,1)S(1)}, u32[]{:S(2)}, u32[]{:S(2)}) %collective-permute-start.1) | collective-permute-done | bytes 524320 | tf_op jit(solution)/shard_map/ppermute | solution.py:87
  67.7 2.1 %dynamic-slice_dynamic-update-slice_fusion.5 = bf16[1024,2048]{1,0:T(8,128)(2,1)} fusion(bf16[1024,2048]{1,0:T(8,128)(2,1)} %dynamic-slice_dynamic-update-slice_fusion.6, bf16[1024,2048]{1,0:T(8,128)(2,1)} %param.4, s32[]{:T(128)S(6)} %select_n.122), kind=kLoop, calls=%fused_computation.23 | loop fusion | bytes 1048580
  69.8 1.9 dynamic-slice_dynamic-update-slice_fusion.4
  71.7 1.9 dynamic-slice_dynamic-update-slice_fusion.3
  73.5 3.0 %collective-permute-start.8 = (bf16[256,1024]{1,0:T(8,128)(2,1)S(1)}, bf16[256,1024]{1,0:T(8,128)(2,1)}, u32[]{:S(2)}, u32[]{:S(2)}) collective-permute-start(bf16[256,1024]{1,0:T(8,128)(2,1)S(1)} %collective-permute-done.7.refs_4_), channel_id=1, source_target_pairs={{0,120},{8,0},{16,8},{24,16},{32,24},{40,32},{48,40},{56,48},{64,5... | collective-permute-start | bytes 1572872 | tf_op jit(solution)/shard_map/ppermute | solution.py:88
  76.6 4.2 %collective-permute-done.2.refs_5_ = bf16[256,1024]{1,0:T(8,128)(2,1)S(1)} collective-permute-done((bf16[256,1024]{1,0:T(8,128)(2,1)S(1)}, bf16[256,1024]{1,0:T(8,128)(2,1)S(1)}, u32[]{:S(2)}, u32[]{:S(2)}) %collective-permute-start.2) | collective-permute-done | bytes 524320 | tf_op jit(solution)/shard_map/ppermute | solution.py:87
  80.8 2.1 %dynamic-slice_dynamic-update-slice_fusion.2 = bf16[1024,2048]{1,0:T(8,128)(2,1)} fusion(bf16[1024,2048]{1,0:T(8,128)(2,1)} %dynamic-slice_dynamic-update-slice_fusion.3, bf16[1024,2048]{1,0:T(8,128)(2,1)} %param.4, s32[]{:T(128)S(6)} %select_n.127), kind=kLoop, calls=%fused_computation.20 | loop fusion | bytes 1048580
  82.9 1.9 dynamic-slice_dynamic-update-slice_fusion.1
  84.7 1.9 dynamic-slice_dynamic-update-slice_fusion
  86.6 3.2 %collective-permute-start.9 = (bf16[256,1024]{1,0:T(8,128)(2,1)}, bf16[256,1024]{1,0:T(8,128)(2,1)S(1)}, u32[]{:S(2)}, u32[]{:S(2)}) collective-permute-start(bf16[256,1024]{1,0:T(8,128)(2,1)} %collective-permute-done.8.refs_6_), channel_id=1, source_target_pairs={{0,120},{8,0},{16,8},{24,16},{32,24},{40,32},{48,40},{56,48},{64,5... | collective-permute-start | bytes 1572872 | tf_op jit(solution)/shard_map/ppermute | solution.py:88
  89.8 3.3 %collective-permute-done.3.refs_7_ = bf16[256,1024]{1,0:T(8,128)(2,1)} collective-permute-done((bf16[256,1024]{1,0:T(8,128)(2,1)S(1)}, bf16[256,1024]{1,0:T(8,128)(2,1)}, u32[]{:S(2)}, u32[]{:S(2)}) %collective-permute-start.3) | collective-permute-done | bytes 524320 | tf_op jit(solution)/shard_map/ppermute | solution.py:87
  93.1 3.1 %fusion = f32[1024]{0:T(1024)S(1)} fusion(bf16[1024,2048]{1,0:T(8,128)(2,1)} %dynamic-slice_dynamic-update-slice_fusion), kind=kLoop, calls=%fused_computation.2 | loop fusion | flops 6290432 | bytes 4198400 | tf_op jit(solution)/shard_map/reduce_sum | solution.py:123
  96.2 2.7 %collective-permute-done.9.refs_8_ = bf16[256,1024]{1,0:T(8,128)(2,1)S(1)} collective-permute-done((bf16[256,1024]{1,0:T(8,128)(2,1)}, bf16[256,1024]{1,0:T(8,128)(2,1)S(1)}, u32[]{:S(2)}, u32[]{:S(2)}) %collective-permute-start.9) | collective-permute-done | bytes 524320 | tf_op jit(solution)/shard_map/ppermute | solution.py:88
  98.9 3.1 %collective-permute-start.10 = (bf16[256,1024]{1,0:T(8,128)(2,1)S(1)}, bf16[256,1024]{1,0:T(8,128)(2,1)S(1)}, u32[]{:S(2)}, u32[]{:S(2)}) collective-permute-start(bf16[256,1024]{1,0:T(8,128)(2,1)S(1)} %collective-permute-done.9.refs_8_), channel_id=1, source_target_pairs={{0,120},{8,0},{16,8},{24,16},{32,24},{40,32},{48,40},{56,48},{64,5... | collective-permute-start | bytes 1572872 | tf_op jit(solution)/shard_map/ppermute | solution.py:88
  102.1 3.3 %collective-permute-done.4.refs_9_ = bf16[256,1024]{1,0:T(8,128)(2,1)S(1)} collective-permute-done((bf16[256,1024]{1,0:T(8,128)(2,1)}, bf16[256,1024]{1,0:T(8,128)(2,1)S(1)}, u32[]{:S(2)}, u32[]{:S(2)}) %collective-permute-start.4) | collective-permute-done | bytes 524320 | tf_op jit(solution)/shard_map/ppermute | solution.py:87
  105.4 5.1 %fusion.1 = bf16[1024,2048]{1,0:T(8,128)(2,1)} fusion(bf16[1024,2048]{1,0:T(8,128)(2,1)} %dynamic-slice_dynamic-update-slice_fusion, f32[1024]{0:T(1024)S(1)} %add_rsqrt_fusion), kind=kLoop, calls=%fused_computation.3 | loop fusion | flops 6291456 | bytes 8392704 | tf_op jit(solution)/shard_map/convert_element_type | solution.py:123
  110.6 3.6 %collective-permute-start.11 = (bf16[256,1024]{1,0:T(8,128)(2,1)S(1)}, bf16[256,1024]{1,0:T(8,128)(2,1)S(1)}, u32[]{:S(2)}, u32[]{:S(2)}) collective-permute-start(bf16[256,1024]{1,0:T(8,128)(2,1)S(1)} %collective-permute-done.10.refs_10_), channel_id=1, source_target_pairs={{0,120},{8,0},{16,8},{24,16},{32,24},{40,32},{48,40},{56,48},{64,5... | collective-permute-start | bytes 1572872 | tf_op jit(solution)/shard_map/ppermute | solution.py:88
  114.2 1.7 dynamic-slice_dynamic-update-slice_fusion.12
  115.9 1.7 dynamic-slice_dynamic-update-slice_fusion.11
  117.6 1.7 dynamic-slice_dynamic-update-slice_fusion.10
  119.3 1.7 dynamic-slice_dynamic-update-slice_fusion.9
  121.0 1.9 dynamic-slice_dynamic-update-slice_fusion.8
  122.9 0.7 broadcast_in_dim.11.refs_11_
  123.6 4.8 %shard_map.67.refs_5_ = bf16[2048,1024]{1,0:T(8,128)(2,1)} custom-call(s32[1]{0:T(128)} %bitcast.z_ref, bf16[256,1024]{1,0:T(8,128)(2,1)} %copy-done.1, bf16[256,1024]{1,0:T(8,128)(2,1)} %copy-done.7, bf16[256,1024]{1,0:T(8,128)(2,1)} %copy-done.8, bf16[256,1024]{1,0:T(8,128)(2,1)} %copy-done.9, bf16[256,1024]{1,0:T(8,128)(2,1)} %copy-done.10, ...), custom_call_target="tpu_custom_call" | custom-call | tf_op jit(solution)/shard_map/pallas_call | solution.py:38
  128.5 3.1 %collective-permute-start.13 = (bf16[256,1024]{1,0:T(8,128)(2,1)S(1)}, bf16[256,1024]{1,0:T(8,128)(2,1)S(1)}, u32[]{:S(2)}, u32[]{:S(2)}) collective-permute-start(bf16[256,1024]{1,0:T(8,128)(2,1)S(1)} %collective-permute-done.11.refs_1_), channel_id=1, source_target_pairs={{0,120},{8,0},{16,8},{24,16},{32,24},{40,32},{48,40},{56,48},{64,5... | collective-permute-start | bytes 1572872 | tf_op jit(solution)/shard_map/ppermute | solution.py:88
  131.7 1.0 collective-permute-done.12.refs_2_
  132.7 1.2 copy-done.17
  133.9 9.9 %fusion.15 = f32[1024,1024]{1,0:T(8,128)} fusion(bf16[1024,2048]{1,0:T(8,128)(2,1)} %fusion.1, bf16[2048,1024]{1,0:T(8,128)(2,1)} %shard_map.67.refs_5_), kind=kOutput, calls=%fused_computation.47 | convolution fusion | flops 4294967296 | bytes 12582912 | tf_op jit(solution)/shard_map/dot_general | solution.py:127
  143.8 4.4 %shard_map.69.refs_5_ = bf16[1024,2048]{1,0:T(8,128)(2,1)} custom-call(s32[1]{0:T(128)} %bitcast.z_ref, bf16[256,1024]{1,0:T(8,128)(2,1)} %copy-done.1, bf16[256,1024]{1,0:T(8,128)(2,1)} %copy-done.7, bf16[256,1024]{1,0:T(8,128)(2,1)} %copy-done.8, bf16[256,1024]{1,0:T(8,128)(2,1)} %copy-done.9, bf16[256,1024]{1,0:T(8,128)(2,1)} %copy-done.10, ...), custom_call_target="tpu_custom_call" | custom-call | tf_op jit(solution)/shard_map/pallas_call | solution.py:38
  148.2 0.8 slice_dynamic-update-slice_fusion
  149.0 3.2 %collective-permute-start.15 = (bf16[128,1024]{1,0:T(8,128)(2,1)S(1)}, bf16[128,1024]{1,0:T(8,128)(2,1)S(1)}, u32[]{:S(2)}, u32[]{:S(2)}) collective-permute-start(bf16[128,1024]{1,0:T(8,128)(2,1)S(1)} %get-tuple-element.14), channel_id=1, source_target_pairs={{0,120},{8,0},{16,8},{24,16},{32,24},{40,32},{48,40},{56,48},{64,5... | collective-permute-start | bytes 786440 | tf_op jit(solution)/shard_map/ppermute | solution.py:90
  152.3 0.8 constant_dynamic-update-slice_fusion
  153.1 3.6 %fusion.16 = f32[1024,1024]{1,0:T(8,128)S(1)} fusion(bf16[1024,640]{1,0:T(8,128)(2,1)} %dynamic-slice_dynamic-update-slice_fusion.8, bf16[640,1024]{1,0:T(8,128)(2,1)} %constant_dynamic-update-slice_fusion), kind=kOutput, calls=%fused_computation.48 | convolution fusion | flops 1342177280 | bytes 6815744 | tf_op jit(solution)/shard_map/dot_general | solution.py:137
  156.7 1.1 multiply_convert_fusion
  157.9 0.7 copy-done.16
  158.6 2.7 %shard_map.70 = bf16[1024,2048]{1,0:T(8,128)(2,1)} custom-call(s32[1]{0:T(128)} %bitcast.z_ref, bf16[256,1024]{1,0:T(8,128)(2,1)} %copy-done.4, bf16[256,1024]{1,0:T(8,128)(2,1)} %copy-done.5, bf16[256,1024]{1,0:T(8,128)(2,1)} %copy-done.6, bf16[256,1024]{1,0:T(8,128)(2,1)} %copy-done.2, ...), custom_call_target="tpu_custom_call", output_to_operand_aliasing={{}: (6, {})} | custom-call | tf_op jit(solution)/shard_map/pallas_call | solution.py:38
  161.3 3.4 %convolution_convert_fusion.1 = bf16[1024,768]{0,1:T(8,128)(2,1)S(1)} fusion(bf16[1024,1024]{1,0:T(8,128)(2,1)S(1)} %multiply_convert_fusion, bf16[1024,2048]{1,0:T(8,128)(2,1)} %shard_map.70), kind=kOutput, calls=%fused_computation.8 | convolution fusion | flops 1611399168 | bytes 5242880 | tf_op jit(solution)/shard_map/dot_general | solution.py:153
  165.0 3.2 %convolution_convert_fusion = bf16[1024,1280]{1,0:T(8,128)(2,1)S(1)} fusion(bf16[1024,1024]{1,0:T(8,128)(2,1)S(1)} %multiply_convert_fusion, bf16[1024,2048]{1,0:T(8,128)(2,1)S(1)} %copy-done), kind=kOutput, calls=%fused_computation.5 | convolution fusion | flops 2685665280 | bytes 7340032 | tf_op jit(solution)/shard_map/dot_general | solution.py:153
  168.2 0.6 collective-permute-start.20
  168.8 1.5 fusion.10
  170.3 0.8 fusion.13
  171.1 0.6 collective-permute-start.17
  171.7 2.7 %collective-permute-start.19 = (bf16[128,768]{0,1:T(8,128)(2,1)}, bf16[128,768]{0,1:T(8,128)(2,1)S(1)}, u32[]{:S(2)}, u32[]{:S(2)}) collective-permute-start(bf16[128,768]{0,1:T(8,128)(2,1)} %get-tuple-element.11), channel_id=1, source_target_pairs={{0,6},{1,7},{2,0},{3,1},{4,2},{5,3},{6,4},{7,5},{8,14},{9,15},{10,... | collective-permute-start | bytes 589832 | tf_op jit(solution)/shard_map/ppermute | solution.py:160
  174.3 0.3 fusion.11
  174.7 1.0 fusion.12
  175.7 0.9 collective-permute-start.21
  176.5 2.4 %collective-permute-start.23 = (bf16[128,1280]{1,0:T(8,128)(2,1)}, bf16[128,1280]{1,0:T(8,128)(2,1)}, u32[]{:S(2)}, u32[]{:S(2)}) collective-permute-start(bf16[128,1280]{1,0:T(8,128)(2,1)} %get-tuple-element.8), channel_id=1, source_target_pairs={{0,6},{1,7},{2,0},{3,1},{4,2},{5,3},{6,4},{7,5},{8,14},{9,15},{10,... | collective-permute-start | bytes 983048 | tf_op jit(solution)/shard_map/ppermute | solution.py:160
  178.9 5.1 %collective-permute-done.17 = bf16[128,768]{0,1:T(8,128)(2,1)S(1)} collective-permute-done((bf16[128,768]{0,1:T(8,128)(2,1)S(1)}, bf16[128,768]{0,1:T(8,128)(2,1)S(1)}, u32[]{:S(2)}, u32[]{:S(2)}) %collective-permute-start.17) | collective-permute-done | bytes 196640 | tf_op jit(solution)/shard_map/ppermute | solution.py:160
  184.0 2.7 %shard_map.68 = bf16[2048,1024]{1,0:T(8,128)(2,1)} custom-call(s32[1]{0:T(128)} %bitcast.z_ref, bf16[256,1024]{1,0:T(8,128)(2,1)} %copy-done.4, bf16[256,1024]{1,0:T(8,128)(2,1)} %copy-done.5, bf16[256,1024]{1,0:T(8,128)(2,1)} %copy-done.6, bf16[256,1024]{1,0:T(8,128)(2,1)} %copy-done.2, ...), custom_call_target="tpu_custom_call", output_to_operand_aliasing={{}: (6, {})} | custom-call | tf_op jit(solution)/shard_map/pallas_call | solution.py:38
  186.7 1.1 fusion.9
  188.0 9.4 %collective-permute-done.21 = bf16[128,1280]{1,0:T(8,128)(2,1)S(1)} collective-permute-done((bf16[128,1280]{1,0:T(8,128)(2,1)}, bf16[128,1280]{1,0:T(8,128)(2,1)S(1)}, u32[]{:S(2)}, u32[]{:S(2)}) %collective-permute-start.21) | collective-permute-done | bytes 327712 | tf_op jit(solution)/shard_map/ppermute | solution.py:160
  197.4 1.2 fusion.6
  198.7 0.8 pad_maximum_fusion.2
  (77 shorter events, 1.6 us)
Async XLA Ops:
  19.7 66.9 %copy-start.1 = (bf16[256,1024]{1,0:T(8,128)(2,1)}, bf16[256,1024]{1,0:T(8,128)(2,1)S(1)}, u32[]{:S(2)}) copy-start(bf16[256,1024]{1,0:T(8,128)(2,1)S(1)} %pad_maximum_fusion.1.refs_0_) | copy-start | bytes 1572868
  19.7 34.1 %collective-permute-start = (bf16[256,1024]{1,0:T(8,128)(2,1)S(1)}, bf16[256,1024]{1,0:T(8,128)(2,1)S(1)}, u32[]{:S(2)}, u32[]{:S(2)}) collective-permute-start(bf16[256,1024]{1,0:T(8,128)(2,1)S(1)} %pad_maximum_fusion.1.refs_0_), channel_id=1, source_target_pairs={{0,8},{8,16},{16,24},{24,32},{32,40},{40,48},{48,56},{56,64},{64,7... | collective-permute-start | bytes 1572872 | tf_op jit(solution)/shard_map/ppermute | solution.py:87
  22.6 35.1 %collective-permute-start.6 = (bf16[256,1024]{1,0:T(8,128)(2,1)S(1)}, bf16[256,1024]{1,0:T(8,128)(2,1)S(1)}, u32[]{:S(2)}, u32[]{:S(2)}) collective-permute-start(bf16[256,1024]{1,0:T(8,128)(2,1)S(1)} %pad_maximum_fusion.1.refs_0_), channel_id=1, source_target_pairs={{0,120},{8,0},{16,8},{24,16},{32,24},{40,32},{48,40},{56,48},{64,5... | collective-permute-start | bytes 1572872 | tf_op jit(solution)/shard_map/ppermute | solution.py:88
  53.8 32.9 %copy-start.7 = (bf16[256,1024]{1,0:T(8,128)(2,1)}, bf16[256,1024]{1,0:T(8,128)(2,1)S(1)}, u32[]{:S(2)}) copy-start(bf16[256,1024]{1,0:T(8,128)(2,1)S(1)} %collective-permute-done.refs_1_) | copy-start | bytes 1572868
  53.8 13.9 %collective-permute-start.1 = (bf16[256,1024]{1,0:T(8,128)(2,1)S(1)}, bf16[256,1024]{1,0:T(8,128)(2,1)S(1)}, u32[]{:S(2)}, u32[]{:S(2)}) collective-permute-start(bf16[256,1024]{1,0:T(8,128)(2,1)S(1)} %collective-permute-done.refs_1_), channel_id=1, source_target_pairs={{0,8},{8,16},{16,24},{24,32},{32,40},{40,48},{48,56},{56,64},{64,7... | collective-permute-start | bytes 1572872 | tf_op jit(solution)/shard_map/ppermute | solution.py:87
  57.7 38.5 %copy-start.8 = (bf16[256,1024]{1,0:T(8,128)(2,1)}, bf16[256,1024]{1,0:T(8,128)(2,1)S(1)}, u32[]{:S(2)}) copy-start(bf16[256,1024]{1,0:T(8,128)(2,1)S(1)} %collective-permute-done.6.refs_2_) | copy-start | bytes 1572868
  57.7 15.8 %collective-permute-start.7 = (bf16[256,1024]{1,0:T(8,128)(2,1)S(1)}, bf16[256,1024]{1,0:T(8,128)(2,1)S(1)}, u32[]{:S(2)}, u32[]{:S(2)}) collective-permute-start(bf16[256,1024]{1,0:T(8,128)(2,1)S(1)} %collective-permute-done.6.refs_2_), channel_id=1, source_target_pairs={{0,120},{8,0},{16,8},{24,16},{32,24},{40,32},{48,40},{56,48},{64,5... | collective-permute-start | bytes 1572872 | tf_op jit(solution)/shard_map/ppermute | solution.py:88
  67.7 28.5 %copy-start.9 = (bf16[256,1024]{1,0:T(8,128)(2,1)}, bf16[256,1024]{1,0:T(8,128)(2,1)S(1)}, u32[]{:S(2)}) copy-start(bf16[256,1024]{1,0:T(8,128)(2,1)S(1)} %collective-permute-done.1.refs_3_) | copy-start | bytes 1572868
  67.7 13.1 %collective-permute-start.2 = (bf16[256,1024]{1,0:T(8,128)(2,1)S(1)}, bf16[256,1024]{1,0:T(8,128)(2,1)S(1)}, u32[]{:S(2)}, u32[]{:S(2)}) collective-permute-start(bf16[256,1024]{1,0:T(8,128)(2,1)S(1)} %collective-permute-done.1.refs_3_), channel_id=1, source_target_pairs={{0,8},{8,16},{16,24},{24,32},{32,40},{40,48},{48,56},{56,64},{64,7... | collective-permute-start | bytes 1572872 | tf_op jit(solution)/shard_map/ppermute | solution.py:87
  73.5 37.0 %copy-start.10 = (bf16[256,1024]{1,0:T(8,128)(2,1)}, bf16[256,1024]{1,0:T(8,128)(2,1)S(1)}, u32[]{:S(2)}) copy-start(bf16[256,1024]{1,0:T(8,128)(2,1)S(1)} %collective-permute-done.7.refs_4_) | copy-start | bytes 1572868
  73.5 13.1 %collective-permute-start.8 = (bf16[256,1024]{1,0:T(8,128)(2,1)S(1)}, bf16[256,1024]{1,0:T(8,128)(2,1)}, u32[]{:S(2)}, u32[]{:S(2)}) collective-permute-start(bf16[256,1024]{1,0:T(8,128)(2,1)S(1)} %collective-permute-done.7.refs_4_), channel_id=1, source_target_pairs={{0,120},{8,0},{16,8},{24,16},{32,24},{40,32},{48,40},{56,48},{64,5... | collective-permute-start | bytes 1572872 | tf_op jit(solution)/shard_map/ppermute | solution.py:88
  80.8 21.3 %copy-start.11 = (bf16[256,1024]{1,0:T(8,128)(2,1)}, bf16[256,1024]{1,0:T(8,128)(2,1)S(1)}, u32[]{:S(2)}) copy-start(bf16[256,1024]{1,0:T(8,128)(2,1)S(1)} %collective-permute-done.2.refs_5_) | copy-start | bytes 1572868
  80.8 12.3 %collective-permute-start.3 = (bf16[256,1024]{1,0:T(8,128)(2,1)S(1)}, bf16[256,1024]{1,0:T(8,128)(2,1)}, u32[]{:S(2)}, u32[]{:S(2)}) collective-permute-start(bf16[256,1024]{1,0:T(8,128)(2,1)S(1)} %collective-permute-done.2.refs_5_), channel_id=1, source_target_pairs={{0,8},{8,16},{16,24},{24,32},{32,40},{40,48},{48,56},{56,64},{64,7... | collective-permute-start | bytes 1572872 | tf_op jit(solution)/shard_map/ppermute | solution.py:87
  86.6 12.3 %collective-permute-start.9 = (bf16[256,1024]{1,0:T(8,128)(2,1)}, bf16[256,1024]{1,0:T(8,128)(2,1)S(1)}, u32[]{:S(2)}, u32[]{:S(2)}) collective-permute-start(bf16[256,1024]{1,0:T(8,128)(2,1)} %collective-permute-done.8.refs_6_), channel_id=1, source_target_pairs={{0,120},{8,0},{16,8},{24,16},{32,24},{40,32},{48,40},{56,48},{64,5... | collective-permute-start | bytes 1572872 | tf_op jit(solution)/shard_map/ppermute | solution.py:88
  93.1 12.3 %collective-permute-start.4 = (bf16[256,1024]{1,0:T(8,128)(2,1)}, bf16[256,1024]{1,0:T(8,128)(2,1)S(1)}, u32[]{:S(2)}, u32[]{:S(2)}) collective-permute-start(bf16[256,1024]{1,0:T(8,128)(2,1)} %collective-permute-done.3.refs_7_), channel_id=1, source_target_pairs={{0,8},{8,16},{16,24},{24,32},{32,40},{40,48},{48,56},{56,64},{64,7... | collective-permute-start | bytes 1572872 | tf_op jit(solution)/shard_map/ppermute | solution.py:87
  98.9 11.6 %copy-start.12 = (bf16[256,1024]{1,0:T(8,128)(2,1)}, bf16[256,1024]{1,0:T(8,128)(2,1)S(1)}, u32[]{:S(2)}) copy-start(bf16[256,1024]{1,0:T(8,128)(2,1)S(1)} %collective-permute-done.9.refs_8_) | copy-start | bytes 1572868
  98.9 11.6 %collective-permute-start.10 = (bf16[256,1024]{1,0:T(8,128)(2,1)S(1)}, bf16[256,1024]{1,0:T(8,128)(2,1)S(1)}, u32[]{:S(2)}, u32[]{:S(2)}) collective-permute-start(bf16[256,1024]{1,0:T(8,128)(2,1)S(1)} %collective-permute-done.9.refs_8_), channel_id=1, source_target_pairs={{0,120},{8,0},{16,8},{24,16},{32,24},{40,32},{48,40},{56,48},{64,5... | collective-permute-start | bytes 1572872 | tf_op jit(solution)/shard_map/ppermute | solution.py:88
  105.4 5.1 %copy-start.13 = (bf16[256,1024]{1,0:T(8,128)(2,1)}, bf16[256,1024]{1,0:T(8,128)(2,1)S(1)}, u32[]{:S(2)}) copy-start(bf16[256,1024]{1,0:T(8,128)(2,1)S(1)} %collective-permute-done.4.refs_9_) | copy-start | bytes 1572868
  105.4 15.6 %collective-permute-start.5 = (bf16[256,1024]{1,0:T(8,128)(2,1)S(1)}, bf16[256,1024]{1,0:T(8,128)(2,1)S(1)}, u32[]{:S(2)}, u32[]{:S(2)}) collective-permute-start(bf16[256,1024]{1,0:T(8,128)(2,1)S(1)} %collective-permute-done.4.refs_9_), channel_id=1, source_target_pairs={{0,8},{8,16},{16,24},{24,32},{32,40},{40,48},{48,56},{56,64},{64,7... | collective-permute-start | bytes 1572872 | tf_op jit(solution)/shard_map/ppermute | solution.py:87
  110.6 13.0 %copy-start.14 = (bf16[256,1024]{1,0:T(8,128)(2,1)}, bf16[256,1024]{1,0:T(8,128)(2,1)S(1)}, u32[]{:S(2)}) copy-start(bf16[256,1024]{1,0:T(8,128)(2,1)S(1)} %collective-permute-done.10.refs_10_) | copy-start | bytes 1572868
  110.6 17.8 %collective-permute-start.11 = (bf16[256,1024]{1,0:T(8,128)(2,1)S(1)}, bf16[256,1024]{1,0:T(8,128)(2,1)S(1)}, u32[]{:S(2)}, u32[]{:S(2)}) collective-permute-start(bf16[256,1024]{1,0:T(8,128)(2,1)S(1)} %collective-permute-done.10.refs_10_), channel_id=1, source_target_pairs={{0,120},{8,0},{16,8},{24,16},{32,24},{40,32},{48,40},{56,48},{64,5... | collective-permute-start | bytes 1572872 | tf_op jit(solution)/shard_map/ppermute | solution.py:88
  121.0 10.6 %copy-start.4 = (bf16[256,1024]{1,0:T(8,128)(2,1)}, bf16[256,1024]{1,0:T(8,128)(2,1)S(1)}, u32[]{:S(2)}) copy-start(bf16[256,1024]{1,0:T(8,128)(2,1)S(1)} %collective-permute-done.5.refs_0_) | copy-start | bytes 1572868
  121.0 11.7 %collective-permute-start.12 = (bf16[256,1024]{1,0:T(8,128)(2,1)S(1)}, bf16[256,1024]{1,0:T(8,128)(2,1)S(1)}, u32[]{:S(2)}, u32[]{:S(2)}) collective-permute-start(bf16[256,1024]{1,0:T(8,128)(2,1)S(1)} %collective-permute-done.5.refs_0_), channel_id=1, source_target_pairs={{0,8},{8,16},{16,24},{24,32},{32,40},{40,48},{48,56},{56,64},{64,7... | collective-permute-start | bytes 1572872 | tf_op jit(solution)/shard_map/ppermute | solution.py:87
  128.4 15.4 %copy-start.5 = (bf16[256,1024]{1,0:T(8,128)(2,1)}, bf16[256,1024]{1,0:T(8,128)(2,1)S(1)}, u32[]{:S(2)}) copy-start(bf16[256,1024]{1,0:T(8,128)(2,1)S(1)} %collective-permute-done.11.refs_1_) | copy-start | bytes 1572868
  128.5 19.7 %collective-permute-start.13 = (bf16[256,1024]{1,0:T(8,128)(2,1)S(1)}, bf16[256,1024]{1,0:T(8,128)(2,1)S(1)}, u32[]{:S(2)}, u32[]{:S(2)}) collective-permute-start(bf16[256,1024]{1,0:T(8,128)(2,1)S(1)} %collective-permute-done.11.refs_1_), channel_id=1, source_target_pairs={{0,120},{8,0},{16,8},{24,16},{32,24},{40,32},{48,40},{56,48},{64,5... | collective-permute-start | bytes 1572872 | tf_op jit(solution)/shard_map/ppermute | solution.py:88
  132.7 11.1 %copy-start.6 = (bf16[256,1024]{1,0:T(8,128)(2,1)}, bf16[256,1024]{1,0:T(8,128)(2,1)S(1)}, u32[]{:S(2)}) copy-start(bf16[256,1024]{1,0:T(8,128)(2,1)S(1)} %collective-permute-done.12.refs_2_) | copy-start | bytes 1572868
  132.7 1.2 copy-start.17
  133.9 18.4 %collective-permute-start.14 = (bf16[128,1024]{1,0:T(8,128)(2,1)S(1)}, bf16[128,1024]{1,0:T(8,128)(2,1)S(1)}, u32[]{:S(2)}, u32[]{:S(2)}) collective-permute-start(bf16[128,1024]{1,0:T(8,128)(2,1)S(1)} %get-tuple-element.16), channel_id=1, source_target_pairs={{0,8},{8,16},{16,24},{24,32},{32,40},{40,48},{48,56},{56,64},{64,7... | collective-permute-start | bytes 786440 | tf_op jit(solution)/shard_map/ppermute | solution.py:89
  148.2 8.5 %copy-start.2 = (bf16[256,1024]{1,0:T(8,128)(2,1)}, bf16[256,1024]{1,0:T(8,128)(2,1)S(1)}, u32[]{:S(2)}) copy-start(bf16[256,1024]{1,0:T(8,128)(2,1)S(1)} %collective-permute-done.13.refs_3_) | copy-start | bytes 1572868
  149.0 8.9 %collective-permute-start.15 = (bf16[128,1024]{1,0:T(8,128)(2,1)S(1)}, bf16[128,1024]{1,0:T(8,128)(2,1)S(1)}, u32[]{:S(2)}, u32[]{:S(2)}) collective-permute-start(bf16[128,1024]{1,0:T(8,128)(2,1)S(1)} %get-tuple-element.14), channel_id=1, source_target_pairs={{0,120},{8,0},{16,8},{24,16},{32,24},{40,32},{48,40},{56,48},{64,5... | collective-permute-start | bytes 786440 | tf_op jit(solution)/shard_map/ppermute | solution.py:90
  152.3 4.5 %copy-start.15 = (bf16[128,1024]{1,0:T(8,128)(2,1)}, bf16[128,1024]{1,0:T(8,128)(2,1)S(1)}, u32[]{:S(2)}) copy-start(bf16[128,1024]{1,0:T(8,128)(2,1)S(1)} %collective-permute-done.14.refs_4_) | copy-start | bytes 786436
  153.1 3.7 %copy-start.3 = (f32[1024,1024]{1,0:T(8,128)S(1)}, f32[1024,1024]{1,0:T(8,128)}, u32[]{:S(2)}) copy-start(f32[1024,1024]{1,0:T(8,128)} %fusion.15) | copy-start | bytes 12582916
  157.9 0.7 copy-start.16
  161.3 3.6 %copy-start = (bf16[1024,2048]{1,0:T(8,128)(2,1)S(1)}, bf16[1024,2048]{1,0:T(8,128)(2,1)}, u32[]{:S(2)}) copy-start(bf16[1024,2048]{1,0:T(8,128)(2,1)} %shard_map.70) | copy-start | bytes 12582916
  164.8 4.0 %collective-permute-start.16 = (bf16[512,768]{0,1:T(8,128)(2,1)S(1)}, bf16[512,768]{0,1:T(8,128)(2,1)S(1)}, u32[]{:S(2)}, u32[]{:S(2)}) collective-permute-start(bf16[512,768]{0,1:T(8,128)(2,1)S(1)} %slice.104), channel_id=1, source_target_pairs={{0,1},{1,0},{2,3},{3,2},{4,5},{5,4},{6,7},{7,6},{8,9},{9,8},{10,11... | collective-permute-start | bytes 2359304 | tf_op jit(solution)/shard_map/ppermute | solution.py:154
  168.2 6.1 %collective-permute-start.20 = (bf16[512,1280]{1,0:T(8,128)(2,1)S(1)}, bf16[512,1280]{1,0:T(8,128)(2,1)S(1)}, u32[]{:S(2)}, u32[]{:S(2)}) collective-permute-start(bf16[512,1280]{1,0:T(8,128)(2,1)S(1)} %slice.111), channel_id=1, source_target_pairs={{0,1},{1,0},{2,3},{3,2},{4,5},{5,4},{6,7},{7,6},{8,9},{9,8},{10,11... | collective-permute-start | bytes 3932168 | tf_op jit(solution)/shard_map/ppermute | solution.py:154
  171.1 12.9 %collective-permute-start.17 = (bf16[128,768]{0,1:T(8,128)(2,1)S(1)}, bf16[128,768]{0,1:T(8,128)(2,1)S(1)}, u32[]{:S(2)}, u32[]{:S(2)}) collective-permute-start(bf16[128,768]{0,1:T(8,128)(2,1)S(1)} %get-tuple-element.10), channel_id=1, source_target_pairs={{0,2},{1,3},{2,4},{3,5},{4,6},{5,7},{6,0},{7,1},{8,10},{9,11},{10,... | collective-permute-start | bytes 589832 | tf_op jit(solution)/shard_map/ppermute | solution.py:160
  171.7 15.0 %collective-permute-start.19 = (bf16[128,768]{0,1:T(8,128)(2,1)}, bf16[128,768]{0,1:T(8,128)(2,1)S(1)}, u32[]{:S(2)}, u32[]{:S(2)}) collective-permute-start(bf16[128,768]{0,1:T(8,128)(2,1)} %get-tuple-element.11), channel_id=1, source_target_pairs={{0,6},{1,7},{2,0},{3,1},{4,2},{5,3},{6,4},{7,5},{8,14},{9,15},{10,... | collective-permute-start | bytes 589832 | tf_op jit(solution)/shard_map/ppermute | solution.py:160
  174.3 12.4 %collective-permute-start.18 = (bf16[128,768]{0,1:T(8,128)(2,1)S(1)}, bf16[128,768]{0,1:T(8,128)(2,1)}, u32[]{:S(2)}, u32[]{:S(2)}) collective-permute-start(bf16[128,768]{0,1:T(8,128)(2,1)S(1)} %get-tuple-element.12), channel_id=1, source_target_pairs={{0,4},{1,5},{2,6},{3,7},{4,0},{5,1},{6,2},{7,3},{8,12},{9,13},{10,... | collective-permute-start | bytes 589832 | tf_op jit(solution)/shard_map/ppermute | solution.py:160
  175.7 21.8 %collective-permute-start.21 = (bf16[128,1280]{1,0:T(8,128)(2,1)}, bf16[128,1280]{1,0:T(8,128)(2,1)S(1)}, u32[]{:S(2)}, u32[]{:S(2)}) collective-permute-start(bf16[128,1280]{1,0:T(8,128)(2,1)} %get-tuple-element.7), channel_id=1, source_target_pairs={{0,2},{1,3},{2,4},{3,5},{4,6},{5,7},{6,0},{7,1},{8,10},{9,11},{10,... | collective-permute-start | bytes 983048 | tf_op jit(solution)/shard_map/ppermute | solution.py:160
  176.5 20.9 %collective-permute-start.23 = (bf16[128,1280]{1,0:T(8,128)(2,1)}, bf16[128,1280]{1,0:T(8,128)(2,1)}, u32[]{:S(2)}, u32[]{:S(2)}) collective-permute-start(bf16[128,1280]{1,0:T(8,128)(2,1)} %get-tuple-element.8), channel_id=1, source_target_pairs={{0,6},{1,7},{2,0},{3,1},{4,2},{5,3},{6,4},{7,5},{8,14},{9,15},{10,... | collective-permute-start | bytes 983048 | tf_op jit(solution)/shard_map/ppermute | solution.py:160
  184.0 13.4 %collective-permute-start.22 = (bf16[128,1280]{1,0:T(8,128)(2,1)}, bf16[128,1280]{1,0:T(8,128)(2,1)}, u32[]{:S(2)}, u32[]{:S(2)}) collective-permute-start(bf16[128,1280]{1,0:T(8,128)(2,1)} %get-tuple-element.9), channel_id=1, source_target_pairs={{0,4},{1,5},{2,6},{3,7},{4,0},{5,1},{6,2},{7,3},{8,12},{9,13},{10,... | collective-permute-start | bytes 983048 | tf_op jit(solution)/shard_map/ppermute | solution.py:160
where the time goes:
time: 201 us; the launch traced here: 200 us
  starting transfers between devices  52.2 us (26%)
  waiting for transfers between devices  47.5 us (24%)
  local copies, waits for them, and re-layouts  33.1 us (16%)
  matrix products  20.1 us (10%)
  other arithmetic  16.2 us (8%)
  blocking collectives  14.7 us (7%)
  Pallas kernels  14.6 us (7%)
    ppermute x7, starting transfers between devices, on_device(): held[step] = lax.ppermute(held[step - 1], 'fs', back)  38.9 us
    ppermute x7, waiting for transfers between devices, on_device(): held[-step] = lax.ppermute(held[1 - step], 'fs', fore)  30.2 us
    unnamed x53, local copies, waits for them, and re-layouts  24.8 us
    all_to_all x1, blocking collectives, on_device(): parts = lax.all_to_all(parts, 'tp', split_axis=0, concat_axis=0, tiled=True)  14.7 us
    pallas_call x4, Pallas kernels, place(): pl.pallas_call(body, out_shape=outs, in_specs=[pl.BlockSpec(memory_space=...  14.6 us
    ppermute x6, waiting for transfers between devices, on_device(): total = total + lax.ppermute(sent, 'tp', hop).astype(jnp.float32)  14.5 us
    dot_general x1, matrix products, on_device(): pre_act = jnp.dot(normed, up_sampler[0], preferred_element_type=jnp.float32)  9.91 us
    dot_general x2, matrix products, on_device(): jnp.dot(hidden, weights, preferred_element_type=jnp.float32)  6.56 us
  transfers between devices with their start and end apart: 24, of which 9 were waited for; matrix products, arithmetic and copies ran while one was open for 29% of the time, Pallas kernels for 6%

commit v1 on v0

--- a/solution.py
+++ b/solution.py
@@ -99,16 +99,19 @@
             for s in range(sides)
         ]
 
-    near = half - 3
-    early = [k for k in held if abs(k) <= near]
-    late = [k for k in held if abs(k) > near]
+    def within(least, most):
+        return [k for k in held if least <= abs(k) <= most]
+
+    late = [half - 2, half - 1, half, half + 1, half + 2]
     up_shape = [jax.ShapeDtypeStruct((n_fs * up_rows, width), jnp.bfloat16)]
     down_shape = [jax.ShapeDtypeStruct((n_fs * span, full), jnp.bfloat16)]
     blank = jnp.zeros((up_rows, width), jnp.bfloat16)
-    moves = up_moves(early)
-    moves += [(blank, 0, up_rows, 0, k, up_rows, 0, 0) for k in late + [half]]
+    moves = up_moves(within(0, half - 3))
+    moves += [(blank, 0, up_rows, 0, k, up_rows, 0, 0) for k in late]
     up_sampler = place(z, moves, up_shape, n_fs)
-    down_sampler = place(z, down_moves(early), down_shape, n_fs)
+    down_sampler = place(z, down_moves(within(0, half - 4)), down_shape, n_fs)
+    moves = down_moves(within(half - 3, half - 2))
+    down_sampler = place(z, moves, down_shape, n_fs, down_sampler)
 
     tokens = prompt_rows.shape[0]
     block = tokens // n_tp
@@ -120,32 +123,32 @@
         for dx, dc in order
     ]
     values = lax.optimization_barrier(jnp.concatenate(rows, axis=0)).astype(jnp.float32)
-    normed = (values * lax.rsqrt(jnp.mean(values * values, axis=-1, keepdims=True) + eps)).astype(
-        jnp.bfloat16
-    )
-    normed = lax.optimization_barrier(normed)
+    scale = lax.rsqrt(jnp.mean(values * values, axis=-1, keepdims=True) + eps)
+    normed = lax.optimization_barrier((values * scale).astype(jnp.bfloat16))
     pre_act = jnp.dot(normed, up_sampler[0], preferred_element_type=jnp.float32)
     pre_act = lax.optimization_barrier(pre_act)
 
-    rest = [held[k][:up_rows] for k in late] + [up_far]
+    rest = [up_far if k == half else held[k if k < half else k - n_fs][:up_rows] for k in late]
     rest = jnp.concatenate(rest, axis=0)
-    features = [
-        lax.dynamic_slice_in_dim(normed, (z + n_fs + k) % n_fs * up_rows, up_rows, axis=1)
-        for k in late + [half]
-    ]
-    features = lax.optimization_barrier(jnp.concatenate(features, axis=1))
+    ends = (len(late) - 1) * up_rows
+    features = jnp.concatenate([normed, normed[:, :ends]], axis=1)
+    features = lax.dynamic_slice_in_dim(
+        features, (z + late[0]) % n_fs * up_rows, len(late) * up_rows, axis=1
+    )
+    features = lax.optimization_barrier(features)
     pre_act = pre_act + jnp.dot(features, rest, preferred_element_type=jnp.float32)
     hidden = jnp.square(jax.nn.relu(pre_act)).astype(jnp.bfloat16)
 
-    moves = down_moves(late)
+    moves = down_moves(within(half - 1, half - 1))
     moves += [(down_far, k * span, span, 0, half, span, 0, k * width) for k in range(sides)]
     down_sampler = place(z, moves, down_shape, n_fs, down_sampler)[0]
-    moves = up_moves(late)
+    moves = up_moves(within(half - 2, half - 1))
     moves += [(up_far, 0, up_rows, 0, half, up_rows, 0, 0)]
     up_sampler = place(z, moves, up_shape, n_fs, up_sampler)[0]
 
     pair = [(k, k ^ 1) for k in range(n_tp)]
-    hops = [[(j, (j + 2 * dx) % n_tp) for j in range(n_tp)] for dx in range(1, n_x)]
+    right = [(j, (j + 2) % n_tp) for j in range(n_tp)]
+    left = [(j, (j - 2) % n_tp) for j in range(n_tp)]
     bounds = [0, 3 * full // 8, full]
     sums = []
     for lo, hi in zip(bounds[:-1], bounds[1:]):
@@ -153,11 +156,16 @@
         partial = jnp.dot(hidden, weights, preferred_element_type=jnp.float32).astype(jnp.bfloat16)
         theirs = lax.ppermute(partial[: tokens // 2], "tp", pair)
         chip = partial[tokens // 2 :].astype(jnp.float32) + theirs.astype(jnp.float32)
-        total = chip[(n_x - 1) * block :]
-        chip = chip[: (n_x - 1) * block].astype(jnp.bfloat16)
-        for k, hop in enumerate(hops):
-            sent = chip[k * block : (k + 1) * block]
-            total = total + lax.ppermute(sent, "tp", hop).astype(jnp.float32)
+        after, across, before, total = [chip[k * block : (k + 1) * block] for k in range(n_x)]
+        across = across.astype(jnp.bfloat16)
+        mid = (hi - lo) // 2
+        first = lax.ppermute(across[:, :mid], "tp", right).astype(jnp.float32)
+        second = lax.ppermute(across[:, mid:], "tp", left).astype(jnp.float32)
+        after = jnp.concatenate([after[:, :mid] + first, after[:, mid:]], axis=1)
+        before = jnp.concatenate([before[:, :mid], before[:, mid:] + second], axis=1)
+        after = lax.ppermute(after.astype(jnp.bfloat16), "tp", right).astype(jnp.float32)
+        before = lax.ppermute(before.astype(jnp.bfloat16), "tp", left).astype(jnp.float32)
+        total = total + after + before
         sums.append(total.astype(jnp.bfloat16))
     return (up_sampler[None], down_sampler[None], jnp.concatenate(sums, axis=1))
 

time: 201 us -> 198 us (0.985)
  waiting for transfers between devices: 47.5 us -> 36.1 us
  starting transfers between devices: 52.2 us -> 61.8 us
  local copies, waits for them, and re-layouts: 33.1 us -> 27.2 us
  matrix products: 20.1 us -> 23 us
    ppermute x7, waiting for transfers between devices: 30.2 us -> 2.44 us  [on_device(): held[-step] = lax.ppermute(held[1 - step], 'fs', fore)]
    ppermute x7, waiting for transfers between devices: 2.73 us -> 28.3 us  [on_device(): held[step] = lax.ppermute(held[step - 1], 'fs', back)]
    ppermute x6 -> x8, waiting for transfers between devices: 14.5 us -> 4.97 us  [the longest x2 2.73 us: on_device(): first = lax.ppermute(across[:, :mid], 'tp', right).astype(jnp.float32)]
    ppermute x6 -> x8, starting transfers between devices: 6.48 us -> 13.3 us  [the longest x2 5.9 us: on_device(): second = lax.ppermute(across[:, mid:], 'tp', left).astype(jnp.float32)]
    ppermute x7, starting transfers between devices: 38.9 us -> 44.3 us  [on_device(): held[step] = lax.ppermute(held[step - 1], 'fs', back)]
    concatenate x0 -> x5, other arithmetic: none -> 4.97 us  [the longest x1 2.83 us: on_device(): features = jnp.concatenate([normed, normed[:, :ends]], axis=1)]
    convert_element_type x2 -> x1, other arithmetic: 6.27 us -> 2.93 us  [on_device(): normed = lax.optimization_barrier((values * scale).astype(jnp.bfloat16))]
    unnamed x53 -> x49, local copies, waits for them, and re-layouts: 24.8 us -> 21.6 us
  transfers between devices with their start and end apart: 24 -> 26, of which waited for: 9 -> 10; matrix products, arithmetic and copies ran while one was open for 29% -> 27% of each run, Pallas kernels for 6% -> 7%
where the time goes in v1:
time: 198 us; the launch traced here: 197 us
  starting transfers between devices  61.8 us (31%)
  waiting for transfers between devices  36.1 us (18%)
  local copies, waits for them, and re-layouts  27.2 us (14%)
  matrix products  23 us (12%)
  other arithmetic  16.8 us (8%)
  Pallas kernels  16.2 us (8%)
  blocking collectives  14.7 us (7%)
    ppermute x7, starting transfers between devices, on_device(): held[step] = lax.ppermute(held[step - 1], 'fs', back)  44.3 us
    ppermute x7, waiting for transfers between devices, on_device(): held[step] = lax.ppermute(held[step - 1], 'fs', back)  28.3 us
    unnamed x49, local copies, waits for them, and re-layouts  21.6 us
    pallas_call x5, Pallas kernels, place(): pl.pallas_call(body, out_shape=outs, in_specs=[pl.BlockSpec(memory_space=...  16.2 us
    all_to_all x1, blocking collectives, on_device(): parts = lax.all_to_all(parts, 'tp', split_axis=0, concat_axis=0, tiled=True)  14.7 us
    dot_general x1, matrix products, on_device(): pre_act = jnp.dot(normed, up_sampler[0], preferred_element_type=jnp.float32)  10.1 us
    dot_general x2, matrix products, on_device(): jnp.dot(hidden, weights, preferred_element_type=jnp.float32)  7.16 us
    ppermute x2, starting transfers between devices, on_device(): second = lax.ppermute(across[:, mid:], 'tp', left).astype(jnp.float32)  5.9 us
  transfers between devices with their start and end apart: 26, of which 10 were waited for; matrix products, arithmetic and copies ran while one was open for 27% of the time, Pallas kernels for 7%

profile of v1, /device:TPU:40, one launch (start us, length us, event | category | flops | bytes accessed | tf_op | source)
XLA Modules:
  0.0 197.0 jit_solution(18216291233238253024)
XLA Ops:
  0.6 1.2 copy.35
  1.9 0.7 multiply_convert_fusion.1
  2.6 1.1 convert_element_type.70
  4.1 14.7 %all_to_all.5 = bf16[8,2,128,128]{2,3,1,0:T(8,128)(2,1)S(1)} all-to-all(bf16[8,2,128,128]{2,3,1,0:T(8,128)(2,1)S(1)} %copy.39), channel_id=1, replica_groups=mesh['grp'=2,'fs'=16,'tp'=8] {'tp'}, dimensions={0} | all-to-all | bytes 1048576 | tf_op jit(solution)/shard_map/all_to_all | solution.py:76
  19.7 22.5 %collective-permute-start.6 = (bf16[256,1024]{1,0:T(8,128)(2,1)S(1)}, bf16[256,1024]{1,0:T(8,128)(2,1)S(1)}, u32[]{:S(2)}, u32[]{:S(2)}) collective-permute-start(bf16[256,1024]{1,0:T(8,128)(2,1)S(1)} %pad_maximum_fusion.1.refs_0_), channel_id=1, source_target_pairs={{0,120},{8,0},{16,8},{24,16},{32,24},{40,32},{48,40},{56,48},{64,5... | collective-permute-start | bytes 1572872 | tf_op jit(solution)/shard_map/ppermute | solution.py:88
  42.2 10.8 %collective-permute-done.6.refs_2_ = bf16[256,1024]{1,0:T(8,128)(2,1)S(1)} collective-permute-done((bf16[256,1024]{1,0:T(8,128)(2,1)S(1)}, bf16[256,1024]{1,0:T(8,128)(2,1)S(1)}, u32[]{:S(2)}, u32[]{:S(2)}) %collective-permute-start.6) | collective-permute-done | bytes 524320 | tf_op jit(solution)/shard_map/ppermute | solution.py:88
  53.0 3.7 %collective-permute-start.7 = (bf16[256,1024]{1,0:T(8,128)(2,1)S(1)}, bf16[256,1024]{1,0:T(8,128)(2,1)S(1)}, u32[]{:S(2)}, u32[]{:S(2)}) collective-permute-start(bf16[256,1024]{1,0:T(8,128)(2,1)S(1)} %collective-permute-done.6.refs_2_), channel_id=1, source_target_pairs={{0,120},{8,0},{16,8},{24,16},{32,24},{40,32},{48,40},{56,48},{64,5... | collective-permute-start | bytes 1572872 | tf_op jit(solution)/shard_map/ppermute | solution.py:88
  56.8 2.0 %dynamic-slice_dynamic-update-slice_fusion.7 = bf16[1024,2048]{1,0:T(8,128)(2,1)} fusion(bf16[1024,2048]{1,0:T(8,128)(2,1)} %param.4, s32[]{:T(128)S(6)} %select_n.90), kind=kLoop, calls=%fused_computation.27 | loop fusion | bytes 1048580
  58.8 1.9 dynamic-slice_dynamic-update-slice_fusion.6
  60.7 6.0 %collective-permute-done.7.refs_4_ = bf16[256,1024]{1,0:T(8,128)(2,1)S(1)} collective-permute-done((bf16[256,1024]{1,0:T(8,128)(2,1)S(1)}, bf16[256,1024]{1,0:T(8,128)(2,1)S(1)}, u32[]{:S(2)}, u32[]{:S(2)}) %collective-permute-start.7) | collective-permute-done | bytes 524320 | tf_op jit(solution)/shard_map/ppermute | solution.py:88
  66.7 3.7 %collective-permute-start.8 = (bf16[256,1024]{1,0:T(8,128)(2,1)S(1)}, bf16[256,1024]{1,0:T(8,128)(2,1)S(1)}, u32[]{:S(2)}, u32[]{:S(2)}) collective-permute-start(bf16[256,1024]{1,0:T(8,128)(2,1)S(1)} %collective-permute-done.7.refs_4_), channel_id=1, source_target_pairs={{0,120},{8,0},{16,8},{24,16},{32,24},{40,32},{48,40},{56,48},{64,5... | collective-permute-start | bytes 1572872 | tf_op jit(solution)/shard_map/ppermute | solution.py:88
  70.4 2.1 %dynamic-slice_dynamic-update-slice_fusion.5 = bf16[1024,2048]{1,0:T(8,128)(2,1)} fusion(bf16[1024,2048]{1,0:T(8,128)(2,1)} %dynamic-slice_dynamic-update-slice_fusion.6, bf16[1024,2048]{1,0:T(8,128)(2,1)} %param.4, s32[]{:T(128)S(6)} %select_n.94), kind=kLoop, calls=%fused_computation.25 | loop fusion | bytes 1048580
  72.4 1.9 dynamic-slice_dynamic-update-slice_fusion.4
  74.3 1.9 dynamic-slice_dynamic-update-slice_fusion.3
  76.2 3.3 %collective-permute-done.8.refs_6_ = bf16[256,1024]{1,0:T(8,128)(2,1)S(1)} collective-permute-done((bf16[256,1024]{1,0:T(8,128)(2,1)S(1)}, bf16[256,1024]{1,0:T(8,128)(2,1)S(1)}, u32[]{:S(2)}, u32[]{:S(2)}) %collective-permute-start.8) | collective-permute-done | bytes 524320 | tf_op jit(solution)/shard_map/ppermute | solution.py:88
  79.5 3.7 %collective-permute-start.9 = (bf16[256,1024]{1,0:T(8,128)(2,1)S(1)}, bf16[256,1024]{1,0:T(8,128)(2,1)}, u32[]{:S(2)}, u32[]{:S(2)}) collective-permute-start(bf16[256,1024]{1,0:T(8,128)(2,1)S(1)} %collective-permute-done.8.refs_6_), channel_id=1, source_target_pairs={{0,120},{8,0},{16,8},{24,16},{32,24},{40,32},{48,40},{56,48},{64,5... | collective-permute-start | bytes 1572872 | tf_op jit(solution)/shard_map/ppermute | solution.py:88
  83.2 1.9 dynamic-slice_dynamic-update-slice_fusion.2
  85.0 1.9 dynamic-slice_dynamic-update-slice_fusion.1
  86.9 1.9 dynamic-slice_dynamic-update-slice_fusion
  88.8 2.6 %collective-permute-done.9.refs_8_ = bf16[256,1024]{1,0:T(8,128)(2,1)} collective-permute-done((bf16[256,1024]{1,0:T(8,128)(2,1)S(1)}, bf16[256,1024]{1,0:T(8,128)(2,1)}, u32[]{:S(2)}, u32[]{:S(2)}) %collective-permute-start.9) | collective-permute-done | bytes 524320 | tf_op jit(solution)/shard_map/ppermute | solution.py:88
  91.4 3.8 %collective-permute-start.10 = (bf16[256,1024]{1,0:T(8,128)(2,1)}, bf16[256,1024]{1,0:T(8,128)(2,1)S(1)}, u32[]{:S(2)}, u32[]{:S(2)}) collective-permute-start(bf16[256,1024]{1,0:T(8,128)(2,1)} %collective-permute-done.9.refs_8_), channel_id=1, source_target_pairs={{0,120},{8,0},{16,8},{24,16},{32,24},{40,32},{48,40},{56,48},{64,5... | collective-permute-start | bytes 1572872 | tf_op jit(solution)/shard_map/ppermute | solution.py:88
  95.2 3.1 %fusion = f32[1024]{0:T(1024)S(1)} fusion(bf16[1024,2048]{1,0:T(8,128)(2,1)} %dynamic-slice_dynamic-update-slice_fusion), kind=kLoop, calls=%fused_computation.2 | loop fusion | flops 6290432 | bytes 4198400 | tf_op jit(solution)/shard_map/reduce_sum | solution.py:126
  98.3 5.6 %collective-permute-done.10.refs_10_.refs_1_ = bf16[256,1024]{1,0:T(8,128)(2,1)S(1)} collective-permute-done((bf16[256,1024]{1,0:T(8,128)(2,1)}, bf16[256,1024]{1,0:T(8,128)(2,1)S(1)}, u32[]{:S(2)}, u32[]{:S(2)}) %collective-permute-start.10) | collective-permute-done | bytes 524320 | tf_op jit(solution)/shard_map/ppermute | solution.py:88
  103.9 3.6 %collective-permute-start.11 = (bf16[256,1024]{1,0:T(8,128)(2,1)S(1)}, bf16[256,1024]{1,0:T(8,128)(2,1)S(1)}, u32[]{:S(2)}, u32[]{:S(2)}) collective-permute-start(bf16[256,1024]{1,0:T(8,128)(2,1)S(1)} %collective-permute-done.10.refs_10_.refs_1_), channel_id=1, source_target_pairs={{0,120},{8,0},{16,8},{24,16},{32,24},{40,32},{48,40},{56,48},{64,5... | collective-permute-start | bytes 1572872 | tf_op jit(solution)/shard_map/ppermute | solution.py:88
  107.5 2.9 %fusion.1 = bf16[1024,2048]{1,0:T(8,128)(2,1)S(1)} fusion(bf16[1024,2048]{1,0:T(8,128)(2,1)} %dynamic-slice_dynamic-update-slice_fusion, f32[1024]{0:T(1024)S(1)} %add_rsqrt_fusion), kind=kLoop, calls=%fused_computation.3 | loop fusion | flops 6291456 | bytes 8392704 | tf_op jit(solution)/shard_map/convert_element_type | solution.py:127
  110.5 2.0 %copy-done.1 = bf16[1024,2048]{1,0:T(8,128)(2,1)} copy-done((bf16[1024,2048]{1,0:T(8,128)(2,1)}, bf16[1024,2048]{1,0:T(8,128)(2,1)S(1)}, u32[]{:S(2)}) %copy-start.1) | copy-done | bytes 4194328
  112.6 2.8 %fusion.4 = bf16[1024,640]{1,0:T(8,128)(2,1)} fusion(s32[]{:T(128)S(6)} %select_n.103, bf16[1024,2048]{1,0:T(8,128)(2,1)} %copy-done.1, bf16[1024,512]{1,0:T(8,128)(2,1)S(1)} %slice.141), kind=kLoop, calls=%fused_computation.13 | loop fusion | flops 2621440 | bytes 6553604 | tf_op jit(solution)/shard_map/concatenate | solution.py:134
  115.4 3.8 %shard_map.69.refs_4_ = bf16[1024,2048]{1,0:T(8,128)(2,1)} custom-call(s32[1]{0:T(128)} %bitcast.z_ref, bf16[256,1024]{1,0:T(8,128)(2,1)} %copy-done.2, bf16[256,1024]{1,0:T(8,128)(2,1)} %copy-done.10, bf16[256,1024]{1,0:T(8,128)(2,1)} %copy-done.9, bf16[256,1024]{1,0:T(8,128)(2,1)} %copy-done.12, bf16[256,1024]{1,0:T(8,128)(2,1)} %copy-done.11, ...), custom_call_target="tpu_custom_call" | custom-call | tf_op jit(solution)/shard_map/pallas_call | solution.py:38
  119.3 0.7 broadcast_in_dim.11.refs_11_
  120.0 4.8 %shard_map.67.refs_5_ = bf16[2048,1024]{1,0:T(8,128)(2,1)} custom-call(s32[1]{0:T(128)} %bitcast.z_ref, bf16[256,1024]{1,0:T(8,128)(2,1)} %copy-done.2, bf16[256,1024]{1,0:T(8,128)(2,1)} %copy-done.10, bf16[256,1024]{1,0:T(8,128)(2,1)} %copy-done.9, bf16[256,1024]{1,0:T(8,128)(2,1)} %copy-done.12, bf16[256,1024]{1,0:T(8,128)(2,1)} %copy-done.11, ...), custom_call_target="tpu_custom_call" | custom-call | tf_op jit(solution)/shard_map/pallas_call | solution.py:38
  124.9 3.3 %collective-permute-start.13 = (bf16[256,1024]{1,0:T(8,128)(2,1)S(1)}, bf16[256,1024]{1,0:T(8,128)(2,1)S(1)}, u32[]{:S(2)}, u32[]{:S(2)}) collective-permute-start(bf16[256,1024]{1,0:T(8,128)(2,1)S(1)} %collective-permute-done.11.refs_1_.refs_3_), channel_id=1, source_target_pairs={{0,120},{8,0},{16,8},{24,16},{32,24},{40,32},{48,40},{56,48},{64,5... | collective-permute-start | bytes 1572872 | tf_op jit(solution)/shard_map/ppermute | solution.py:88
  128.2 10.1 %fusion.18 = f32[1024,1024]{1,0:T(8,128)} fusion(bf16[1024,2048]{1,0:T(8,128)(2,1)} %copy-done.1, bf16[2048,1024]{1,0:T(8,128)(2,1)} %shard_map.67.refs_5_), kind=kOutput, calls=%fused_computation.55 | convolution fusion | flops 4294967296 | bytes 12582912 | tf_op jit(solution)/shard_map/dot_general | solution.py:128
  138.3 2.4 %collective-permute-done.12.refs_2_.refs_0_ = bf16[256,1024]{1,0:T(8,128)(2,1)S(1)} collective-permute-done((bf16[256,1024]{1,0:T(8,128)(2,1)S(1)}, bf16[256,1024]{1,0:T(8,128)(2,1)S(1)}, u32[]{:S(2)}, u32[]{:S(2)}) %collective-permute-start.12) | collective-permute-done | bytes 524320 | tf_op jit(solution)/shard_map/ppermute | solution.py:87
  140.7 0.8 slice.139
  141.5 0.7 slice_dynamic-update-slice_fusion.2
  142.3 2.7 %shard_map.70.refs_3_ = bf16[1024,2048]{1,0:T(8,128)(2,1)} custom-call(s32[1]{0:T(128)} %bitcast.z_ref, bf16[256,1024]{1,0:T(8,128)(2,1)} %collective-permute-done.4.refs_9_.refs_0_, bf16[256,1024]{1,0:T(8,128)(2,1)} %copy-done.14, bf16[256,1024]{1,0:T(8,128)(2,1)} %copy-done.7, bf16[256,1024]{1,0:T(8,128)(2,1)} %copy-done.6, ...), custom_call_target="tpu_custom_call", output_to_operand_aliasing={{}: (5, {})} | custom-call | tf_op jit(solution)/shard_map/pallas_call | solution.py:38
  145.0 0.8 slice_dynamic-update-slice_fusion.1
  145.8 3.2 %collective-permute-start.15 = (bf16[128,1024]{1,0:T(8,128)(2,1)S(1)}, bf16[128,1024]{1,0:T(8,128)(2,1)S(1)}, u32[]{:S(2)}, u32[]{:S(2)}) collective-permute-start(bf16[128,1024]{1,0:T(8,128)(2,1)S(1)} %get-tuple-element.20), channel_id=1, source_target_pairs={{0,120},{8,0},{16,8},{24,16},{32,24},{40,32},{48,40},{56,48},{64,5... | collective-permute-start | bytes 786440 | tf_op jit(solution)/shard_map/ppermute | solution.py:90
  149.1 0.4 collective-permute-done.14.refs_4_
  149.4 1.7 constant_dynamic-update-slice_fusion.1
  151.1 0.7 constant_dynamic-update-slice_fusion
  151.8 0.7 slice_dynamic-update-slice_fusion
  152.6 5.7 %multiply_convert_fusion = bf16[1024,1024]{1,0:T(8,128)(2,1)} fusion(f32[1024,1024]{1,0:T(8,128)} %fusion.18, bf16[1024,640]{1,0:T(8,128)(2,1)S(1)} %copy-done.15, bf16[640,1024]{1,0:T(8,128)(2,1)} %slice_dynamic-update-slice_fusion), kind=kOutput, calls=%fused_computation.6 | convolution fusion | flops 1346371584 | bytes 8912896 | tf_op jit(solution)/shard_map/dot_general | solution.py:139
  158.3 0.7 copy-done.16
  159.0 2.2 %shard_map.71 = bf16[1024,2048]{1,0:T(8,128)(2,1)} custom-call(s32[1]{0:T(128)} %bitcast.z_ref, bf16[256,1024]{1,0:T(8,128)(2,1)} %copy-done.3, bf16[256,1024]{1,0:T(8,128)(2,1)} %copy-done.4, bf16[128,1024]{1,0:T(8,128)(2,1)} %copy-done.16, bf16[1024,2048]{1,0:T(8,128)(2,1)} %shard_map.70.refs_3_), custom_call_target="tpu_custom_call", output_to_operand_aliasing={{}: (4, {})} | custom-call | tf_op jit(solution)/shard_map/pallas_call | solution.py:38
  161.2 4.0 %convolution_convert_fusion.1 = bf16[1024,768]{0,1:T(8,128)(2,1)S(1)} fusion(bf16[1024,1024]{1,0:T(8,128)(2,1)} %multiply_convert_fusion, bf16[1024,2048]{1,0:T(8,128)(2,1)} %shard_map.71), kind=kOutput, calls=%fused_computation.10 | convolution fusion | flops 1611399168 | bytes 5242880 | tf_op jit(solution)/shard_map/dot_general | solution.py:156
  165.3 0.4 collective-permute-start.16
  165.7 3.1 %convolution_convert_fusion = bf16[1024,1280]{1,0:T(8,128)(2,1)S(1)} fusion(bf16[1024,1024]{1,0:T(8,128)(2,1)S(1)} %copy-done.17, bf16[1024,2048]{1,0:T(8,128)(2,1)S(1)} %copy-done), kind=kOutput, calls=%fused_computation.7 | convolution fusion | flops 2685665280 | bytes 7340032 | tf_op jit(solution)/shard_map/dot_general | solution.py:156
  169.0 0.6 collective-permute-start.21
  170.0 0.7 collective-permute-start.17
  170.6 2.7 %collective-permute-start.19 = (bf16[128,384]{0,1:T(8,128)(2,1)S(1)}, bf16[128,384]{0,1:T(8,128)(2,1)S(1)}, u32[]{:S(2)}, u32[]{:S(2)}) collective-permute-start(bf16[128,384]{0,1:T(8,128)(2,1)S(1)} %get-tuple-element.16), channel_id=1, source_target_pairs={{0,6},{1,7},{2,0},{3,1},{4,2},{5,3},{6,4},{7,5},{8,14},{9,15},{10,... | collective-permute-start | bytes 294920 | tf_op jit(solution)/shard_map/ppermute | solution.py:163
  173.3 2.7 %collective-permute-done.17 = bf16[128,384]{0,1:T(8,128)(2,1)S(1)} collective-permute-done((bf16[128,384]{0,1:T(8,128)(2,1)S(1)}, bf16[128,384]{0,1:T(8,128)(2,1)S(1)}, u32[]{:S(2)}, u32[]{:S(2)}) %collective-permute-start.17) | collective-permute-done | bytes 98336 | tf_op jit(solution)/shard_map/ppermute | solution.py:162
  176.6 3.2 %collective-permute-start.24 = (bf16[128,640]{1,0:T(8,128)(2,1)S(1)}, bf16[128,640]{1,0:T(8,128)(2,1)S(1)}, u32[]{:S(2)}, u32[]{:S(2)}) collective-permute-start(bf16[128,640]{1,0:T(8,128)(2,1)S(1)} %get-tuple-element.12), channel_id=1, source_target_pairs={{0,6},{1,7},{2,0},{3,1},{4,2},{5,3},{6,4},{7,5},{8,14},{9,15},{10,... | collective-permute-start | bytes 491528 | tf_op jit(solution)/shard_map/ppermute | solution.py:163
  179.9 0.7 pad_maximum_fusion.5
  180.5 0.7 pad_maximum_fusion.6
  181.2 3.2 %collective-permute-start.20 = (bf16[128,768]{0,1:T(8,128)(2,1)}, bf16[128,768]{0,1:T(8,128)(2,1)}, u32[]{:S(2)}, u32[]{:S(2)}) collective-permute-start(bf16[128,768]{0,1:T(8,128)(2,1)} %pad_maximum_fusion.6), channel_id=1, source_target_pairs={{0,6},{1,7},{2,0},{3,1},{4,2},{5,3},{6,4},{7,5},{8,14},{9,15},{10,... | collective-permute-start | bytes 589832 | tf_op jit(solution)/shard_map/ppermute | solution.py:167
  184.6 1.1 collective-permute-start.23
  185.7 0.8 pad_maximum_fusion.4
  186.5 2.2 %collective-permute-start.25 = (bf16[128,1280]{1,0:T(8,128)(2,1)}, bf16[128,1280]{1,0:T(8,128)(2,1)}, u32[]{:S(2)}, u32[]{:S(2)}) collective-permute-start(bf16[128,1280]{1,0:T(8,128)(2,1)} %pad_maximum_fusion.4), channel_id=1, source_target_pairs={{0,6},{1,7},{2,0},{3,1},{4,2},{5,3},{6,4},{7,5},{8,14},{9,15},{10,... | collective-permute-start | bytes 983048 | tf_op jit(solution)/shard_map/ppermute | solution.py:167
  188.7 2.7 %shard_map.68 = bf16[2048,1024]{1,0:T(8,128)(2,1)} custom-call(s32[1]{0:T(128)} %bitcast.z_ref, bf16[256,1024]{1,0:T(8,128)(2,1)} %copy-done.7, bf16[256,1024]{1,0:T(8,128)(2,1)} %copy-done.6, bf16[256,1024]{1,0:T(8,128)(2,1)} %copy-done.3, bf16[256,1024]{1,0:T(8,128)(2,1)} %copy-done.4, ...), custom_call_target="tpu_custom_call", output_to_operand_aliasing={{}: (6, {})} | custom-call | tf_op jit(solution)/shard_map/pallas_call | solution.py:38
  191.4 1.2 fusion.8
  192.8 2.0 %collective-permute-done.23 = bf16[128,1280]{1,0:T(8,128)(2,1)} collective-permute-done((bf16[128,1280]{1,0:T(8,128)(2,1)S(1)}, bf16[128,1280]{1,0:T(8,128)(2,1)}, u32[]{:S(2)}, u32[]{:S(2)}) %collective-permute-start.23) | collective-permute-done | bytes 327712 | tf_op jit(solution)/shard_map/ppermute | solution.py:166
  195.0 1.2 fusion.6
  196.2 0.8 pad_maximum_fusion.2
  (85 shorter events, 3.1 us)
Async XLA Ops:
  19.7 69.1 %copy-start.2 = (bf16[256,1024]{1,0:T(8,128)(2,1)}, bf16[256,1024]{1,0:T(8,128)(2,1)S(1)}, u32[]{:S(2)}) copy-start(bf16[256,1024]{1,0:T(8,128)(2,1)S(1)} %pad_maximum_fusion.1.refs_0_) | copy-start | bytes 1572868
  19.7 33.3 %collective-permute-start.6 = (bf16[256,1024]{1,0:T(8,128)(2,1)S(1)}, bf16[256,1024]{1,0:T(8,128)(2,1)S(1)}, u32[]{:S(2)}, u32[]{:S(2)}) collective-permute-start(bf16[256,1024]{1,0:T(8,128)(2,1)S(1)} %pad_maximum_fusion.1.refs_0_), channel_id=1, source_target_pairs={{0,120},{8,0},{16,8},{24,16},{32,24},{40,32},{48,40},{56,48},{64,5... | collective-permute-start | bytes 1572872 | tf_op jit(solution)/shard_map/ppermute | solution.py:88
  42.2 14.5 %collective-permute-start = (bf16[256,1024]{1,0:T(8,128)(2,1)S(1)}, bf16[256,1024]{1,0:T(8,128)(2,1)S(1)}, u32[]{:S(2)}, u32[]{:S(2)}) collective-permute-start(bf16[256,1024]{1,0:T(8,128)(2,1)S(1)} %pad_maximum_fusion.1.refs_0_), channel_id=1, source_target_pairs={{0,8},{8,16},{16,24},{24,32},{32,40},{40,48},{48,56},{56,64},{64,7... | collective-permute-start | bytes 1572872 | tf_op jit(solution)/shard_map/ppermute | solution.py:87
  53.0 35.8 %copy-start.9 = (bf16[256,1024]{1,0:T(8,128)(2,1)}, bf16[256,1024]{1,0:T(8,128)(2,1)S(1)}, u32[]{:S(2)}) copy-start(bf16[256,1024]{1,0:T(8,128)(2,1)S(1)} %collective-permute-done.6.refs_2_) | copy-start | bytes 1572868
  53.0 13.7 %collective-permute-start.7 = (bf16[256,1024]{1,0:T(8,128)(2,1)S(1)}, bf16[256,1024]{1,0:T(8,128)(2,1)S(1)}, u32[]{:S(2)}, u32[]{:S(2)}) collective-permute-start(bf16[256,1024]{1,0:T(8,128)(2,1)S(1)} %collective-permute-done.6.refs_2_), channel_id=1, source_target_pairs={{0,120},{8,0},{16,8},{24,16},{32,24},{40,32},{48,40},{56,48},{64,5... | collective-permute-start | bytes 1572872 | tf_op jit(solution)/shard_map/ppermute | solution.py:88
  56.7 32.1 %copy-start.10 = (bf16[256,1024]{1,0:T(8,128)(2,1)}, bf16[256,1024]{1,0:T(8,128)(2,1)S(1)}, u32[]{:S(2)}) copy-start(bf16[256,1024]{1,0:T(8,128)(2,1)S(1)} %collective-permute-done.refs_1_) | copy-start | bytes 1572868
  56.7 13.7 %collective-permute-start.1 = (bf16[256,1024]{1,0:T(8,128)(2,1)S(1)}, bf16[256,1024]{1,0:T(8,128)(2,1)S(1)}, u32[]{:S(2)}, u32[]{:S(2)}) collective-permute-start(bf16[256,1024]{1,0:T(8,128)(2,1)S(1)} %collective-permute-done.refs_1_), channel_id=1, source_target_pairs={{0,8},{8,16},{16,24},{24,32},{32,40},{40,48},{48,56},{56,64},{64,7... | collective-permute-start | bytes 1572872 | tf_op jit(solution)/shard_map/ppermute | solution.py:87
  66.7 31.6 %copy-start.11 = (bf16[256,1024]{1,0:T(8,128)(2,1)}, bf16[256,1024]{1,0:T(8,128)(2,1)S(1)}, u32[]{:S(2)}) copy-start(bf16[256,1024]{1,0:T(8,128)(2,1)S(1)} %collective-permute-done.7.refs_4_) | copy-start | bytes 1572868
  66.7 12.8 %collective-permute-start.8 = (bf16[256,1024]{1,0:T(8,128)(2,1)S(1)}, bf16[256,1024]{1,0:T(8,128)(2,1)S(1)}, u32[]{:S(2)}, u32[]{:S(2)}) collective-permute-start(bf16[256,1024]{1,0:T(8,128)(2,1)S(1)} %collective-permute-done.7.refs_4_), channel_id=1, source_target_pairs={{0,120},{8,0},{16,8},{24,16},{32,24},{40,32},{48,40},{56,48},{64,5... | collective-permute-start | bytes 1572872 | tf_op jit(solution)/shard_map/ppermute | solution.py:88
  70.4 27.9 %copy-start.12 = (bf16[256,1024]{1,0:T(8,128)(2,1)}, bf16[256,1024]{1,0:T(8,128)(2,1)S(1)}, u32[]{:S(2)}) copy-start(bf16[256,1024]{1,0:T(8,128)(2,1)S(1)} %collective-permute-done.1.refs_3_) | copy-start | bytes 1572868
  70.4 12.8 %collective-permute-start.2 = (bf16[256,1024]{1,0:T(8,128)(2,1)S(1)}, bf16[256,1024]{1,0:T(8,128)(2,1)}, u32[]{:S(2)}, u32[]{:S(2)}) collective-permute-start(bf16[256,1024]{1,0:T(8,128)(2,1)S(1)} %collective-permute-done.1.refs_3_), channel_id=1, source_target_pairs={{0,8},{8,16},{16,24},{24,32},{32,40},{40,48},{48,56},{56,64},{64,7... | collective-permute-start | bytes 1572872 | tf_op jit(solution)/shard_map/ppermute | solution.py:87
  79.5 28.0 %copy-start.13 = (bf16[256,1024]{1,0:T(8,128)(2,1)}, bf16[256,1024]{1,0:T(8,128)(2,1)S(1)}, u32[]{:S(2)}) copy-start(bf16[256,1024]{1,0:T(8,128)(2,1)S(1)} %collective-permute-done.8.refs_6_) | copy-start | bytes 1572868
  79.5 11.9 %collective-permute-start.9 = (bf16[256,1024]{1,0:T(8,128)(2,1)S(1)}, bf16[256,1024]{1,0:T(8,128)(2,1)}, u32[]{:S(2)}, u32[]{:S(2)}) collective-permute-start(bf16[256,1024]{1,0:T(8,128)(2,1)S(1)} %collective-permute-done.8.refs_6_), channel_id=1, source_target_pairs={{0,120},{8,0},{16,8},{24,16},{32,24},{40,32},{48,40},{56,48},{64,5... | collective-permute-start | bytes 1572872 | tf_op jit(solution)/shard_map/ppermute | solution.py:88
  83.2 12.0 %collective-permute-start.3 = (bf16[256,1024]{1,0:T(8,128)(2,1)}, bf16[256,1024]{1,0:T(8,128)(2,1)}, u32[]{:S(2)}, u32[]{:S(2)}) collective-permute-start(bf16[256,1024]{1,0:T(8,128)(2,1)} %collective-permute-done.2.refs_5_), channel_id=1, source_target_pairs={{0,8},{8,16},{16,24},{24,32},{32,40},{40,48},{48,56},{56,64},{64,7... | collective-permute-start | bytes 1572872 | tf_op jit(solution)/shard_map/ppermute | solution.py:87
  91.4 12.5 %collective-permute-start.10 = (bf16[256,1024]{1,0:T(8,128)(2,1)}, bf16[256,1024]{1,0:T(8,128)(2,1)S(1)}, u32[]{:S(2)}, u32[]{:S(2)}) collective-permute-start(bf16[256,1024]{1,0:T(8,128)(2,1)} %collective-permute-done.9.refs_8_), channel_id=1, source_target_pairs={{0,120},{8,0},{16,8},{24,16},{32,24},{40,32},{48,40},{56,48},{64,5... | collective-permute-start | bytes 1572872 | tf_op jit(solution)/shard_map/ppermute | solution.py:88
  95.2 12.3 %collective-permute-start.4 = (bf16[256,1024]{1,0:T(8,128)(2,1)}, bf16[256,1024]{1,0:T(8,128)(2,1)}, u32[]{:S(2)}, u32[]{:S(2)}) collective-permute-start(bf16[256,1024]{1,0:T(8,128)(2,1)} %collective-permute-done.3.refs_7_), channel_id=1, source_target_pairs={{0,8},{8,16},{16,24},{24,32},{32,40},{40,48},{48,56},{56,64},{64,7... | collective-permute-start | bytes 1572872 | tf_op jit(solution)/shard_map/ppermute | solution.py:87
  103.9 6.5 %copy-start.14 = (bf16[256,1024]{1,0:T(8,128)(2,1)}, bf16[256,1024]{1,0:T(8,128)(2,1)S(1)}, u32[]{:S(2)}) copy-start(bf16[256,1024]{1,0:T(8,128)(2,1)S(1)} %collective-permute-done.10.refs_10_.refs_1_) | copy-start | bytes 1572868
  103.9 20.9 %collective-permute-start.11 = (bf16[256,1024]{1,0:T(8,128)(2,1)S(1)}, bf16[256,1024]{1,0:T(8,128)(2,1)S(1)}, u32[]{:S(2)}, u32[]{:S(2)}) collective-permute-start(bf16[256,1024]{1,0:T(8,128)(2,1)S(1)} %collective-permute-done.10.refs_10_.refs_1_), channel_id=1, source_target_pairs={{0,120},{8,0},{16,8},{24,16},{32,24},{40,32},{48,40},{56,48},{64,5... | collective-permute-start | bytes 1572872 | tf_op jit(solution)/shard_map/ppermute | solution.py:88
  107.5 20.7 %collective-permute-start.5 = (bf16[256,1024]{1,0:T(8,128)(2,1)}, bf16[256,1024]{1,0:T(8,128)(2,1)S(1)}, u32[]{:S(2)}, u32[]{:S(2)}) collective-permute-start(bf16[256,1024]{1,0:T(8,128)(2,1)} %collective-permute-done.4.refs_9_.refs_0_), channel_id=1, source_target_pairs={{0,8},{8,16},{16,24},{24,32},{32,40},{40,48},{48,56},{56,64},{64,7... | collective-permute-start | bytes 1572872 | tf_op jit(solution)/shard_map/ppermute | solution.py:87
  110.5 2.0 %copy-start.1 = (bf16[1024,2048]{1,0:T(8,128)(2,1)}, bf16[1024,2048]{1,0:T(8,128)(2,1)S(1)}, u32[]{:S(2)}) copy-start(bf16[1024,2048]{1,0:T(8,128)(2,1)S(1)} %fusion.1) | copy-start | bytes 12582916
  124.9 16.7 %copy-start.6 = (bf16[256,1024]{1,0:T(8,128)(2,1)}, bf16[256,1024]{1,0:T(8,128)(2,1)S(1)}, u32[]{:S(2)}) copy-start(bf16[256,1024]{1,0:T(8,128)(2,1)S(1)} %collective-permute-done.11.refs_1_.refs_3_) | copy-start | bytes 1572868
  124.9 20.1 %collective-permute-start.13 = (bf16[256,1024]{1,0:T(8,128)(2,1)S(1)}, bf16[256,1024]{1,0:T(8,128)(2,1)S(1)}, u32[]{:S(2)}, u32[]{:S(2)}) collective-permute-start(bf16[256,1024]{1,0:T(8,128)(2,1)S(1)} %collective-permute-done.11.refs_1_.refs_3_), channel_id=1, source_target_pairs={{0,120},{8,0},{16,8},{24,16},{32,24},{40,32},{48,40},{56,48},{64,5... | collective-permute-start | bytes 1572872 | tf_op jit(solution)/shard_map/ppermute | solution.py:88
  128.2 10.1 %copy-start.7 = (bf16[256,1024]{1,0:T(8,128)(2,1)}, bf16[256,1024]{1,0:T(8,128)(2,1)S(1)}, u32[]{:S(2)}) copy-start(bf16[256,1024]{1,0:T(8,128)(2,1)S(1)} %collective-permute-done.5.refs_0_.refs_2_) | copy-start | bytes 1572868
  128.2 12.5 %collective-permute-start.12 = (bf16[256,1024]{1,0:T(8,128)(2,1)S(1)}, bf16[256,1024]{1,0:T(8,128)(2,1)S(1)}, u32[]{:S(2)}, u32[]{:S(2)}) collective-permute-start(bf16[256,1024]{1,0:T(8,128)(2,1)S(1)} %collective-permute-done.5.refs_0_.refs_2_), channel_id=1, source_target_pairs={{0,8},{8,16},{16,24},{24,32},{32,40},{40,48},{48,56},{56,64},{64,7... | collective-permute-start | bytes 1572872 | tf_op jit(solution)/shard_map/ppermute | solution.py:87
  140.7 10.4 %copy-start.3 = (bf16[256,1024]{1,0:T(8,128)(2,1)}, bf16[256,1024]{1,0:T(8,128)(2,1)S(1)}, u32[]{:S(2)}) copy-start(bf16[256,1024]{1,0:T(8,128)(2,1)S(1)} %collective-permute-done.12.refs_2_.refs_0_) | copy-start | bytes 1572868
  141.5 7.9 %collective-permute-start.14 = (bf16[128,1024]{1,0:T(8,128)(2,1)}, bf16[128,1024]{1,0:T(8,128)(2,1)}, u32[]{:S(2)}, u32[]{:S(2)}) collective-permute-start(bf16[128,1024]{1,0:T(8,128)(2,1)} %slice.139), channel_id=1, source_target_pairs={{0,8},{8,16},{16,24},{24,32},{32,40},{40,48},{48,56},{56,64},{64,7... | collective-permute-start | bytes 786440 | tf_op jit(solution)/shard_map/ppermute | solution.py:89
  142.3 9.5 %copy-start.8 = (bf16[256,1024]{1,0:T(8,128)(2,1)S(1)}, bf16[256,1024]{1,0:T(8,128)(2,1)}, u32[]{:S(2)}) copy-start(bf16[256,1024]{1,0:T(8,128)(2,1)} %copy-done.7) | copy-start | bytes 1572868
  142.3 10.3 %copy-start.15 = (bf16[1024,640]{1,0:T(8,128)(2,1)S(1)}, bf16[1024,640]{1,0:T(8,128)(2,1)}, u32[]{:S(2)}) copy-start(bf16[1024,640]{1,0:T(8,128)(2,1)} %fusion.4) | copy-start | bytes 3932164
  145.0 13.3 %copy-start.4 = (bf16[256,1024]{1,0:T(8,128)(2,1)}, bf16[256,1024]{1,0:T(8,128)(2,1)S(1)}, u32[]{:S(2)}) copy-start(bf16[256,1024]{1,0:T(8,128)(2,1)S(1)} %collective-permute-done.13.refs_3_.refs_1_) | copy-start | bytes 1572868
  145.8 12.5 %collective-permute-start.15 = (bf16[128,1024]{1,0:T(8,128)(2,1)S(1)}, bf16[128,1024]{1,0:T(8,128)(2,1)S(1)}, u32[]{:S(2)}, u32[]{:S(2)}) collective-permute-start(bf16[128,1024]{1,0:T(8,128)(2,1)S(1)} %get-tuple-element.20), channel_id=1, source_target_pairs={{0,120},{8,0},{16,8},{24,16},{32,24},{40,32},{48,40},{56,48},{64,5... | collective-permute-start | bytes 786440 | tf_op jit(solution)/shard_map/ppermute | solution.py:90
  158.3 0.7 copy-start.16
  161.2 4.5 %copy-start = (bf16[1024,2048]{1,0:T(8,128)(2,1)S(1)}, bf16[1024,2048]{1,0:T(8,128)(2,1)}, u32[]{:S(2)}) copy-start(bf16[1024,2048]{1,0:T(8,128)(2,1)} %shard_map.71) | copy-start | bytes 12582916
  161.2 4.5 %copy-start.17 = (bf16[1024,1024]{1,0:T(8,128)(2,1)S(1)}, bf16[1024,1024]{1,0:T(8,128)(2,1)}, u32[]{:S(2)}) copy-start(bf16[1024,1024]{1,0:T(8,128)(2,1)} %multiply_convert_fusion) | copy-start | bytes 6291460
  165.3 4.2 %collective-permute-start.16 = (bf16[512,768]{0,1:T(8,128)(2,1)S(1)}, bf16[512,768]{0,1:T(8,128)(2,1)S(1)}, u32[]{:S(2)}, u32[]{:S(2)}) collective-permute-start(bf16[512,768]{0,1:T(8,128)(2,1)S(1)} %slice.147), channel_id=1, source_target_pairs={{0,1},{1,0},{2,3},{3,2},{4,5},{5,4},{6,7},{7,6},{8,9},{9,8},{10,11... | collective-permute-start | bytes 2359304 | tf_op jit(solution)/shard_map/ppermute | solution.py:157
  169.0 7.2 %collective-permute-start.21 = (bf16[512,1280]{1,0:T(8,128)(2,1)S(1)}, bf16[512,1280]{1,0:T(8,128)(2,1)S(1)}, u32[]{:S(2)}, u32[]{:S(2)}) collective-permute-start(bf16[512,1280]{1,0:T(8,128)(2,1)S(1)} %slice.157), channel_id=1, source_target_pairs={{0,1},{1,0},{2,3},{3,2},{4,5},{5,4},{6,7},{7,6},{8,9},{9,8},{10,11... | collective-permute-start | bytes 3932168 | tf_op jit(solution)/shard_map/ppermute | solution.py:157
  169.9 6.2 %copy-start.5 = (f32[512,768]{0,1:T(8,128)}, f32[512,768]{0,1:T(8,128)S(1)}, u32[]{:S(2)}) copy-start(f32[512,768]{0,1:T(8,128)S(1)} %get-tuple-element.8) | copy-start | bytes 4718596
  170.0 6.1 %collective-permute-start.17 = (bf16[128,384]{0,1:T(8,128)(2,1)S(1)}, bf16[128,384]{0,1:T(8,128)(2,1)S(1)}, u32[]{:S(2)}, u32[]{:S(2)}) collective-permute-start(bf16[128,384]{0,1:T(8,128)(2,1)S(1)} %get-tuple-element.15), channel_id=1, source_target_pairs={{0,2},{1,3},{2,4},{3,5},{4,6},{5,7},{6,0},{7,1},{8,10},{9,11},{10,... | collective-permute-start | bytes 294920 | tf_op jit(solution)/shard_map/ppermute | solution.py:162
  170.6 5.4 %collective-permute-start.19 = (bf16[128,384]{0,1:T(8,128)(2,1)S(1)}, bf16[128,384]{0,1:T(8,128)(2,1)S(1)}, u32[]{:S(2)}, u32[]{:S(2)}) collective-permute-start(bf16[128,384]{0,1:T(8,128)(2,1)S(1)} %get-tuple-element.16), channel_id=1, source_target_pairs={{0,6},{1,7},{2,0},{3,1},{4,2},{5,3},{6,4},{7,5},{8,14},{9,15},{10,... | collective-permute-start | bytes 294920 | tf_op jit(solution)/shard_map/ppermute | solution.py:163
  176.5 8.0 %collective-permute-start.22 = (bf16[128,640]{1,0:T(8,128)(2,1)S(1)}, bf16[128,640]{1,0:T(8,128)(2,1)S(1)}, u32[]{:S(2)}, u32[]{:S(2)}) collective-permute-start(bf16[128,640]{1,0:T(8,128)(2,1)S(1)} %get-tuple-element.11), channel_id=1, source_target_pairs={{0,2},{1,3},{2,4},{3,5},{4,6},{5,7},{6,0},{7,1},{8,10},{9,11},{10,... | collective-permute-start | bytes 491528 | tf_op jit(solution)/shard_map/ppermute | solution.py:162
  176.6 7.8 %collective-permute-start.24 = (bf16[128,640]{1,0:T(8,128)(2,1)S(1)}, bf16[128,640]{1,0:T(8,128)(2,1)S(1)}, u32[]{:S(2)}, u32[]{:S(2)}) collective-permute-start(bf16[128,640]{1,0:T(8,128)(2,1)S(1)} %get-tuple-element.12), channel_id=1, source_target_pairs={{0,6},{1,7},{2,0},{3,1},{4,2},{5,3},{6,4},{7,5},{8,14},{9,15},{10,... | collective-permute-start | bytes 491528 | tf_op jit(solution)/shard_map/ppermute | solution.py:163
  180.5 10.8 %collective-permute-start.18 = (bf16[128,768]{0,1:T(8,128)(2,1)}, bf16[128,768]{0,1:T(8,128)(2,1)}, u32[]{:S(2)}, u32[]{:S(2)}) collective-permute-start(bf16[128,768]{0,1:T(8,128)(2,1)} %pad_maximum_fusion.5), channel_id=1, source_target_pairs={{0,2},{1,3},{2,4},{3,5},{4,6},{5,7},{6,0},{7,1},{8,10},{9,11},{10,... | collective-permute-start | bytes 589832 | tf_op jit(solution)/shard_map/ppermute | solution.py:166
  181.2 10.1 %collective-permute-start.20 = (bf16[128,768]{0,1:T(8,128)(2,1)}, bf16[128,768]{0,1:T(8,128)(2,1)}, u32[]{:S(2)}, u32[]{:S(2)}) collective-permute-start(bf16[128,768]{0,1:T(8,128)(2,1)} %pad_maximum_fusion.6), channel_id=1, source_target_pairs={{0,6},{1,7},{2,0},{3,1},{4,2},{5,3},{6,4},{7,5},{8,14},{9,15},{10,... | collective-permute-start | bytes 589832 | tf_op jit(solution)/shard_map/ppermute | solution.py:167
  184.6 10.2 %collective-permute-start.23 = (bf16[128,1280]{1,0:T(8,128)(2,1)S(1)}, bf16[128,1280]{1,0:T(8,128)(2,1)}, u32[]{:S(2)}, u32[]{:S(2)}) collective-permute-start(bf16[128,1280]{1,0:T(8,128)(2,1)S(1)} %pad_maximum_fusion.3), channel_id=1, source_target_pairs={{0,2},{1,3},{2,4},{3,5},{4,6},{5,7},{6,0},{7,1},{8,10},{9,11},{10,... | collective-permute-start | bytes 983048 | tf_op jit(solution)/shard_map/ppermute | solution.py:166
  186.5 8.5 %collective-permute-start.25 = (bf16[128,1280]{1,0:T(8,128)(2,1)}, bf16[128,1280]{1,0:T(8,128)(2,1)}, u32[]{:S(2)}, u32[]{:S(2)}) collective-permute-start(bf16[128,1280]{1,0:T(8,128)(2,1)} %pad_maximum_fusion.4), channel_id=1, source_target_pairs={{0,6},{1,7},{2,0},{3,1},{4,2},{5,3},{6,4},{7,5},{8,14},{9,15},{10,... | collective-permute-start | bytes 983048 | tf_op jit(solution)/shard_map/ppermute | solution.py:167

commit v2 on v1

v2 whole, which is shorter than its diff:
```python
import jax
import jax.numpy as jnp
from jax import lax
from jax.experimental import pallas as pl
from jax.experimental.pallas import tpu as pltpu
from jax.sharding import PartitionSpec as P


eps = 1e-06


def place(home, moves, outs, n_fs, earlier=None):
    pieces = []
    used = []
    for piece, row, rows, *_ in moves:
        if not any(piece is known for known in pieces):
            pieces.append(piece)
            used.append(0)
        at = next(k for k, known in enumerate(pieces) if known is piece)
        used[at] = max(used[at], row + rows)
    where = [next(k for k, known in enumerate(pieces) if known is move[0]) for move in moves]
    n_old = 0 if earlier is None else 1

    def body(home_ref, *refs):
        ins = refs[: len(pieces)]
        out = refs[len(pieces) + n_old]
        sems = refs[-1]
        copies = []
        for k, (_, row, rows, offset, block, within, col) in enumerate(moves):
            slot = lax.rem(home_ref[0] + offset * home_ref[1] + n_fs, n_fs)
            start = pl.multiple_of(slot * block + within, 16)
            src = ins[where[k]]
            dst = out.at[pl.ds(start, rows), pl.ds(col, src.shape[1])]
            copies.append(pltpu.make_async_copy(src.at[pl.ds(row, rows)], dst, sems.at[k]))
        for copy in copies:
            copy.start()
        for copy in copies:
            copy.wait()

    anywhere = pl.BlockSpec(memory_space=pl.ANY)
    bands = [
        pl.BlockSpec((rows, piece.shape[1]), lambda _: (0, 0), memory_space=pltpu.VMEM)
        for piece, rows in zip(pieces, used)
    ]
    return pl.pallas_call(
        body,
        out_shape=outs,
        grid=(1,),
        in_specs=[pl.BlockSpec(memory_space=pltpu.SMEM)] + bands + [anywhere] * n_old,
        out_specs=anywhere,
        scratch_shapes=[pltpu.SemaphoreType.DMA((len(moves),))],
        input_output_aliases={1 + len(pieces): 0} if n_old else {},
    )(home, *pieces, *([] if earlier is None else [earlier]))


def on_device(prompt_rows, up_master, down_master, norm_gain):
    n_fs = lax.axis_size("fs")
    n_tp = lax.axis_size("tp")
    n_x = n_tp // 2
    half = n_fs // 2
    z = lax.axis_index("fs")
    tp = lax.axis_index("tp")
    x = tp // 2
    core = tp % 2
    direction = 1 - 2 * core
    home = jnp.stack([z, direction])

    up_rows, width = up_master.shape
    span = width // n_fs
    per_tp = n_fs // n_tp
    piece = per_tp * span
    down_cols = down_master.shape[1]
    full = down_cols * n_tp
    folds = down_cols // piece
    sides = full // width

    up_cast = (up_master * norm_gain[:, None]).astype(jnp.bfloat16)
    down_cast = down_master.astype(jnp.bfloat16)
    up_parts = up_cast.reshape(up_rows, per_tp, n_tp, span).transpose(2, 0, 1, 3)
    up_parts = up_parts.reshape(n_tp, 1, up_rows, piece)
    down_parts = down_cast.reshape(n_tp, span, folds, piece).transpose(0, 2, 1, 3)
    down_parts = down_parts.reshape(n_tp, 1, folds * span, piece)
    parts = jnp.concatenate([up_parts, down_parts], axis=1)
    pair = [(k, k ^ 1) for k in range(n_tp)]
    chips = [[2 * k + c for k in range(n_x)] for c in range(2)]
    parts = parts.reshape(n_x, 2, 2, *parts.shape[2:])
    parts = lax.all_to_all(
        parts, "tp", split_axis=0, concat_axis=0, tiled=True, axis_index_groups=chips
    )
    theirs = lax.ppermute(parts, "tp", pair)
    even = core == 0
    parts = jnp.stack([jnp.where(even, parts, theirs), jnp.where(even, theirs, parts)], axis=1)
    up_both = []
    down_both = []
    for group in (0, 1):
        chosen = jnp.where(even, parts[:, :, group], parts[:, :, 1 - group])
        chosen = chosen.reshape(n_tp, 2, *chosen.shape[3:])
        up_both.append(chosen[:, 0].transpose(1, 0, 2).reshape(up_rows, width))
        block = chosen[:, 1].reshape(sides, n_tp // sides, folds, span, piece)
        down_both.append(block.transpose(0, 3, 1, 2, 4).reshape(sides * span, width))

    ring = [
        (f * n_tp + k, (f + (1 if k % 2 == 0 else -1)) % n_fs * n_tp + k)
        for f in range(n_fs)
        for k in range(n_tp)
    ]
    up_msg = [jnp.concatenate(up_both, axis=0)]
    down_msg = [jnp.concatenate(down_both, axis=0)]
    last_sent = {}
    for step in range(1, half + 1):
        for name, msgs in (("up", up_msg), ("down", down_msg)):
            sent = msgs[-1]
            if step == half:
                sent = lax.optimization_barrier(sent[:up_rows])
                last_sent[name] = sent
            msgs.append(lax.ppermute(sent, ("fs", "tp"), ring))

    up = {-k: (up_msg[k], 0) for k in range(half)} | {half: (up_msg[half], 0)}
    down = {-k: (down_msg[k], 0) for k in range(half)} | {half: (down_msg[half], 0)}
    up[1 - half] = (last_sent["up"], 0)
    down[1 - half] = (last_sent["down"], 0)
    batches = [(1, half - 5), (half - 4, half - 3), (half - 2, half - 1)]
    for first, last in batches:
        steps = range(first, last + 1)
        bands = [m[k][up_rows:] for k in steps for m in (up_msg, down_msg)]
        got = lax.ppermute(jnp.concatenate(bands, axis=0), "tp", pair)
        for k in steps:
            up[k] = (got, 2 * (k - first) * up_rows)
            down[k] = (got, (2 * (k - first) + 1) * up_rows)

    def up_moves(keys):
        return [(up[k][0], up[k][1], up_rows, k, up_rows, 0, 0) for k in keys]

    def down_moves(keys):
        return [
            (down[k][0], down[k][1] + s * span, span, k, span, 0, s * width)
            for k in keys
            for s in range(sides)
        ]

    def within(least, most):
        return [k for k in sorted(up) if least <= abs(k) <= most]

    late = within(half - 2, half)
    up_shape = jax.ShapeDtypeStruct((n_fs * up_rows, width), jnp.bfloat16)
    down_shape = jax.ShapeDtypeStruct((n_fs * span, full), jnp.bfloat16)
    blank = jnp.zeros((up_rows, width), jnp.bfloat16)
    moves = up_moves(within(0, half - 3))
    moves += [(blank, 0, up_rows, k, up_rows, 0, 0) for k in late]
    up_sampler = place(home, moves, up_shape, n_fs)
    down_sampler = place(home, down_moves(within(0, half - 3)), down_shape, n_fs)

    tokens = prompt_rows.shape[0]
    block = tokens // n_tp
    order = [(dx % n_x, dc) for dc in (1, 0) for dx in range(1, n_x + 1)]
    rows = [
        lax.dynamic_slice_in_dim(
            prompt_rows, ((x + dx) % n_x * 2 + (core + dc) % 2) * block, block, axis=0
        )
        for dx, dc in order
    ]
    values = lax.optimization_barrier(jnp.concatenate(rows, axis=0)).astype(jnp.float32)
    scale = lax.rsqrt(jnp.mean(values * values, axis=-1, keepdims=True) + eps)
    normed = lax.optimization_barrier((values * scale).astype(jnp.bfloat16))
    pre_act = jnp.dot(normed, up_sampler, preferred_element_type=jnp.float32)
    pre_act = lax.optimization_barrier(pre_act)

    first = late[-1] - len(late) // 2
    rest = jnp.zeros((len(late) * up_rows, width), jnp.bfloat16)
    for k in sorted(late, key=lambda k: (abs(k), k > 0)):
        slot = (k * direction - first + 2 * n_fs) % n_fs
        band = up[k][0][up[k][1] : up[k][1] + up_rows]
        rest = lax.dynamic_update_slice_in_dim(rest, band, slot * up_rows, axis=0)
    ends = (len(late) - 1) * up_rows
    features = jnp.concatenate([normed, normed[:, :ends]], axis=1)
    features = lax.dynamic_slice_in_dim(
        features, (z + first) % n_fs * up_rows, len(late) * up_rows, axis=1
    )
    features = lax.optimization_barrier(features)
    pre_act = pre_act + jnp.dot(features, rest, preferred_element_type=jnp.float32)
    hidden = jnp.square(jax.nn.relu(pre_act)).astype(jnp.bfloat16)

    down_sampler = place(home, down_moves(late), down_shape, n_fs, down_sampler)
    up_sampler = place(home, up_moves(late), up_shape, n_fs, up_sampler)

    right = [(j, (j + 2) % n_tp) for j in range(n_tp)]
    left = [(j, (j - 2) % n_tp) for j in range(n_tp)]
    theirs = jnp.dot(hidden[: tokens // 2], down_sampler, preferred_element_type=jnp.float32)
    theirs = lax.ppermute(theirs.astype(jnp.bfloat16), "tp", pair)
    mine = jnp.dot(hidden[tokens // 2 :], down_sampler, preferred_element_type=jnp.float32)
    mine = lax.optimization_barrier(mine.astype(jnp.bfloat16))
    chip = mine.astype(jnp.float32) + theirs.astype(jnp.float32)
    after, across, before, total = [chip[k * block : (k + 1) * block] for k in range(n_x)]
    across = across.astype(jnp.bfloat16)
    mid = full // 2
    one = lax.ppermute(across[:, :mid], "tp", right).astype(jnp.float32)
    two = lax.ppermute(across[:, mid:], "tp", left).astype(jnp.float32)
    after = jnp.concatenate([after[:, :mid] + one, after[:, mid:]], axis=1)
    before = jnp.concatenate([before[:, :mid], before[:, mid:] + two], axis=1)
    after = lax.ppermute(after.astype(jnp.bfloat16), "tp", right).astype(jnp.float32)
    before = lax.ppermute(before.astype(jnp.bfloat16), "tp", left).astype(jnp.float32)
    total = (total + after + before).astype(jnp.bfloat16)
    return (up_sampler[None], down_sampler[None], total)


def solution(mesh):
    in_specs = (P(("grp", "fs"), None), P("fs", "tp"), P("fs", "tp"), P("fs"))
    out_specs = (
        P(("grp", "tp"), None, None),
        P(("grp", "tp"), None, None),
        P(("grp", "fs", "tp"), None),
    )

    return jax.shard_map(
        on_device, mesh=mesh, in_specs=in_specs, out_specs=out_specs, check_vma=False
    )
```

time: 198 us -> 200 us (1.010)
  waiting for transfers between devices: 36.1 us -> 78.4 us
  starting transfers between devices: 61.8 us -> 19.9 us
  local copies, waits for them, and re-layouts: 27.2 us -> 31.2 us
  other arithmetic: 16.8 us -> 20.4 us
  Pallas kernels: 16.2 us -> 13.3 us
  matrix products: 23 us -> 20.4 us
    ppermute x22 -> x23, starting transfers between devices: 55.2 us -> 16.7 us  [the longest x16 8.29 us: on_device(): msgs.append(lax.ppermute(sent, ('fs', 'tp'), ring))]
    ppermute x22 -> x23, waiting for transfers between devices: 33.8 us -> 66.9 us  [the longest x16 58.9 us: on_device(): msgs.append(lax.ppermute(sent, ('fs', 'tp'), ring))]
    ppermute x2 -> x1, waiting for transfers between devices: 0.23 us -> 7.94 us  [on_device(): lax.ppermute(before.astype(jnp.bfloat16), 'tp', left).astype(jnp.float32)]
    slice x6 -> x10, local copies, waits for them, and re-layouts: 1.13 us -> 6.89 us  [the longest x6 5.99 us: on_device(): bands = [m[k][up_rows:] for k in steps for m in (up_msg, down_msg)]]
    pallas_call x5 -> x4, Pallas kernels: 16.2 us -> 13.3 us  [place(): pl.pallas_call(body, out_shape=outs, grid=(1,), in_specs=[pl.BlockSpec(me...]
    unnamed x49 -> x55, local copies, waits for them, and re-layouts: 21.6 us -> 19 us
    ppermute x2 -> x1, starting transfers between devices: 5.44 us -> 3.07 us  [on_device(): lax.ppermute(before.astype(jnp.bfloat16), 'tp', left).astype(jnp.float32)]
    dot_general x1, matrix products: 5.74 us -> 3.44 us  [on_device(): jnp.dot(features, rest, preferred_element_type=jnp.float32)]
  transfers between devices with their start and end apart: 26 -> 25, of which waited for: 10 -> 15; matrix products, arithmetic and copies ran while one was open for 27% -> 29% of each run, Pallas kernels for 7% -> 5%
where the time goes in v2:
time: 200 us; the launch traced here: 199 us
  waiting for transfers between devices  78.4 us (39%)
  local copies, waits for them, and re-layouts  31.2 us (16%)
  other arithmetic  20.4 us (10%)
  matrix products  20.4 us (10%)
  starting transfers between devices  19.9 us (10%)
  blocking collectives  13.9 us (7%)
  Pallas kernels  13.3 us (7%)
    ppermute x16, waiting for transfers between devices, on_device(): msgs.append(lax.ppermute(sent, ('fs', 'tp'), ring))  58.9 us
    unnamed x55, local copies, waits for them, and re-layouts  19 us
    all_to_all x1, blocking collectives, on_device(): lax.all_to_all(parts, 'tp', split_axis=0, concat_axis=0, tiled=True, axis...  13.9 us
    pallas_call x4, Pallas kernels, place(): pl.pallas_call(body, out_shape=outs, grid=(1,), in_specs=[pl.BlockSpec(me...  13.3 us
    dot_general x1, matrix products, on_device(): pre_act = jnp.dot(normed, up_sampler, preferred_element_type=jnp.float32)  9.95 us
    ppermute x16, starting transfers between devices, on_device(): msgs.append(lax.ppermute(sent, ('fs', 'tp'), ring))  8.29 us
    ppermute x1, waiting for transfers between devices, on_device(): lax.ppermute(before.astype(jnp.bfloat16), 'tp', left).astype(jnp.float32)  7.94 us
    ppermute x1, waiting for transfers between devices, on_device(): one = lax.ppermute(across[:, :mid], 'tp', right).astype(jnp.float32)  6.56 us
  transfers between devices with their start and end apart: 25, of which 15 were waited for; matrix products, arithmetic and copies ran while one was open for 29% of the time, Pallas kernels for 5%

profile of v2, /device:TPU:40, one launch (start us, length us, event | category | flops | bytes accessed | tf_op | source)
XLA Modules:
  0.0 198.8 jit_solution(14960658175209099930)
XLA Ops:
  0.6 1.1 convert_element_type.46
  2.0 1.2 copy.31
  3.3 0.7 multiply_convert_fusion.1
  4.1 13.9 %all_to_all.5 = bf16[4,2,2,128,128]{3,4,1,2,0:T(8,128)(2,1)S(1)} all-to-all(bf16[4,2,2,128,128]{3,4,1,2,0:T(8,128)(2,1)S(1)} %copy.35), channel_id=1, replica_groups={{0,2,4,6},{1,3,5,7},{8,10,12,14},{9,11,13,15},{16,18,20,22},{17,19,21,2..., dimensions={0} | all-to-all | bytes 1048576 | tf_op jit(solution)/shard_map/all_to_all | solution.py:87
  18.5 1.9 dynamic-slice_dynamic-update-slice_fusion.7
  20.4 1.9 dynamic-slice_dynamic-update-slice_fusion.6
  23.7 2.9 %collective-permute-start.1 = (bf16[256,1024]{1,0:T(8,128)(2,1)S(1)}, bf16[256,1024]{1,0:T(8,128)(2,1)S(1)}, u32[]{:S(2)}, u32[]{:S(2)}) collective-permute-start(bf16[256,1024]{1,0:T(8,128)(2,1)S(1)} %bitcast_dynamic-update-slice_fusion.refs_5_), channel_id=1, source_target_pairs={{0,8},{1,121},{2,10},{3,123},{4,12},{5,125},{6,14},{7,127},{8,16},... | collective-permute-start | bytes 1572872 | tf_op jit(solution)/shard_map/ppermute | solution.py:116
  26.6 2.9 %collective-permute-start.8 = (bf16[256,1024]{1,0:T(8,128)(2,1)S(1)}, bf16[256,1024]{1,0:T(8,128)(2,1)S(1)}, u32[]{:S(2)}, u32[]{:S(2)}) collective-permute-start(bf16[256,1024]{1,0:T(8,128)(2,1)S(1)} %constant_dynamic-update-slice_fusion.refs_5_), channel_id=1, source_target_pairs={{0,8},{1,121},{2,10},{3,123},{4,12},{5,125},{6,14},{7,127},{8,16},... | collective-permute-start | bytes 1572872 | tf_op jit(solution)/shard_map/ppermute | solution.py:116
  29.5 1.9 dynamic-slice_dynamic-update-slice_fusion.5
  31.4 1.9 dynamic-slice_dynamic-update-slice_fusion.4
  33.3 1.9 dynamic-slice_dynamic-update-slice_fusion.3
  35.2 18.2 %collective-permute-done.1.refs_4_ = bf16[256,1024]{1,0:T(8,128)(2,1)S(1)} collective-permute-done((bf16[256,1024]{1,0:T(8,128)(2,1)S(1)}, bf16[256,1024]{1,0:T(8,128)(2,1)S(1)}, u32[]{:S(2)}, u32[]{:S(2)}) %collective-permute-start.1) | collective-permute-done | bytes 524320 | tf_op jit(solution)/shard_map/ppermute | solution.py:116
  53.4 5.6 %collective-permute-done.8.refs_4_ = bf16[256,1024]{1,0:T(8,128)(2,1)S(1)} collective-permute-done((bf16[256,1024]{1,0:T(8,128)(2,1)S(1)}, bf16[256,1024]{1,0:T(8,128)(2,1)S(1)}, u32[]{:S(2)}, u32[]{:S(2)}) %collective-permute-start.8) | collective-permute-done | bytes 524320 | tf_op jit(solution)/shard_map/ppermute | solution.py:116
  59.0 2.1 %dynamic-slice_dynamic-update-slice_fusion.2 = bf16[1024,2048]{1,0:T(8,128)(2,1)} fusion(bf16[1024,2048]{1,0:T(8,128)(2,1)} %dynamic-slice_dynamic-update-slice_fusion.3, bf16[1024,2048]{1,0:T(8,128)(2,1)} %param.4, s32[]{:T(128)S(6)} %select_n.172), kind=kLoop, calls=%fused_computation.31 | loop fusion | bytes 1048580
  61.1 1.9 dynamic-slice_dynamic-update-slice_fusion.1
  62.9 1.9 dynamic-slice_dynamic-update-slice_fusion
  64.8 5.4 %collective-permute-done.9.refs_3_ = bf16[256,1024]{1,0:T(8,128)(2,1)S(1)} collective-permute-done((bf16[256,1024]{1,0:T(8,128)(2,1)S(1)}, bf16[256,1024]{1,0:T(8,128)(2,1)S(1)}, u32[]{:S(2)}, u32[]{:S(2)}) %collective-permute-start.9) | collective-permute-done | bytes 524320 | tf_op jit(solution)/shard_map/ppermute | solution.py:116
  70.2 3.3 %fusion = f32[1024]{0:T(1024)S(1)} fusion(bf16[1024,2048]{1,0:T(8,128)(2,1)} %dynamic-slice_dynamic-update-slice_fusion), kind=kLoop, calls=%fused_computation.2 | loop fusion | flops 6290432 | bytes 4198400 | tf_op jit(solution)/shard_map/reduce_sum | solution.py:163
  73.5 2.3 %collective-permute-done.3.refs_2_ = bf16[256,1024]{1,0:T(8,128)(2,1)S(1)} collective-permute-done((bf16[256,1024]{1,0:T(8,128)(2,1)S(1)}, bf16[256,1024]{1,0:T(8,128)(2,1)S(1)}, u32[]{:S(2)}, u32[]{:S(2)}) %collective-permute-start.3) | collective-permute-done | bytes 524320 | tf_op jit(solution)/shard_map/ppermute | solution.py:116
  75.8 5.6 %collective-permute-done.10.refs_2_ = bf16[256,1024]{1,0:T(8,128)(2,1)S(1)} collective-permute-done((bf16[256,1024]{1,0:T(8,128)(2,1)S(1)}, bf16[256,1024]{1,0:T(8,128)(2,1)S(1)}, u32[]{:S(2)}, u32[]{:S(2)}) %collective-permute-start.10) | collective-permute-done | bytes 524320 | tf_op jit(solution)/shard_map/ppermute | solution.py:116
  81.5 0.8 slice_dynamic-update-slice_fusion.8
  82.2 0.7 slice_dynamic-update-slice_fusion.7
  83.0 0.7 slice_dynamic-update-slice_fusion.6
  83.7 3.4 %collective-permute-done.4.refs_1_ = bf16[256,1024]{1,0:T(8,128)(2,1)S(1)} collective-permute-done((bf16[256,1024]{1,0:T(8,128)(2,1)S(1)}, bf16[256,1024]{1,0:T(8,128)(2,1)S(1)}, u32[]{:S(2)}, u32[]{:S(2)}) %collective-permute-start.4) | collective-permute-done | bytes 524320 | tf_op jit(solution)/shard_map/ppermute | solution.py:116
  87.1 5.6 %collective-permute-done.11.refs_1_ = bf16[256,1024]{1,0:T(8,128)(2,1)S(1)} collective-permute-done((bf16[256,1024]{1,0:T(8,128)(2,1)S(1)}, bf16[256,1024]{1,0:T(8,128)(2,1)S(1)}, u32[]{:S(2)}, u32[]{:S(2)}) %collective-permute-start.11) | collective-permute-done | bytes 524320 | tf_op jit(solution)/shard_map/ppermute | solution.py:116
  92.7 0.8 slice_dynamic-update-slice_fusion.5
  93.5 0.7 slice_dynamic-update-slice_fusion.4
  94.2 0.7 slice_dynamic-update-slice_fusion.3
  94.9 2.1 %collective-permute-start.17 = (bf16[768,1024]{1,0:T(8,128)(2,1)}, bf16[768,1024]{1,0:T(8,128)(2,1)S(1)}, u32[]{:S(2)}, u32[]{:S(2)}) collective-permute-start(bf16[768,1024]{1,0:T(8,128)(2,1)} %slice_dynamic-update-slice_fusion.3), channel_id=1, source_target_pairs={{0,1},{1,0},{2,3},{3,2},{4,5},{5,4},{6,7},{7,6},{8,9},{9,8},{10,11... | collective-permute-start | bytes 4718600 | tf_op jit(solution)/shard_map/ppermute | solution.py:126
  97.0 1.4 collective-permute-done.5.refs_0_
  98.4 5.6 %collective-permute-done.12.refs_0_ = bf16[256,1024]{1,0:T(8,128)(2,1)} collective-permute-done((bf16[256,1024]{1,0:T(8,128)(2,1)S(1)}, bf16[256,1024]{1,0:T(8,128)(2,1)}, u32[]{:S(2)}, u32[]{:S(2)}) %collective-permute-start.12) | collective-permute-done | bytes 524320 | tf_op jit(solution)/shard_map/ppermute | solution.py:116
  104.0 4.9 %fusion.1 = bf16[1024,2048]{1,0:T(8,128)(2,1)} fusion(bf16[1024,2048]{1,0:T(8,128)(2,1)} %dynamic-slice_dynamic-update-slice_fusion, f32[1024]{0:T(1024)S(1)} %add_rsqrt_fusion), kind=kLoop, calls=%fused_computation.3 | loop fusion | flops 6291456 | bytes 8392704 | tf_op jit(solution)/shard_map/convert_element_type | solution.py:164
  109.0 1.1 slice.171
  110.1 1.0 slice.172
  111.0 1.0 slice.173
  112.0 1.0 slice.174
  113.1 1.1 pad_maximum_fusion.1
  114.2 2.2 %collective-permute-start.18 = (bf16[512,1024]{1,0:T(8,128)(2,1)}, bf16[512,1024]{1,0:T(8,128)(2,1)}, u32[]{:S(2)}, u32[]{:S(2)}) collective-permute-start(bf16[512,1024]{1,0:T(8,128)(2,1)} %pad_maximum_fusion.1), channel_id=1, source_target_pairs={{0,1},{1,0},{2,3},{3,2},{4,5},{5,4},{6,7},{7,6},{8,9},{9,8},{10,11... | collective-permute-start | bytes 3145736 | tf_op jit(solution)/shard_map/ppermute | solution.py:126
  116.4 2.8 %fusion.2 = bf16[1024,640]{1,0:T(8,128)(2,1)} fusion(s32[]{:T(128)S(6)} %select_n.176, bf16[1024,2048]{1,0:T(8,128)(2,1)} %fusion.1, bf16[1024,512]{1,0:T(8,128)(2,1)S(1)} %slice-done), kind=kLoop, calls=%fused_computation.10 | loop fusion | flops 2621440 | bytes 6553604 | tf_op jit(solution)/shard_map/concatenate | solution.py:175
  119.2 1.7 collective-permute-start.14
  121.6 1.0 slice.162
  122.8 0.8 collective-permute-done.7
  123.6 1.1 fusion.13
  124.8 5.0 %collective-permute-done.14 = bf16[256,1024]{1,0:T(8,128)(2,1)S(1)} collective-permute-done((bf16[256,1024]{1,0:T(8,128)(2,1)}, bf16[256,1024]{1,0:T(8,128)(2,1)S(1)}, u32[]{:S(2)}, u32[]{:S(2)}) %collective-permute-start.14) | collective-permute-done | bytes 524320 | tf_op jit(solution)/shard_map/ppermute | solution.py:116
  129.8 0.7 fusion.12
  131.0 1.0 pad_maximum_fusion
  132.1 0.8 broadcast_in_dim.14.refs_8_
  133.4 4.2 %shard_map.67.refs_4_ = bf16[2048,1024]{1,0:T(8,128)(2,1)} custom-call(s32[2]{0:T(128)} %pad_add_fusion.home_ref, bf16[256,1024]{1,0:T(8,128)(2,1)} %collective-permute-done.5.refs_0_, bf16[256,1024]{1,0:T(8,128)(2,1)} %copy-done.16, bf16[256,1024]{1,0:T(8,128)(2,1)} %copy-done.14, bf16[256,1024]{1,0:T(8,128)(2,1)} %copy-done.12, ...), custom_call_target="tpu_custom_call" | custom-call | tf_op jit(solution)/shard_map/pallas_call | solution.py:45
  137.6 9.9 %fusion.16 = f32[1024,1024]{1,0:T(8,128)} fusion(bf16[1024,2048]{1,0:T(8,128)(2,1)} %fusion.1, bf16[2048,1024]{1,0:T(8,128)(2,1)} %shard_map.67.refs_4_), kind=kOutput, calls=%fused_computation.69 | convolution fusion | flops 4294967296 | bytes 12582912 | tf_op jit(solution)/shard_map/dot_general | solution.py:165
  147.5 4.0 %shard_map.69.refs_4_ = bf16[1024,2048]{1,0:T(8,128)(2,1)} custom-call(s32[2]{0:T(128)} %pad_add_fusion.home_ref, bf16[256,1024]{1,0:T(8,128)(2,1)} %collective-permute-done.12.refs_0_, bf16[256,1024]{1,0:T(8,128)(2,1)} %copy-done.15, bf16[256,1024]{1,0:T(8,128)(2,1)} %copy-done.13, bf16[256,1024]{1,0:T(8,128)(2,1)} %copy-done.11, ...), custom_call_target="tpu_custom_call" | custom-call | tf_op jit(solution)/shard_map/pallas_call | solution.py:45
  151.8 3.4 %fusion.17 = f32[1024,1024]{1,0:T(8,128)S(1)} fusion(bf16[1024,640]{1,0:T(8,128)(2,1)} %fusion.2, bf16[640,1024]{1,0:T(8,128)(2,1)S(1)} %constant_dynamic-update-slice_fusion.2), kind=kOutput, calls=%fused_computation.70 | convolution fusion | flops 1342177280 | bytes 6815744 | tf_op jit(solution)/shard_map/dot_general | solution.py:180
  155.3 1.1 multiply_convert_fusion
  156.4 2.6 %shard_map.70 = bf16[1024,2048]{1,0:T(8,128)(2,1)} custom-call(s32[2]{0:T(128)} %pad_add_fusion.home_ref, bf16[128,1024]{1,0:T(8,128)(2,1)} %get-tuple-element.17.refs_0_, bf16[256,1024]{1,0:T(8,128)(2,1)} %collective-permute-done.13.refs_1_, bf16[512,1024]{1,0:T(8,128)(2,1)} %copy-done.2, ...), custom_call_target="tpu_custom_call", output_to_operand_aliasing={{}: (5, {})} | custom-call | tf_op jit(solution)/shard_map/pallas_call | solution.py:45
  159.0 4.7 %convolution_convert_fusion = bf16[512,2048]{1,0:T(8,128)(2,1)S(1)} fusion(bf16[1024,2048]{1,0:T(8,128)(2,1)} %shard_map.70, bf16[1024,1024]{1,0:T(8,128)(2,1)S(1)} %multiply_convert_fusion), kind=kOutput, calls=%fused_computation.8 | convolution fusion | flops 2148532224 | bytes 7340032 | tf_op jit(solution)/shard_map/dot_general | solution.py:188
  164.3 2.4 %convolution_convert_fusion.1 = bf16[512,2048]{1,0:T(8,128)(2,1)S(1)} fusion(bf16[1024,2048]{1,0:T(8,128)(2,1)S(1)} %copy-done, bf16[1024,1024]{1,0:T(8,128)(2,1)S(1)} %multiply_convert_fusion), kind=kOutput, calls=%fused_computation.9 | convolution fusion | flops 2148532224 | bytes 7340032 | tf_op jit(solution)/shard_map/dot_general | solution.py:190
  166.7 1.4 collective-permute-done.20
  168.1 1.0 fusion.10
  169.9 2.7 %collective-permute-start.23 = (bf16[128,1024]{1,0:T(8,128)(2,1)S(1)}, bf16[128,1024]{1,0:T(8,128)(2,1)S(1)}, u32[]{:S(2)}, u32[]{:S(2)}) collective-permute-start(bf16[128,1024]{1,0:T(8,128)(2,1)S(1)} %get-tuple-element.8), channel_id=1, source_target_pairs={{0,6},{1,7},{2,0},{3,1},{4,2},{5,3},{6,4},{7,5},{8,14},{9,15},{10,... | collective-permute-start | bytes 786440 | tf_op jit(solution)/shard_map/ppermute | solution.py:197
  172.6 6.6 %collective-permute-done.21 = bf16[128,1024]{1,0:T(8,128)(2,1)S(1)} collective-permute-done((bf16[128,1024]{1,0:T(8,128)(2,1)S(1)}, bf16[128,1024]{1,0:T(8,128)(2,1)S(1)}, u32[]{:S(2)}, u32[]{:S(2)}) %collective-permute-start.21) | collective-permute-done | bytes 262176 | tf_op jit(solution)/shard_map/ppermute | solution.py:196
  179.4 3.1 %collective-permute-start.24 = (bf16[128,2048]{1,0:T(8,128)(2,1)S(1)}, bf16[128,2048]{1,0:T(8,128)(2,1)S(1)}, u32[]{:S(2)}, u32[]{:S(2)}) collective-permute-start(bf16[128,2048]{1,0:T(8,128)(2,1)S(1)} %pad_maximum_fusion.5), channel_id=1, source_target_pairs={{0,6},{1,7},{2,0},{3,1},{4,2},{5,3},{6,4},{7,5},{8,14},{9,15},{10,... | collective-permute-start | bytes 1572872 | tf_op jit(solution)/shard_map/ppermute | solution.py:201
  182.6 2.5 %shard_map.68 = bf16[2048,1024]{1,0:T(8,128)(2,1)} custom-call(s32[2]{0:T(128)} %pad_add_fusion.home_ref, bf16[128,1024]{1,0:T(8,128)(2,1)} %copy-done.5, bf16[256,1024]{1,0:T(8,128)(2,1)} %copy-done.6, bf16[512,1024]{1,0:T(8,128)(2,1)} %copy-done.2, bf16[128,1024]{1,0:T(8,128)(2,1)} %copy-done.19, ...), custom_call_target="tpu_custom_call", output_to_operand_aliasing={{}: (5, {})} | custom-call | tf_op jit(solution)/shard_map/pallas_call | solution.py:45
  185.1 7.9 %collective-permute-done.24 = bf16[128,2048]{1,0:T(8,128)(2,1)S(1)} collective-permute-done((bf16[128,2048]{1,0:T(8,128)(2,1)S(1)}, bf16[128,2048]{1,0:T(8,128)(2,1)S(1)}, u32[]{:S(2)}, u32[]{:S(2)}) %collective-permute-start.24) | collective-permute-done | bytes 524320 | tf_op jit(solution)/shard_map/ppermute | solution.py:201
  193.0 3.6 %collective-permute-done.22 = bf16[128,2048]{1,0:T(8,128)(2,1)S(1)} collective-permute-done((bf16[128,2048]{1,0:T(8,128)(2,1)S(1)}, bf16[128,2048]{1,0:T(8,128)(2,1)S(1)}, u32[]{:S(2)}, u32[]{:S(2)}) %collective-permute-start.22) | collective-permute-done | bytes 524320 | tf_op jit(solution)/shard_map/ppermute | solution.py:200
  196.6 2.2 %fusion.4 = bf16[128,2048]{1,0:T(8,128)(2,1)} fusion(f32[512,2048]{1,0:T(8,128)} %copy-done.1, bf16[128,2048]{1,0:T(8,128)(2,1)S(1)} %collective-permute-done.24, bf16[128,2048]{1,0:T(8,128)(2,1)S(1)} %collective-permute-done.22), kind=kLoop, calls=%fused_computation.13 | loop fusion | flops 1310720 | bytes 2621440 | tf_op jit(solution)/shard_map/convert_element_type | solution.py:202
  (103 shorter events, 6.3 us)
Async XLA Ops:
  18.3 4.0 %collective-permute-start = (bf16[4,2,2,128,128]{4,3,2,1,0:T(8,128)(2,1)S(1)}, bf16[4,2,2,128,128]{4,3,2,1,0:T(8,128)(2,1)S(1)}, u32[]{:S(2)}, u32[]{:S(2)}) collective-permute-start(bf16[4,2,2,128,128]{4,3,2,1,0:T(8,128)(2,1)S(1)} %copy.37), channel_id=1, source_target_pairs={{0,1},{1,0},{2,3},{3,2},{4,5},{5,4},{6,7},{7,6},{8,9},{9,8},{10,11... | collective-permute-start | bytes 1572872 | tf_op jit(solution)/shard_map/ppermute | solution.py:90
  23.7 11.5 %copy-start.18 = (bf16[256,1024]{1,0:T(8,128)(2,1)}, bf16[256,1024]{1,0:T(8,128)(2,1)S(1)}, u32[]{:S(2)}) copy-start(bf16[256,1024]{1,0:T(8,128)(2,1)S(1)} %bitcast_dynamic-update-slice_fusion.refs_5_) | copy-start | bytes 1572868
  23.7 29.7 %collective-permute-start.1 = (bf16[256,1024]{1,0:T(8,128)(2,1)S(1)}, bf16[256,1024]{1,0:T(8,128)(2,1)S(1)}, u32[]{:S(2)}, u32[]{:S(2)}) collective-permute-start(bf16[256,1024]{1,0:T(8,128)(2,1)S(1)} %bitcast_dynamic-update-slice_fusion.refs_5_), channel_id=1, source_target_pairs={{0,8},{1,121},{2,10},{3,123},{4,12},{5,125},{6,14},{7,127},{8,16},... | collective-permute-start | bytes 1572872 | tf_op jit(solution)/shard_map/ppermute | solution.py:116
  26.6 26.8 %copy-start.17 = (bf16[256,1024]{1,0:T(8,128)(2,1)}, bf16[256,1024]{1,0:T(8,128)(2,1)S(1)}, u32[]{:S(2)}) copy-start(bf16[256,1024]{1,0:T(8,128)(2,1)S(1)} %constant_dynamic-update-slice_fusion.refs_5_) | copy-start | bytes 1572868
  26.6 32.4 %collective-permute-start.8 = (bf16[256,1024]{1,0:T(8,128)(2,1)S(1)}, bf16[256,1024]{1,0:T(8,128)(2,1)S(1)}, u32[]{:S(2)}, u32[]{:S(2)}) collective-permute-start(bf16[256,1024]{1,0:T(8,128)(2,1)S(1)} %constant_dynamic-update-slice_fusion.refs_5_), channel_id=1, source_target_pairs={{0,8},{1,121},{2,10},{3,123},{4,12},{5,125},{6,14},{7,127},{8,16},... | collective-permute-start | bytes 1572872 | tf_op jit(solution)/shard_map/ppermute | solution.py:116
  53.4 29.6 %copy-start.10 = (bf16[256,1024]{1,0:T(8,128)(2,1)}, bf16[256,1024]{1,0:T(8,128)(2,1)S(1)}, u32[]{:S(2)}) copy-start(bf16[256,1024]{1,0:T(8,128)(2,1)S(1)} %collective-permute-done.1.refs_4_) | copy-start | bytes 1572868
  53.4 11.5 %collective-permute-start.2 = (bf16[256,1024]{1,0:T(8,128)(2,1)S(1)}, bf16[256,1024]{1,0:T(8,128)(2,1)S(1)}, u32[]{:S(2)}, u32[]{:S(2)}) collective-permute-start(bf16[256,1024]{1,0:T(8,128)(2,1)S(1)} %collective-permute-done.1.refs_4_), channel_id=1, source_target_pairs={{0,8},{1,121},{2,10},{3,123},{4,12},{5,125},{6,14},{7,127},{8,16},... | collective-permute-start | bytes 1572872 | tf_op jit(solution)/shard_map/ppermute | solution.py:116
  59.0 24.0 %copy-start.9 = (bf16[256,1024]{1,0:T(8,128)(2,1)}, bf16[256,1024]{1,0:T(8,128)(2,1)S(1)}, u32[]{:S(2)}) copy-start(bf16[256,1024]{1,0:T(8,128)(2,1)S(1)} %collective-permute-done.8.refs_4_) | copy-start | bytes 1572868
  59.0 11.2 %collective-permute-start.9 = (bf16[256,1024]{1,0:T(8,128)(2,1)S(1)}, bf16[256,1024]{1,0:T(8,128)(2,1)S(1)}, u32[]{:S(2)}, u32[]{:S(2)}) collective-permute-start(bf16[256,1024]{1,0:T(8,128)(2,1)S(1)} %collective-permute-done.8.refs_4_), channel_id=1, source_target_pairs={{0,8},{1,121},{2,10},{3,123},{4,12},{5,125},{6,14},{7,127},{8,16},... | collective-permute-start | bytes 1572872 | tf_op jit(solution)/shard_map/ppermute | solution.py:116
  64.8 29.4 %copy-start.12 = (bf16[256,1024]{1,0:T(8,128)(2,1)}, bf16[256,1024]{1,0:T(8,128)(2,1)S(1)}, u32[]{:S(2)}) copy-start(bf16[256,1024]{1,0:T(8,128)(2,1)S(1)} %collective-permute-done.2.refs_3_) | copy-start | bytes 1572868
  64.8 11.0 %collective-permute-start.3 = (bf16[256,1024]{1,0:T(8,128)(2,1)S(1)}, bf16[256,1024]{1,0:T(8,128)(2,1)S(1)}, u32[]{:S(2)}, u32[]{:S(2)}) collective-permute-start(bf16[256,1024]{1,0:T(8,128)(2,1)S(1)} %collective-permute-done.2.refs_3_), channel_id=1, source_target_pairs={{0,8},{1,121},{2,10},{3,123},{4,12},{5,125},{6,14},{7,127},{8,16},... | collective-permute-start | bytes 1572872 | tf_op jit(solution)/shard_map/ppermute | solution.py:116
  70.2 24.0 %copy-start.11 = (bf16[256,1024]{1,0:T(8,128)(2,1)}, bf16[256,1024]{1,0:T(8,128)(2,1)S(1)}, u32[]{:S(2)}) copy-start(bf16[256,1024]{1,0:T(8,128)(2,1)S(1)} %collective-permute-done.9.refs_3_) | copy-start | bytes 1572868
  70.2 11.2 %collective-permute-start.10 = (bf16[256,1024]{1,0:T(8,128)(2,1)S(1)}, bf16[256,1024]{1,0:T(8,128)(2,1)S(1)}, u32[]{:S(2)}, u32[]{:S(2)}) collective-permute-start(bf16[256,1024]{1,0:T(8,128)(2,1)S(1)} %collective-permute-done.9.refs_3_), channel_id=1, source_target_pairs={{0,8},{1,121},{2,10},{3,123},{4,12},{5,125},{6,14},{7,127},{8,16},... | collective-permute-start | bytes 1572872 | tf_op jit(solution)/shard_map/ppermute | solution.py:116
  75.8 22.6 %copy-start.14 = (bf16[256,1024]{1,0:T(8,128)(2,1)}, bf16[256,1024]{1,0:T(8,128)(2,1)S(1)}, u32[]{:S(2)}) copy-start(bf16[256,1024]{1,0:T(8,128)(2,1)S(1)} %collective-permute-done.3.refs_2_) | copy-start | bytes 1572868
  75.8 11.2 %collective-permute-start.4 = (bf16[256,1024]{1,0:T(8,128)(2,1)S(1)}, bf16[256,1024]{1,0:T(8,128)(2,1)S(1)}, u32[]{:S(2)}, u32[]{:S(2)}) collective-permute-start(bf16[256,1024]{1,0:T(8,128)(2,1)S(1)} %collective-permute-done.3.refs_2_), channel_id=1, source_target_pairs={{0,8},{1,121},{2,10},{3,123},{4,12},{5,125},{6,14},{7,127},{8,16},... | collective-permute-start | bytes 1572872 | tf_op jit(solution)/shard_map/ppermute | solution.py:116
  81.5 15.6 %copy-start.13 = (bf16[256,1024]{1,0:T(8,128)(2,1)}, bf16[256,1024]{1,0:T(8,128)(2,1)S(1)}, u32[]{:S(2)}) copy-start(bf16[256,1024]{1,0:T(8,128)(2,1)S(1)} %collective-permute-done.10.refs_2_) | copy-start | bytes 1572868
  81.5 11.2 %collective-permute-start.11 = (bf16[256,1024]{1,0:T(8,128)(2,1)S(1)}, bf16[256,1024]{1,0:T(8,128)(2,1)S(1)}, u32[]{:S(2)}, u32[]{:S(2)}) collective-permute-start(bf16[256,1024]{1,0:T(8,128)(2,1)S(1)} %collective-permute-done.10.refs_2_), channel_id=1, source_target_pairs={{0,8},{1,121},{2,10},{3,123},{4,12},{5,125},{6,14},{7,127},{8,16},... | collective-permute-start | bytes 1572872 | tf_op jit(solution)/shard_map/ppermute | solution.py:116
  87.1 17.0 %copy-start.16 = (bf16[256,1024]{1,0:T(8,128)(2,1)}, bf16[256,1024]{1,0:T(8,128)(2,1)S(1)}, u32[]{:S(2)}) copy-start(bf16[256,1024]{1,0:T(8,128)(2,1)S(1)} %collective-permute-done.4.refs_1_) | copy-start | bytes 1572868
  87.1 11.3 %collective-permute-start.5 = (bf16[256,1024]{1,0:T(8,128)(2,1)S(1)}, bf16[256,1024]{1,0:T(8,128)(2,1)}, u32[]{:S(2)}, u32[]{:S(2)}) collective-permute-start(bf16[256,1024]{1,0:T(8,128)(2,1)S(1)} %collective-permute-done.4.refs_1_), channel_id=1, source_target_pairs={{0,8},{1,121},{2,10},{3,123},{4,12},{5,125},{6,14},{7,127},{8,16},... | collective-permute-start | bytes 1572872 | tf_op jit(solution)/shard_map/ppermute | solution.py:116
  92.7 5.7 %copy-start.15 = (bf16[256,1024]{1,0:T(8,128)(2,1)}, bf16[256,1024]{1,0:T(8,128)(2,1)S(1)}, u32[]{:S(2)}) copy-start(bf16[256,1024]{1,0:T(8,128)(2,1)S(1)} %collective-permute-done.11.refs_1_) | copy-start | bytes 1572868
  92.7 11.3 %collective-permute-start.12 = (bf16[256,1024]{1,0:T(8,128)(2,1)S(1)}, bf16[256,1024]{1,0:T(8,128)(2,1)}, u32[]{:S(2)}, u32[]{:S(2)}) collective-permute-start(bf16[256,1024]{1,0:T(8,128)(2,1)S(1)} %collective-permute-done.11.refs_1_), channel_id=1, source_target_pairs={{0,8},{1,121},{2,10},{3,123},{4,12},{5,125},{6,14},{7,127},{8,16},... | collective-permute-start | bytes 1572872 | tf_op jit(solution)/shard_map/ppermute | solution.py:116
  94.9 37.2 %collective-permute-start.17 = (bf16[768,1024]{1,0:T(8,128)(2,1)}, bf16[768,1024]{1,0:T(8,128)(2,1)S(1)}, u32[]{:S(2)}, u32[]{:S(2)}) collective-permute-start(bf16[768,1024]{1,0:T(8,128)(2,1)} %slice_dynamic-update-slice_fusion.3), channel_id=1, source_target_pairs={{0,1},{1,0},{2,3},{3,2},{4,5},{5,4},{6,7},{7,6},{8,9},{9,8},{10,11... | collective-permute-start | bytes 4718600 | tf_op jit(solution)/shard_map/ppermute | solution.py:126
  98.4 14.5 %collective-permute-start.6 = (bf16[256,1024]{1,0:T(8,128)(2,1)}, bf16[256,1024]{1,0:T(8,128)(2,1)S(1)}, u32[]{:S(2)}, u32[]{:S(2)}) collective-permute-start(bf16[256,1024]{1,0:T(8,128)(2,1)} %collective-permute-done.5.refs_0_), channel_id=1, source_target_pairs={{0,8},{1,121},{2,10},{3,123},{4,12},{5,125},{6,14},{7,127},{8,16},... | collective-permute-start | bytes 1572872 | tf_op jit(solution)/shard_map/ppermute | solution.py:116
  104.0 15.2 %collective-permute-start.13 = (bf16[256,1024]{1,0:T(8,128)(2,1)}, bf16[256,1024]{1,0:T(8,128)(2,1)}, u32[]{:S(2)}, u32[]{:S(2)}) collective-permute-start(bf16[256,1024]{1,0:T(8,128)(2,1)} %collective-permute-done.12.refs_0_), channel_id=1, source_target_pairs={{0,8},{1,121},{2,10},{3,123},{4,12},{5,125},{6,14},{7,127},{8,16},... | collective-permute-start | bytes 1572872 | tf_op jit(solution)/shard_map/ppermute | solution.py:116
  109.0 7.4 %slice-start = ((bf16[1024,2048]{1,0:T(8,128)(2,1)}), bf16[1024,512]{1,0:T(8,128)(2,1)S(1)}, s32[]{:S(2)}) async-start(bf16[1024,2048]{1,0:T(8,128)(2,1)} %fusion.1), calls=%async_computation.1 | async-start | bytes 2097152 | tf_op jit(solution)/shard_map/slice | solution.py:175
  113.0 9.7 %copy-start.6 = (bf16[256,1024]{1,0:T(8,128)(2,1)}, bf16[256,1024]{1,0:T(8,128)(2,1)S(1)}, u32[]{:S(2)}) copy-start(bf16[256,1024]{1,0:T(8,128)(2,1)S(1)} %collective-permute-done.6.refs_1_) | copy-start | bytes 1572868
  113.0 10.6 %collective-permute-start.7 = (bf16[256,1024]{1,0:T(8,128)(2,1)S(1)}, bf16[256,1024]{1,0:T(8,128)(2,1)}, u32[]{:S(2)}, u32[]{:S(2)}) collective-permute-start(bf16[256,1024]{1,0:T(8,128)(2,1)S(1)} %collective-permute-done.6.refs_1_), channel_id=1, source_target_pairs={{0,8},{1,121},{2,10},{3,123},{4,12},{5,125},{6,14},{7,127},{8,16},... | collective-permute-start | bytes 1572872 | tf_op jit(solution)/shard_map/ppermute | solution.py:116
  114.2 17.9 %collective-permute-start.18 = (bf16[512,1024]{1,0:T(8,128)(2,1)}, bf16[512,1024]{1,0:T(8,128)(2,1)}, u32[]{:S(2)}, u32[]{:S(2)}) collective-permute-start(bf16[512,1024]{1,0:T(8,128)(2,1)} %pad_maximum_fusion.1), channel_id=1, source_target_pairs={{0,1},{1,0},{2,3},{3,2},{4,5},{5,4},{6,7},{7,6},{8,9},{9,8},{10,11... | collective-permute-start | bytes 3145736 | tf_op jit(solution)/shard_map/ppermute | solution.py:126
  119.2 10.6 %collective-permute-start.14 = (bf16[256,1024]{1,0:T(8,128)(2,1)}, bf16[256,1024]{1,0:T(8,128)(2,1)S(1)}, u32[]{:S(2)}, u32[]{:S(2)}) collective-permute-start(bf16[256,1024]{1,0:T(8,128)(2,1)} %collective-permute-done.13.refs_1_), channel_id=1, source_target_pairs={{0,8},{1,121},{2,10},{3,123},{4,12},{5,125},{6,14},{7,127},{8,16},... | collective-permute-start | bytes 1572872 | tf_op jit(solution)/shard_map/ppermute | solution.py:116
  122.8 1.9 copy-start.7
  124.7 27.0 %copy-start.5 = (bf16[128,1024]{1,0:T(8,128)(2,1)}, bf16[128,1024]{1,0:T(8,128)(2,1)S(1)}, u32[]{:S(2)}) copy-start(bf16[128,1024]{1,0:T(8,128)(2,1)S(1)} %get-tuple-element.20.refs_0_) | copy-start | bytes 786436
  124.7 27.0 %collective-permute-start.16 = (bf16[128,1024]{1,0:T(8,128)(2,1)S(1)}, bf16[128,1024]{1,0:T(8,128)(2,1)S(1)}, u32[]{:S(2)}, u32[]{:S(2)}) collective-permute-start(bf16[128,1024]{1,0:T(8,128)(2,1)S(1)} %get-tuple-element.20.refs_0_), channel_id=1, source_target_pairs={{0,8},{1,121},{2,10},{3,123},{4,12},{5,125},{6,14},{7,127},{8,16},... | collective-permute-start | bytes 786440 | tf_op jit(solution)/shard_map/ppermute | solution.py:116
  130.5 25.9 %collective-permute-start.19 = (bf16[128,1024]{1,0:T(8,128)(2,1)}, bf16[128,1024]{1,0:T(8,128)(2,1)}, u32[]{:S(2)}, u32[]{:S(2)}) collective-permute-start(bf16[128,1024]{1,0:T(8,128)(2,1)} %get-tuple-element.17.refs_0_), channel_id=1, source_target_pairs={{0,8},{1,121},{2,10},{3,123},{4,12},{5,125},{6,14},{7,127},{8,16},... | collective-permute-start | bytes 786440 | tf_op jit(solution)/shard_map/ppermute | solution.py:116
  132.1 19.5 %collective-permute-start.15 = (bf16[512,1024]{1,0:T(8,128)(2,1)}, bf16[512,1024]{1,0:T(8,128)(2,1)S(1)}, u32[]{:S(2)}, u32[]{:S(2)}) collective-permute-start(bf16[512,1024]{1,0:T(8,128)(2,1)} %pad_maximum_fusion), channel_id=1, source_target_pairs={{0,1},{1,0},{2,3},{3,2},{4,5},{5,4},{6,7},{7,6},{8,9},{9,8},{10,11... | collective-permute-start | bytes 3145736 | tf_op jit(solution)/shard_map/ppermute | solution.py:126
  132.1 1.3 copy-start.3
  147.5 4.1 %copy-start.8 = (bf16[640,1024]{1,0:T(8,128)(2,1)S(1)}, bf16[640,1024]{1,0:T(8,128)(2,1)}, u32[]{:S(2)}) copy-start(bf16[640,1024]{1,0:T(8,128)(2,1)} %copy-done.7) | copy-start | bytes 3932164
  151.6 3.6 %copy-start.2 = (bf16[512,1024]{1,0:T(8,128)(2,1)}, bf16[512,1024]{1,0:T(8,128)(2,1)S(1)}, u32[]{:S(2)}) copy-start(bf16[512,1024]{1,0:T(8,128)(2,1)S(1)} %collective-permute-done.15.refs_2_) | copy-start | bytes 3145732
  151.7 3.5 %copy-start.19 = (bf16[128,1024]{1,0:T(8,128)(2,1)}, bf16[128,1024]{1,0:T(8,128)(2,1)S(1)}, u32[]{:S(2)}) copy-start(bf16[128,1024]{1,0:T(8,128)(2,1)S(1)} %collective-permute-done.16.refs_3_) | copy-start | bytes 786436
  151.8 3.5 %copy-start.4 = (f32[1024,1024]{1,0:T(8,128)S(1)}, f32[1024,1024]{1,0:T(8,128)}, u32[]{:S(2)}) copy-start(f32[1024,1024]{1,0:T(8,128)} %fusion.16) | copy-start | bytes 12582916
  159.0 5.3 %copy-start = (bf16[1024,2048]{1,0:T(8,128)(2,1)S(1)}, bf16[1024,2048]{1,0:T(8,128)(2,1)}, u32[]{:S(2)}) copy-start(bf16[1024,2048]{1,0:T(8,128)(2,1)} %shard_map.70) | copy-start | bytes 12582916
  163.7 4.4 %collective-permute-start.20 = (bf16[512,2048]{1,0:T(8,128)(2,1)S(1)}, bf16[512,2048]{1,0:T(8,128)(2,1)S(1)}, u32[]{:S(2)}, u32[]{:S(2)}) collective-permute-start(bf16[512,2048]{1,0:T(8,128)(2,1)S(1)} %convolution_convert_fusion), channel_id=1, source_target_pairs={{0,1},{1,0},{2,3},{3,2},{4,5},{5,4},{6,7},{7,6},{8,9},{9,8},{10,11... | collective-permute-start | bytes 6291464 | tf_op jit(solution)/shard_map/ppermute | solution.py:189
  169.2 10.0 %copy-start.1 = (f32[512,2048]{1,0:T(8,128)}, f32[512,2048]{1,0:T(8,128)S(1)}, u32[]{:S(2)}) copy-start(f32[512,2048]{1,0:T(8,128)S(1)} %get-tuple-element.6) | copy-start | bytes 12582916
  169.3 9.9 %collective-permute-start.21 = (bf16[128,1024]{1,0:T(8,128)(2,1)S(1)}, bf16[128,1024]{1,0:T(8,128)(2,1)S(1)}, u32[]{:S(2)}, u32[]{:S(2)}) collective-permute-start(bf16[128,1024]{1,0:T(8,128)(2,1)S(1)} %get-tuple-element.7), channel_id=1, source_target_pairs={{0,2},{1,3},{2,4},{3,5},{4,6},{5,7},{6,0},{7,1},{8,10},{9,11},{10,... | collective-permute-start | bytes 786440 | tf_op jit(solution)/shard_map/ppermute | solution.py:196
  169.9 9.2 %collective-permute-start.23 = (bf16[128,1024]{1,0:T(8,128)(2,1)S(1)}, bf16[128,1024]{1,0:T(8,128)(2,1)S(1)}, u32[]{:S(2)}, u32[]{:S(2)}) collective-permute-start(bf16[128,1024]{1,0:T(8,128)(2,1)S(1)} %get-tuple-element.8), channel_id=1, source_target_pairs={{0,6},{1,7},{2,0},{3,1},{4,2},{5,3},{6,4},{7,5},{8,14},{9,15},{10,... | collective-permute-start | bytes 786440 | tf_op jit(solution)/shard_map/ppermute | solution.py:197
  179.4 13.7 %collective-permute-start.24 = (bf16[128,2048]{1,0:T(8,128)(2,1)S(1)}, bf16[128,2048]{1,0:T(8,128)(2,1)S(1)}, u32[]{:S(2)}, u32[]{:S(2)}) collective-permute-start(bf16[128,2048]{1,0:T(8,128)(2,1)S(1)} %pad_maximum_fusion.5), channel_id=1, source_target_pairs={{0,6},{1,7},{2,0},{3,1},{4,2},{5,3},{6,4},{7,5},{8,14},{9,15},{10,... | collective-permute-start | bytes 1572872 | tf_op jit(solution)/shard_map/ppermute | solution.py:201
  182.5 14.1 %collective-permute-start.22 = (bf16[128,2048]{1,0:T(8,128)(2,1)S(1)}, bf16[128,2048]{1,0:T(8,128)(2,1)S(1)}, u32[]{:S(2)}, u32[]{:S(2)}) collective-permute-start(bf16[128,2048]{1,0:T(8,128)(2,1)S(1)} %pad_maximum_fusion.4), channel_id=1, source_target_pairs={{0,2},{1,3},{2,4},{3,5},{4,6},{5,7},{6,0},{7,1},{8,10},{9,11},{10,... | collective-permute-start | bytes 1572872 | tf_op jit(solution)/shard_map/ppermute | solution.py:200

commit v3 on v1

--- a/solution.py
+++ b/solution.py
@@ -136,7 +136,8 @@
         features, (z + late[0]) % n_fs * up_rows, len(late) * up_rows, axis=1
     )
     features = lax.optimization_barrier(features)
-    pre_act = pre_act + jnp.dot(features, rest, preferred_element_type=jnp.float32)
+    added = jnp.dot(features, rest, preferred_element_type=jnp.float32)
+    pre_act = pre_act + lax.optimization_barrier(added)
     hidden = jnp.square(jax.nn.relu(pre_act)).astype(jnp.bfloat16)
 
     moves = down_moves(within(half - 1, half - 1))
@@ -150,24 +151,27 @@
     right = [(j, (j + 2) % n_tp) for j in range(n_tp)]
     left = [(j, (j - 2) % n_tp) for j in range(n_tp)]
     bounds = [0, 3 * full // 8, full]
-    sums = []
+    summed = jnp.zeros((block, full), jnp.bfloat16)
     for lo, hi in zip(bounds[:-1], bounds[1:]):
         weights = lax.slice_in_dim(down_sampler, lo, hi, axis=1)
         partial = jnp.dot(hidden, weights, preferred_element_type=jnp.float32).astype(jnp.bfloat16)
         theirs = lax.ppermute(partial[: tokens // 2], "tp", pair)
         chip = partial[tokens // 2 :].astype(jnp.float32) + theirs.astype(jnp.float32)
-        after, across, before, total = [chip[k * block : (k + 1) * block] for k in range(n_x)]
+        after, across, before, total = [chip[j * block : (j + 1) * block] for j in range(n_x)]
         across = across.astype(jnp.bfloat16)
         mid = (hi - lo) // 2
-        first = lax.ppermute(across[:, :mid], "tp", right).astype(jnp.float32)
-        second = lax.ppermute(across[:, mid:], "tp", left).astype(jnp.float32)
-        after = jnp.concatenate([after[:, :mid] + first, after[:, mid:]], axis=1)
-        before = jnp.concatenate([before[:, :mid], before[:, mid:] + second], axis=1)
-        after = lax.ppermute(after.astype(jnp.bfloat16), "tp", right).astype(jnp.float32)
-        before = lax.ppermute(before.astype(jnp.bfloat16), "tp", left).astype(jnp.float32)
-        total = total + after + before
-        sums.append(total.astype(jnp.bfloat16))
-    return (up_sampler[None], down_sampler[None], jnp.concatenate(sums, axis=1))
+        ends = across[:, :mid], across[:, mid:]
+        first = lax.ppermute(ends[0], "tp", right).astype(jnp.float32)
+        second = lax.ppermute(ends[1], "tp", left).astype(jnp.float32)
+        first = (after[:, :mid] + first).astype(jnp.bfloat16)
+        second = (before[:, mid:] + second).astype(jnp.bfloat16)
+        after = lax.dynamic_update_slice(after.astype(jnp.bfloat16), first, (0, 0))
+        before = lax.dynamic_update_slice(before.astype(jnp.bfloat16), second, (0, mid))
+        after = lax.ppermute(after, "tp", right).astype(jnp.float32)
+        before = lax.ppermute(before, "tp", left).astype(jnp.float32)
+        total = (total + after + before).astype(jnp.bfloat16)
+        summed = lax.dynamic_update_slice(summed, total, (0, lo))
+    return (up_sampler[None], down_sampler[None], summed)
 
 
 def solution(mesh):

time: 198 us -> 198 us (level)
  waiting for transfers between devices: 36.1 us -> 39.3 us
  matrix products: 23 us -> 19.9 us
    ppermute x8, waiting for transfers between devices: 4.97 us -> 8.15 us  [the longest x2 5.68 us: on_device(): first = lax.ppermute(ends[0], 'tp', right).astype(jnp.float32)]
    concatenate x5 -> x0, other arithmetic: 2.99 us -> none  [the longest x2 1.43 us: on_device(): jnp.concatenate([before[:, :mid], before[:, mid:] + second], axis=1)]
    dot_general x1, matrix products: 5.74 us -> 3.25 us  [on_device(): added = jnp.dot(features, rest, preferred_element_type=jnp.float32)]
    unnamed x49 -> x47, local copies, waits for them, and re-layouts: 21.6 us -> 20.9 us
  transfers between devices with their start and end apart: 26 -> 26, of which waited for: 10 -> 10; matrix products, arithmetic and copies ran while one was open for 27% -> 26% of each run, Pallas kernels for 7% -> 7%
where the time goes in v3:
time: 198 us; the launch traced here: 197 us
  starting transfers between devices  61.5 us (31%)
  waiting for transfers between devices  39.3 us (20%)
  local copies, waits for them, and re-layouts  27.3 us (14%)
  matrix products  19.9 us (10%)
  other arithmetic  16.5 us (8%)
  Pallas kernels  16.2 us (8%)
  blocking collectives  14.7 us (7%)
    ppermute x7, starting transfers between devices, on_device(): held[step] = lax.ppermute(held[step - 1], 'fs', back)  44.3 us
    ppermute x7, waiting for transfers between devices, on_device(): held[step] = lax.ppermute(held[step - 1], 'fs', back)  28.3 us
    unnamed x47, local copies, waits for them, and re-layouts  20.9 us
    pallas_call x5, Pallas kernels, place(): pl.pallas_call(body, out_shape=outs, in_specs=[pl.BlockSpec(memory_space=...  16.2 us
    all_to_all x1, blocking collectives, on_device(): parts = lax.all_to_all(parts, 'tp', split_axis=0, concat_axis=0, tiled=True)  14.7 us
    dot_general x1, matrix products, on_device(): pre_act = jnp.dot(normed, up_sampler[0], preferred_element_type=jnp.float32)  10.1 us
    dot_general x2, matrix products, on_device(): jnp.dot(hidden, weights, preferred_element_type=jnp.float32)  6.56 us
    ppermute x2, starting transfers between devices, on_device(): second = lax.ppermute(ends[1], 'tp', left).astype(jnp.float32)  5.9 us
  transfers between devices with their start and end apart: 26, of which 10 were waited for; matrix products, arithmetic and copies ran while one was open for 26% of the time, Pallas kernels for 7%

profile of v3, /device:TPU:40, one launch (start us, length us, event | category | flops | bytes accessed | tf_op | source)
XLA Modules:
  0.0 196.7 jit_solution(13025978076312263073)
XLA Ops:
  0.6 1.1 convert_element_type.82
  2.0 1.2 copy.35
  3.3 0.7 multiply_convert_fusion.1
  4.1 14.7 %all_to_all.5 = bf16[8,2,128,128]{2,3,1,0:T(8,128)(2,1)S(1)} all-to-all(bf16[8,2,128,128]{2,3,1,0:T(8,128)(2,1)S(1)} %copy.39), channel_id=1, replica_groups=mesh['grp'=2,'fs'=16,'tp'=8] {'tp'}, dimensions={0} | all-to-all | bytes 1048576 | tf_op jit(solution)/shard_map/all_to_all | solution.py:76
  19.7 22.5 %collective-permute-start.6 = (bf16[256,1024]{1,0:T(8,128)(2,1)S(1)}, bf16[256,1024]{1,0:T(8,128)(2,1)S(1)}, u32[]{:S(2)}, u32[]{:S(2)}) collective-permute-start(bf16[256,1024]{1,0:T(8,128)(2,1)S(1)} %pad_maximum_fusion.1.refs_0_), channel_id=1, source_target_pairs={{0,120},{8,0},{16,8},{24,16},{32,24},{40,32},{48,40},{56,48},{64,5... | collective-permute-start | bytes 1572872 | tf_op jit(solution)/shard_map/ppermute | solution.py:88
  42.2 10.8 %collective-permute-done.6.refs_2_ = bf16[256,1024]{1,0:T(8,128)(2,1)S(1)} collective-permute-done((bf16[256,1024]{1,0:T(8,128)(2,1)S(1)}, bf16[256,1024]{1,0:T(8,128)(2,1)S(1)}, u32[]{:S(2)}, u32[]{:S(2)}) %collective-permute-start.6) | collective-permute-done | bytes 524320 | tf_op jit(solution)/shard_map/ppermute | solution.py:88
  53.0 3.7 %collective-permute-start.7 = (bf16[256,1024]{1,0:T(8,128)(2,1)S(1)}, bf16[256,1024]{1,0:T(8,128)(2,1)S(1)}, u32[]{:S(2)}, u32[]{:S(2)}) collective-permute-start(bf16[256,1024]{1,0:T(8,128)(2,1)S(1)} %collective-permute-done.6.refs_2_), channel_id=1, source_target_pairs={{0,120},{8,0},{16,8},{24,16},{32,24},{40,32},{48,40},{56,48},{64,5... | collective-permute-start | bytes 1572872 | tf_op jit(solution)/shard_map/ppermute | solution.py:88
  56.8 2.0 %dynamic-slice_dynamic-update-slice_fusion.7 = bf16[1024,2048]{1,0:T(8,128)(2,1)} fusion(bf16[1024,2048]{1,0:T(8,128)(2,1)} %param.4, s32[]{:T(128)S(6)} %select_n.90), kind=kLoop, calls=%fused_computation.27 | loop fusion | bytes 1048580
  58.8 1.9 dynamic-slice_dynamic-update-slice_fusion.6
  60.7 6.0 %collective-permute-done.7.refs_4_ = bf16[256,1024]{1,0:T(8,128)(2,1)S(1)} collective-permute-done((bf16[256,1024]{1,0:T(8,128)(2,1)S(1)}, bf16[256,1024]{1,0:T(8,128)(2,1)S(1)}, u32[]{:S(2)}, u32[]{:S(2)}) %collective-permute-start.7) | collective-permute-done | bytes 524320 | tf_op jit(solution)/shard_map/ppermute | solution.py:88
  66.7 3.7 %collective-permute-start.8 = (bf16[256,1024]{1,0:T(8,128)(2,1)S(1)}, bf16[256,1024]{1,0:T(8,128)(2,1)S(1)}, u32[]{:S(2)}, u32[]{:S(2)}) collective-permute-start(bf16[256,1024]{1,0:T(8,128)(2,1)S(1)} %collective-permute-done.7.refs_4_), channel_id=1, source_target_pairs={{0,120},{8,0},{16,8},{24,16},{32,24},{40,32},{48,40},{56,48},{64,5... | collective-permute-start | bytes 1572872 | tf_op jit(solution)/shard_map/ppermute | solution.py:88
  70.4 2.1 %dynamic-slice_dynamic-update-slice_fusion.5 = bf16[1024,2048]{1,0:T(8,128)(2,1)} fusion(bf16[1024,2048]{1,0:T(8,128)(2,1)} %dynamic-slice_dynamic-update-slice_fusion.6, bf16[1024,2048]{1,0:T(8,128)(2,1)} %param.4, s32[]{:T(128)S(6)} %select_n.94), kind=kLoop, calls=%fused_computation.25 | loop fusion | bytes 1048580
  72.4 1.9 dynamic-slice_dynamic-update-slice_fusion.4
  74.3 1.9 dynamic-slice_dynamic-update-slice_fusion.3
  76.2 3.3 %collective-permute-done.8.refs_6_ = bf16[256,1024]{1,0:T(8,128)(2,1)S(1)} collective-permute-done((bf16[256,1024]{1,0:T(8,128)(2,1)S(1)}, bf16[256,1024]{1,0:T(8,128)(2,1)S(1)}, u32[]{:S(2)}, u32[]{:S(2)}) %collective-permute-start.8) | collective-permute-done | bytes 524320 | tf_op jit(solution)/shard_map/ppermute | solution.py:88
  79.5 3.7 %collective-permute-start.9 = (bf16[256,1024]{1,0:T(8,128)(2,1)S(1)}, bf16[256,1024]{1,0:T(8,128)(2,1)}, u32[]{:S(2)}, u32[]{:S(2)}) collective-permute-start(bf16[256,1024]{1,0:T(8,128)(2,1)S(1)} %collective-permute-done.8.refs_6_), channel_id=1, source_target_pairs={{0,120},{8,0},{16,8},{24,16},{32,24},{40,32},{48,40},{56,48},{64,5... | collective-permute-start | bytes 1572872 | tf_op jit(solution)/shard_map/ppermute | solution.py:88
  83.2 1.9 dynamic-slice_dynamic-update-slice_fusion.2
  85.0 1.9 dynamic-slice_dynamic-update-slice_fusion.1
  86.9 1.9 dynamic-slice_dynamic-update-slice_fusion
  88.8 2.6 %collective-permute-done.9.refs_8_ = bf16[256,1024]{1,0:T(8,128)(2,1)} collective-permute-done((bf16[256,1024]{1,0:T(8,128)(2,1)S(1)}, bf16[256,1024]{1,0:T(8,128)(2,1)}, u32[]{:S(2)}, u32[]{:S(2)}) %collective-permute-start.9) | collective-permute-done | bytes 524320 | tf_op jit(solution)/shard_map/ppermute | solution.py:88
  91.4 3.8 %collective-permute-start.10 = (bf16[256,1024]{1,0:T(8,128)(2,1)}, bf16[256,1024]{1,0:T(8,128)(2,1)S(1)}, u32[]{:S(2)}, u32[]{:S(2)}) collective-permute-start(bf16[256,1024]{1,0:T(8,128)(2,1)} %collective-permute-done.9.refs_8_), channel_id=1, source_target_pairs={{0,120},{8,0},{16,8},{24,16},{32,24},{40,32},{48,40},{56,48},{64,5... | collective-permute-start | bytes 1572872 | tf_op jit(solution)/shard_map/ppermute | solution.py:88
  95.2 3.1 %fusion = f32[1024]{0:T(1024)S(1)} fusion(bf16[1024,2048]{1,0:T(8,128)(2,1)} %dynamic-slice_dynamic-update-slice_fusion), kind=kLoop, calls=%fused_computation.2 | loop fusion | flops 6290432 | bytes 4198400 | tf_op jit(solution)/shard_map/reduce_sum | solution.py:126
  98.3 5.6 %collective-permute-done.10.refs_10_.refs_1_ = bf16[256,1024]{1,0:T(8,128)(2,1)S(1)} collective-permute-done((bf16[256,1024]{1,0:T(8,128)(2,1)}, bf16[256,1024]{1,0:T(8,128)(2,1)S(1)}, u32[]{:S(2)}, u32[]{:S(2)}) %collective-permute-start.10) | collective-permute-done | bytes 524320 | tf_op jit(solution)/shard_map/ppermute | solution.py:88
  103.9 3.6 %collective-permute-start.11 = (bf16[256,1024]{1,0:T(8,128)(2,1)S(1)}, bf16[256,1024]{1,0:T(8,128)(2,1)S(1)}, u32[]{:S(2)}, u32[]{:S(2)}) collective-permute-start(bf16[256,1024]{1,0:T(8,128)(2,1)S(1)} %collective-permute-done.10.refs_10_.refs_1_), channel_id=1, source_target_pairs={{0,120},{8,0},{16,8},{24,16},{32,24},{40,32},{48,40},{56,48},{64,5... | collective-permute-start | bytes 1572872 | tf_op jit(solution)/shard_map/ppermute | solution.py:88
  107.5 2.9 %fusion.1 = bf16[1024,2048]{1,0:T(8,128)(2,1)S(1)} fusion(bf16[1024,2048]{1,0:T(8,128)(2,1)} %dynamic-slice_dynamic-update-slice_fusion, f32[1024]{0:T(1024)S(1)} %add_rsqrt_fusion), kind=kLoop, calls=%fused_computation.3 | loop fusion | flops 6291456 | bytes 8392704 | tf_op jit(solution)/shard_map/convert_element_type | solution.py:127
  110.5 2.0 %copy-done.1 = bf16[1024,2048]{1,0:T(8,128)(2,1)} copy-done((bf16[1024,2048]{1,0:T(8,128)(2,1)}, bf16[1024,2048]{1,0:T(8,128)(2,1)S(1)}, u32[]{:S(2)}) %copy-start.1) | copy-done | bytes 4194328
  112.6 2.8 %fusion.4 = bf16[1024,640]{1,0:T(8,128)(2,1)} fusion(s32[]{:T(128)S(6)} %select_n.103, bf16[1024,2048]{1,0:T(8,128)(2,1)} %copy-done.1, bf16[1024,512]{1,0:T(8,128)(2,1)S(1)} %slice.133), kind=kLoop, calls=%fused_computation.13 | loop fusion | flops 2621440 | bytes 6553604 | tf_op jit(solution)/shard_map/concatenate | solution.py:134
  115.4 3.8 %shard_map.69.refs_4_ = bf16[1024,2048]{1,0:T(8,128)(2,1)} custom-call(s32[1]{0:T(128)} %bitcast.z_ref, bf16[256,1024]{1,0:T(8,128)(2,1)} %copy-done.2, bf16[256,1024]{1,0:T(8,128)(2,1)} %copy-done.11, bf16[256,1024]{1,0:T(8,128)(2,1)} %copy-done.10, bf16[256,1024]{1,0:T(8,128)(2,1)} %copy-done.13, bf16[256,1024]{1,0:T(8,128)(2,1)} %copy-done.12, ...), custom_call_target="tpu_custom_call" | custom-call | tf_op jit(solution)/shard_map/pallas_call | solution.py:38
  119.3 0.7 broadcast_in_dim.12.refs_11_
  120.0 4.8 %shard_map.67.refs_5_ = bf16[2048,1024]{1,0:T(8,128)(2,1)} custom-call(s32[1]{0:T(128)} %bitcast.z_ref, bf16[256,1024]{1,0:T(8,128)(2,1)} %copy-done.2, bf16[256,1024]{1,0:T(8,128)(2,1)} %copy-done.11, bf16[256,1024]{1,0:T(8,128)(2,1)} %copy-done.10, bf16[256,1024]{1,0:T(8,128)(2,1)} %copy-done.13, bf16[256,1024]{1,0:T(8,128)(2,1)} %copy-done.12, ...), custom_call_target="tpu_custom_call" | custom-call | tf_op jit(solution)/shard_map/pallas_call | solution.py:38
  124.9 3.3 %collective-permute-start.13 = (bf16[256,1024]{1,0:T(8,128)(2,1)S(1)}, bf16[256,1024]{1,0:T(8,128)(2,1)S(1)}, u32[]{:S(2)}, u32[]{:S(2)}) collective-permute-start(bf16[256,1024]{1,0:T(8,128)(2,1)S(1)} %collective-permute-done.11.refs_1_.refs_3_), channel_id=1, source_target_pairs={{0,120},{8,0},{16,8},{24,16},{32,24},{40,32},{48,40},{56,48},{64,5... | collective-permute-start | bytes 1572872 | tf_op jit(solution)/shard_map/ppermute | solution.py:88
  128.2 10.1 %fusion.24 = f32[1024,1024]{1,0:T(8,128)} fusion(bf16[1024,2048]{1,0:T(8,128)(2,1)} %copy-done.1, bf16[2048,1024]{1,0:T(8,128)(2,1)} %shard_map.67.refs_5_), kind=kOutput, calls=%fused_computation.57 | convolution fusion | flops 4294967296 | bytes 12582912 | tf_op jit(solution)/shard_map/dot_general | solution.py:128
  138.3 2.5 %collective-permute-done.12.refs_2_.refs_0_ = bf16[256,1024]{1,0:T(8,128)(2,1)S(1)} collective-permute-done((bf16[256,1024]{1,0:T(8,128)(2,1)S(1)}, bf16[256,1024]{1,0:T(8,128)(2,1)S(1)}, u32[]{:S(2)}, u32[]{:S(2)}) %collective-permute-start.12) | collective-permute-done | bytes 524320 | tf_op jit(solution)/shard_map/ppermute | solution.py:87
  140.8 0.8 slice.131
  141.5 0.7 slice_dynamic-update-slice_fusion.2
  142.3 2.7 %shard_map.70.refs_3_ = bf16[1024,2048]{1,0:T(8,128)(2,1)} custom-call(s32[1]{0:T(128)} %bitcast.z_ref, bf16[256,1024]{1,0:T(8,128)(2,1)} %collective-permute-done.4.refs_9_.refs_0_, bf16[256,1024]{1,0:T(8,128)(2,1)} %copy-done.15, bf16[256,1024]{1,0:T(8,128)(2,1)} %copy-done.8, bf16[256,1024]{1,0:T(8,128)(2,1)} %copy-done.7, ...), custom_call_target="tpu_custom_call", output_to_operand_aliasing={{}: (5, {})} | custom-call | tf_op jit(solution)/shard_map/pallas_call | solution.py:38
  145.0 0.8 slice_dynamic-update-slice_fusion.1
  145.8 3.2 %collective-permute-start.15 = (bf16[128,1024]{1,0:T(8,128)(2,1)S(1)}, bf16[128,1024]{1,0:T(8,128)(2,1)}, u32[]{:S(2)}, u32[]{:S(2)}) collective-permute-start(bf16[128,1024]{1,0:T(8,128)(2,1)S(1)} %get-tuple-element.20), channel_id=1, source_target_pairs={{0,120},{8,0},{16,8},{24,16},{32,24},{40,32},{48,40},{56,48},{64,5... | collective-permute-start | bytes 786440 | tf_op jit(solution)/shard_map/ppermute | solution.py:90
  149.0 0.4 collective-permute-done.14.refs_4_
  149.4 1.7 constant_dynamic-update-slice_fusion.1
  151.1 0.7 constant_dynamic-update-slice_fusion
  151.9 0.7 slice_dynamic-update-slice_fusion
  152.6 3.3 %fusion.25 = f32[1024,1024]{1,0:T(8,128)S(1)} fusion(bf16[1024,640]{1,0:T(8,128)(2,1)S(1)} %copy-done.16, bf16[640,1024]{1,0:T(8,128)(2,1)} %slice_dynamic-update-slice_fusion), kind=kOutput, calls=%fused_computation.58 | convolution fusion | flops 1342177280 | bytes 6815744 | tf_op jit(solution)/shard_map/dot_general | solution.py:139
  155.9 1.1 multiply_convert_fusion
  157.0 2.2 %shard_map.71 = bf16[1024,2048]{1,0:T(8,128)(2,1)} custom-call(s32[1]{0:T(128)} %bitcast.z_ref, bf16[256,1024]{1,0:T(8,128)(2,1)} %copy-done.3, bf16[256,1024]{1,0:T(8,128)(2,1)} %copy-done.4, bf16[128,1024]{1,0:T(8,128)(2,1)} %collective-permute-done.15.refs_2_, bf16[1024,2048]{1,0:T(8,128)(2,1)} %shard_map.70.refs_3_), custom_call_target="tpu_custom_call", output_to_operand_aliasing={{}: (4, {})} | custom-call | tf_op jit(solution)/shard_map/pallas_call | solution.py:38
  159.3 3.4 %convolution_convert_fusion.1 = bf16[1024,768]{0,1:T(8,128)(2,1)S(1)} fusion(bf16[1024,1024]{1,0:T(8,128)(2,1)S(1)} %multiply_convert_fusion, bf16[1024,2048]{1,0:T(8,128)(2,1)} %shard_map.71), kind=kOutput, calls=%fused_computation.10 | convolution fusion | flops 1611399168 | bytes 5242880 | tf_op jit(solution)/shard_map/dot_general | solution.py:157
  162.9 3.2 %convolution_convert_fusion = bf16[1024,1280]{1,0:T(8,128)(2,1)S(1)} fusion(bf16[1024,1024]{1,0:T(8,128)(2,1)S(1)} %multiply_convert_fusion, bf16[1024,2048]{1,0:T(8,128)(2,1)S(1)} %copy-done), kind=kOutput, calls=%fused_computation.7 | convolution fusion | flops 2685665280 | bytes 7340032 | tf_op jit(solution)/shard_map/dot_general | solution.py:157
  166.2 0.6 collective-permute-start.21
  166.7 0.3 fusion.17
  167.1 0.7 collective-permute-start.17
  167.8 2.7 %collective-permute-start.19 = (bf16[128,384]{0,1:T(8,128)(2,1)S(1)}, bf16[128,384]{0,1:T(8,128)(2,1)S(1)}, u32[]{:S(2)}, u32[]{:S(2)}) collective-permute-start(bf16[128,384]{0,1:T(8,128)(2,1)S(1)} %get-tuple-element.16), channel_id=1, source_target_pairs={{0,6},{1,7},{2,0},{3,1},{4,2},{5,3},{6,4},{7,5},{8,14},{9,15},{10,... | collective-permute-start | bytes 294920 | tf_op jit(solution)/shard_map/ppermute | solution.py:165
  170.5 2.7 %collective-permute-done.17 = bf16[128,384]{0,1:T(8,128)(2,1)S(1)} collective-permute-done((bf16[128,384]{0,1:T(8,128)(2,1)S(1)}, bf16[128,384]{0,1:T(8,128)(2,1)S(1)}, u32[]{:S(2)}, u32[]{:S(2)}) %collective-permute-start.17) | collective-permute-done | bytes 98336 | tf_op jit(solution)/shard_map/ppermute | solution.py:164
  173.4 3.2 %collective-permute-start.20 = (bf16[128,768]{0,1:T(8,128)(2,1)S(1)}, bf16[128,768]{0,1:T(8,128)(2,1)}, u32[]{:S(2)}, u32[]{:S(2)}) collective-permute-start(bf16[128,768]{0,1:T(8,128)(2,1)S(1)} %get-tuple-element.10), channel_id=1, source_target_pairs={{0,6},{1,7},{2,0},{3,1},{4,2},{5,3},{6,4},{7,5},{8,14},{9,15},{10,... | collective-permute-start | bytes 589832 | tf_op jit(solution)/shard_map/ppermute | solution.py:171
  177.1 3.2 %collective-permute-start.24 = (bf16[128,640]{1,0:T(8,128)(2,1)S(1)}, bf16[128,640]{1,0:T(8,128)(2,1)S(1)}, u32[]{:S(2)}, u32[]{:S(2)}) collective-permute-start(bf16[128,640]{1,0:T(8,128)(2,1)S(1)} %get-tuple-element.12), channel_id=1, source_target_pairs={{0,6},{1,7},{2,0},{3,1},{4,2},{5,3},{6,4},{7,5},{8,14},{9,15},{10,... | collective-permute-start | bytes 491528 | tf_op jit(solution)/shard_map/ppermute | solution.py:165
  180.3 0.8 fusion.20
  181.1 3.0 %collective-permute-done.22 = bf16[128,640]{1,0:T(8,128)(2,1)S(1)} collective-permute-done((bf16[128,640]{1,0:T(8,128)(2,1)S(1)}, bf16[128,640]{1,0:T(8,128)(2,1)S(1)}, u32[]{:S(2)}, u32[]{:S(2)}) %collective-permute-start.22) | collective-permute-done | bytes 163872 | tf_op jit(solution)/shard_map/ppermute | solution.py:164
  184.1 0.8 fusion.13
  184.9 0.7 collective-permute-start.23
  185.6 2.5 %collective-permute-start.25 = (bf16[128,1280]{1,0:T(8,128)(2,1)}, bf16[128,1280]{1,0:T(8,128)(2,1)}, u32[]{:S(2)}, u32[]{:S(2)}) collective-permute-start(bf16[128,1280]{1,0:T(8,128)(2,1)} %get-tuple-element.6), channel_id=1, source_target_pairs={{0,6},{1,7},{2,0},{3,1},{4,2},{5,3},{6,4},{7,5},{8,14},{9,15},{10,... | collective-permute-start | bytes 983048 | tf_op jit(solution)/shard_map/ppermute | solution.py:171
  188.1 2.7 %shard_map.68 = bf16[2048,1024]{1,0:T(8,128)(2,1)} custom-call(s32[1]{0:T(128)} %bitcast.z_ref, bf16[256,1024]{1,0:T(8,128)(2,1)} %copy-done.8, bf16[256,1024]{1,0:T(8,128)(2,1)} %copy-done.7, bf16[256,1024]{1,0:T(8,128)(2,1)} %copy-done.3, bf16[256,1024]{1,0:T(8,128)(2,1)} %copy-done.4, ...), custom_call_target="tpu_custom_call", output_to_operand_aliasing={{}: (6, {})} | custom-call | tf_op jit(solution)/shard_map/pallas_call | solution.py:38
  190.8 1.2 fusion.8
  192.2 2.5 %collective-permute-done.23 = bf16[128,1280]{1,0:T(8,128)(2,1)} collective-permute-done((bf16[128,1280]{1,0:T(8,128)(2,1)S(1)}, bf16[128,1280]{1,0:T(8,128)(2,1)}, u32[]{:S(2)}, u32[]{:S(2)}) %collective-permute-start.23) | collective-permute-done | bytes 327712 | tf_op jit(solution)/shard_map/ppermute | solution.py:170
  194.7 1.2 fusion.6
  195.8 0.8 pad_maximum_fusion.2
  (82 shorter events, 2.6 us)
Async XLA Ops:
  19.7 69.1 %copy-start.2 = (bf16[256,1024]{1,0:T(8,128)(2,1)}, bf16[256,1024]{1,0:T(8,128)(2,1)S(1)}, u32[]{:S(2)}) copy-start(bf16[256,1024]{1,0:T(8,128)(2,1)S(1)} %pad_maximum_fusion.1.refs_0_) | copy-start | bytes 1572868
  19.7 33.3 %collective-permute-start.6 = (bf16[256,1024]{1,0:T(8,128)(2,1)S(1)}, bf16[256,1024]{1,0:T(8,128)(2,1)S(1)}, u32[]{:S(2)}, u32[]{:S(2)}) collective-permute-start(bf16[256,1024]{1,0:T(8,128)(2,1)S(1)} %pad_maximum_fusion.1.refs_0_), channel_id=1, source_target_pairs={{0,120},{8,0},{16,8},{24,16},{32,24},{40,32},{48,40},{56,48},{64,5... | collective-permute-start | bytes 1572872 | tf_op jit(solution)/shard_map/ppermute | solution.py:88
  42.2 14.5 %collective-permute-start = (bf16[256,1024]{1,0:T(8,128)(2,1)S(1)}, bf16[256,1024]{1,0:T(8,128)(2,1)S(1)}, u32[]{:S(2)}, u32[]{:S(2)}) collective-permute-start(bf16[256,1024]{1,0:T(8,128)(2,1)S(1)} %pad_maximum_fusion.1.refs_0_), channel_id=1, source_target_pairs={{0,8},{8,16},{16,24},{24,32},{32,40},{40,48},{48,56},{56,64},{64,7... | collective-permute-start | bytes 1572872 | tf_op jit(solution)/shard_map/ppermute | solution.py:87
  53.0 35.8 %copy-start.10 = (bf16[256,1024]{1,0:T(8,128)(2,1)}, bf16[256,1024]{1,0:T(8,128)(2,1)S(1)}, u32[]{:S(2)}) copy-start(bf16[256,1024]{1,0:T(8,128)(2,1)S(1)} %collective-permute-done.6.refs_2_) | copy-start | bytes 1572868
  53.0 13.7 %collective-permute-start.7 = (bf16[256,1024]{1,0:T(8,128)(2,1)S(1)}, bf16[256,1024]{1,0:T(8,128)(2,1)S(1)}, u32[]{:S(2)}, u32[]{:S(2)}) collective-permute-start(bf16[256,1024]{1,0:T(8,128)(2,1)S(1)} %collective-permute-done.6.refs_2_), channel_id=1, source_target_pairs={{0,120},{8,0},{16,8},{24,16},{32,24},{40,32},{48,40},{56,48},{64,5... | collective-permute-start | bytes 1572872 | tf_op jit(solution)/shard_map/ppermute | solution.py:88
  56.7 32.1 %copy-start.11 = (bf16[256,1024]{1,0:T(8,128)(2,1)}, bf16[256,1024]{1,0:T(8,128)(2,1)S(1)}, u32[]{:S(2)}) copy-start(bf16[256,1024]{1,0:T(8,128)(2,1)S(1)} %collective-permute-done.refs_1_) | copy-start | bytes 1572868
  56.7 13.7 %collective-permute-start.1 = (bf16[256,1024]{1,0:T(8,128)(2,1)S(1)}, bf16[256,1024]{1,0:T(8,128)(2,1)S(1)}, u32[]{:S(2)}, u32[]{:S(2)}) collective-permute-start(bf16[256,1024]{1,0:T(8,128)(2,1)S(1)} %collective-permute-done.refs_1_), channel_id=1, source_target_pairs={{0,8},{8,16},{16,24},{24,32},{32,40},{40,48},{48,56},{56,64},{64,7... | collective-permute-start | bytes 1572872 | tf_op jit(solution)/shard_map/ppermute | solution.py:87
  66.7 31.6 %copy-start.12 = (bf16[256,1024]{1,0:T(8,128)(2,1)}, bf16[256,1024]{1,0:T(8,128)(2,1)S(1)}, u32[]{:S(2)}) copy-start(bf16[256,1024]{1,0:T(8,128)(2,1)S(1)} %collective-permute-done.7.refs_4_) | copy-start | bytes 1572868
  66.7 12.8 %collective-permute-start.8 = (bf16[256,1024]{1,0:T(8,128)(2,1)S(1)}, bf16[256,1024]{1,0:T(8,128)(2,1)S(1)}, u32[]{:S(2)}, u32[]{:S(2)}) collective-permute-start(bf16[256,1024]{1,0:T(8,128)(2,1)S(1)} %collective-permute-done.7.refs_4_), channel_id=1, source_target_pairs={{0,120},{8,0},{16,8},{24,16},{32,24},{40,32},{48,40},{56,48},{64,5... | collective-permute-start | bytes 1572872 | tf_op jit(solution)/shard_map/ppermute | solution.py:88
  70.4 27.9 %copy-start.13 = (bf16[256,1024]{1,0:T(8,128)(2,1)}, bf16[256,1024]{1,0:T(8,128)(2,1)S(1)}, u32[]{:S(2)}) copy-start(bf16[256,1024]{1,0:T(8,128)(2,1)S(1)} %collective-permute-done.1.refs_3_) | copy-start | bytes 1572868
  70.4 12.8 %collective-permute-start.2 = (bf16[256,1024]{1,0:T(8,128)(2,1)S(1)}, bf16[256,1024]{1,0:T(8,128)(2,1)}, u32[]{:S(2)}, u32[]{:S(2)}) collective-permute-start(bf16[256,1024]{1,0:T(8,128)(2,1)S(1)} %collective-permute-done.1.refs_3_), channel_id=1, source_target_pairs={{0,8},{8,16},{16,24},{24,32},{32,40},{40,48},{48,56},{56,64},{64,7... | collective-permute-start | bytes 1572872 | tf_op jit(solution)/shard_map/ppermute | solution.py:87
  79.5 28.0 %copy-start.14 = (bf16[256,1024]{1,0:T(8,128)(2,1)}, bf16[256,1024]{1,0:T(8,128)(2,1)S(1)}, u32[]{:S(2)}) copy-start(bf16[256,1024]{1,0:T(8,128)(2,1)S(1)} %collective-permute-done.8.refs_6_) | copy-start | bytes 1572868
  79.5 11.9 %collective-permute-start.9 = (bf16[256,1024]{1,0:T(8,128)(2,1)S(1)}, bf16[256,1024]{1,0:T(8,128)(2,1)}, u32[]{:S(2)}, u32[]{:S(2)}) collective-permute-start(bf16[256,1024]{1,0:T(8,128)(2,1)S(1)} %collective-permute-done.8.refs_6_), channel_id=1, source_target_pairs={{0,120},{8,0},{16,8},{24,16},{32,24},{40,32},{48,40},{56,48},{64,5... | collective-permute-start | bytes 1572872 | tf_op jit(solution)/shard_map/ppermute | solution.py:88
  83.2 12.0 %collective-permute-start.3 = (bf16[256,1024]{1,0:T(8,128)(2,1)}, bf16[256,1024]{1,0:T(8,128)(2,1)}, u32[]{:S(2)}, u32[]{:S(2)}) collective-permute-start(bf16[256,1024]{1,0:T(8,128)(2,1)} %collective-permute-done.2.refs_5_), channel_id=1, source_target_pairs={{0,8},{8,16},{16,24},{24,32},{32,40},{40,48},{48,56},{56,64},{64,7... | collective-permute-start | bytes 1572872 | tf_op jit(solution)/shard_map/ppermute | solution.py:87
  91.4 12.5 %collective-permute-start.10 = (bf16[256,1024]{1,0:T(8,128)(2,1)}, bf16[256,1024]{1,0:T(8,128)(2,1)S(1)}, u32[]{:S(2)}, u32[]{:S(2)}) collective-permute-start(bf16[256,1024]{1,0:T(8,128)(2,1)} %collective-permute-done.9.refs_8_), channel_id=1, source_target_pairs={{0,120},{8,0},{16,8},{24,16},{32,24},{40,32},{48,40},{56,48},{64,5... | collective-permute-start | bytes 1572872 | tf_op jit(solution)/shard_map/ppermute | solution.py:88
  95.2 12.3 %collective-permute-start.4 = (bf16[256,1024]{1,0:T(8,128)(2,1)}, bf16[256,1024]{1,0:T(8,128)(2,1)}, u32[]{:S(2)}, u32[]{:S(2)}) collective-permute-start(bf16[256,1024]{1,0:T(8,128)(2,1)} %collective-permute-done.3.refs_7_), channel_id=1, source_target_pairs={{0,8},{8,16},{16,24},{24,32},{32,40},{40,48},{48,56},{56,64},{64,7... | collective-permute-start | bytes 1572872 | tf_op jit(solution)/shard_map/ppermute | solution.py:87
  103.9 6.5 %copy-start.15 = (bf16[256,1024]{1,0:T(8,128)(2,1)}, bf16[256,1024]{1,0:T(8,128)(2,1)S(1)}, u32[]{:S(2)}) copy-start(bf16[256,1024]{1,0:T(8,128)(2,1)S(1)} %collective-permute-done.10.refs_10_.refs_1_) | copy-start | bytes 1572868
  103.9 20.9 %collective-permute-start.11 = (bf16[256,1024]{1,0:T(8,128)(2,1)S(1)}, bf16[256,1024]{1,0:T(8,128)(2,1)S(1)}, u32[]{:S(2)}, u32[]{:S(2)}) collective-permute-start(bf16[256,1024]{1,0:T(8,128)(2,1)S(1)} %collective-permute-done.10.refs_10_.refs_1_), channel_id=1, source_target_pairs={{0,120},{8,0},{16,8},{24,16},{32,24},{40,32},{48,40},{56,48},{64,5... | collective-permute-start | bytes 1572872 | tf_op jit(solution)/shard_map/ppermute | solution.py:88
  107.5 20.7 %collective-permute-start.5 = (bf16[256,1024]{1,0:T(8,128)(2,1)}, bf16[256,1024]{1,0:T(8,128)(2,1)S(1)}, u32[]{:S(2)}, u32[]{:S(2)}) collective-permute-start(bf16[256,1024]{1,0:T(8,128)(2,1)} %collective-permute-done.4.refs_9_.refs_0_), channel_id=1, source_target_pairs={{0,8},{8,16},{16,24},{24,32},{32,40},{40,48},{48,56},{56,64},{64,7... | collective-permute-start | bytes 1572872 | tf_op jit(solution)/shard_map/ppermute | solution.py:87
  110.5 2.0 %copy-start.1 = (bf16[1024,2048]{1,0:T(8,128)(2,1)}, bf16[1024,2048]{1,0:T(8,128)(2,1)S(1)}, u32[]{:S(2)}) copy-start(bf16[1024,2048]{1,0:T(8,128)(2,1)S(1)} %fusion.1) | copy-start | bytes 12582916
  124.8 16.7 %copy-start.7 = (bf16[256,1024]{1,0:T(8,128)(2,1)}, bf16[256,1024]{1,0:T(8,128)(2,1)S(1)}, u32[]{:S(2)}) copy-start(bf16[256,1024]{1,0:T(8,128)(2,1)S(1)} %collective-permute-done.11.refs_1_.refs_3_) | copy-start | bytes 1572868
  124.9 20.1 %collective-permute-start.13 = (bf16[256,1024]{1,0:T(8,128)(2,1)S(1)}, bf16[256,1024]{1,0:T(8,128)(2,1)S(1)}, u32[]{:S(2)}, u32[]{:S(2)}) collective-permute-start(bf16[256,1024]{1,0:T(8,128)(2,1)S(1)} %collective-permute-done.11.refs_1_.refs_3_), channel_id=1, source_target_pairs={{0,120},{8,0},{16,8},{24,16},{32,24},{40,32},{48,40},{56,48},{64,5... | collective-permute-start | bytes 1572872 | tf_op jit(solution)/shard_map/ppermute | solution.py:88
  128.2 10.1 %copy-start.8 = (bf16[256,1024]{1,0:T(8,128)(2,1)}, bf16[256,1024]{1,0:T(8,128)(2,1)S(1)}, u32[]{:S(2)}) copy-start(bf16[256,1024]{1,0:T(8,128)(2,1)S(1)} %collective-permute-done.5.refs_0_.refs_2_) | copy-start | bytes 1572868
  128.2 12.6 %collective-permute-start.12 = (bf16[256,1024]{1,0:T(8,128)(2,1)S(1)}, bf16[256,1024]{1,0:T(8,128)(2,1)S(1)}, u32[]{:S(2)}, u32[]{:S(2)}) collective-permute-start(bf16[256,1024]{1,0:T(8,128)(2,1)S(1)} %collective-permute-done.5.refs_0_.refs_2_), channel_id=1, source_target_pairs={{0,8},{8,16},{16,24},{24,32},{32,40},{40,48},{48,56},{56,64},{64,7... | collective-permute-start | bytes 1572872 | tf_op jit(solution)/shard_map/ppermute | solution.py:87
  140.8 10.4 %copy-start.3 = (bf16[256,1024]{1,0:T(8,128)(2,1)}, bf16[256,1024]{1,0:T(8,128)(2,1)S(1)}, u32[]{:S(2)}) copy-start(bf16[256,1024]{1,0:T(8,128)(2,1)S(1)} %collective-permute-done.12.refs_2_.refs_0_) | copy-start | bytes 1572868
  141.5 7.9 %collective-permute-start.14 = (bf16[128,1024]{1,0:T(8,128)(2,1)}, bf16[128,1024]{1,0:T(8,128)(2,1)}, u32[]{:S(2)}, u32[]{:S(2)}) collective-permute-start(bf16[128,1024]{1,0:T(8,128)(2,1)} %slice.131), channel_id=1, source_target_pairs={{0,8},{8,16},{16,24},{24,32},{32,40},{40,48},{48,56},{56,64},{64,7... | collective-permute-start | bytes 786440 | tf_op jit(solution)/shard_map/ppermute | solution.py:89
  142.3 9.6 %copy-start.9 = (bf16[256,1024]{1,0:T(8,128)(2,1)S(1)}, bf16[256,1024]{1,0:T(8,128)(2,1)}, u32[]{:S(2)}) copy-start(bf16[256,1024]{1,0:T(8,128)(2,1)} %copy-done.8) | copy-start | bytes 1572868
  142.3 10.3 %copy-start.16 = (bf16[1024,640]{1,0:T(8,128)(2,1)S(1)}, bf16[1024,640]{1,0:T(8,128)(2,1)}, u32[]{:S(2)}) copy-start(bf16[1024,640]{1,0:T(8,128)(2,1)} %fusion.4) | copy-start | bytes 3932164
  145.0 10.9 %copy-start.4 = (bf16[256,1024]{1,0:T(8,128)(2,1)}, bf16[256,1024]{1,0:T(8,128)(2,1)S(1)}, u32[]{:S(2)}) copy-start(bf16[256,1024]{1,0:T(8,128)(2,1)S(1)} %collective-permute-done.13.refs_3_.refs_1_) | copy-start | bytes 1572868
  145.8 11.2 %collective-permute-start.15 = (bf16[128,1024]{1,0:T(8,128)(2,1)S(1)}, bf16[128,1024]{1,0:T(8,128)(2,1)}, u32[]{:S(2)}, u32[]{:S(2)}) collective-permute-start(bf16[128,1024]{1,0:T(8,128)(2,1)S(1)} %get-tuple-element.20), channel_id=1, source_target_pairs={{0,120},{8,0},{16,8},{24,16},{32,24},{40,32},{48,40},{56,48},{64,5... | collective-permute-start | bytes 786440 | tf_op jit(solution)/shard_map/ppermute | solution.py:90
  152.6 3.3 %copy-start.5 = (f32[1024,1024]{1,0:T(8,128)S(1)}, f32[1024,1024]{1,0:T(8,128)}, u32[]{:S(2)}) copy-start(f32[1024,1024]{1,0:T(8,128)} %fusion.24) | copy-start | bytes 12582916
  159.2 3.6 %copy-start = (bf16[1024,2048]{1,0:T(8,128)(2,1)S(1)}, bf16[1024,2048]{1,0:T(8,128)(2,1)}, u32[]{:S(2)}) copy-start(bf16[1024,2048]{1,0:T(8,128)(2,1)} %shard_map.71) | copy-start | bytes 12582916
  162.7 4.0 %collective-permute-start.16 = (bf16[512,768]{0,1:T(8,128)(2,1)S(1)}, bf16[512,768]{0,1:T(8,128)(2,1)S(1)}, u32[]{:S(2)}, u32[]{:S(2)}) collective-permute-start(bf16[512,768]{0,1:T(8,128)(2,1)S(1)} %slice.139), channel_id=1, source_target_pairs={{0,1},{1,0},{2,3},{3,2},{4,5},{5,4},{6,7},{7,6},{8,9},{9,8},{10,11... | collective-permute-start | bytes 2359304 | tf_op jit(solution)/shard_map/ppermute | solution.py:158
  166.2 10.5 %collective-permute-start.21 = (bf16[512,1280]{1,0:T(8,128)(2,1)S(1)}, bf16[512,1280]{1,0:T(8,128)(2,1)S(1)}, u32[]{:S(2)}, u32[]{:S(2)}) collective-permute-start(bf16[512,1280]{1,0:T(8,128)(2,1)S(1)} %slice.149), channel_id=1, source_target_pairs={{0,1},{1,0},{2,3},{3,2},{4,5},{5,4},{6,7},{7,6},{8,9},{9,8},{10,11... | collective-permute-start | bytes 3932168 | tf_op jit(solution)/shard_map/ppermute | solution.py:158
  167.1 9.5 %copy-start.6 = (f32[512,768]{0,1:T(8,128)}, f32[512,768]{0,1:T(8,128)S(1)}, u32[]{:S(2)}) copy-start(f32[512,768]{0,1:T(8,128)S(1)} %get-tuple-element.8) | copy-start | bytes 4718596
  167.1 6.1 %collective-permute-start.17 = (bf16[128,384]{0,1:T(8,128)(2,1)S(1)}, bf16[128,384]{0,1:T(8,128)(2,1)S(1)}, u32[]{:S(2)}, u32[]{:S(2)}) collective-permute-start(bf16[128,384]{0,1:T(8,128)(2,1)S(1)} %get-tuple-element.15), channel_id=1, source_target_pairs={{0,2},{1,3},{2,4},{3,5},{4,6},{5,7},{6,0},{7,1},{8,10},{9,11},{10,... | collective-permute-start | bytes 294920 | tf_op jit(solution)/shard_map/ppermute | solution.py:164
  167.8 5.4 %collective-permute-start.19 = (bf16[128,384]{0,1:T(8,128)(2,1)S(1)}, bf16[128,384]{0,1:T(8,128)(2,1)S(1)}, u32[]{:S(2)}, u32[]{:S(2)}) collective-permute-start(bf16[128,384]{0,1:T(8,128)(2,1)S(1)} %get-tuple-element.16), channel_id=1, source_target_pairs={{0,6},{1,7},{2,0},{3,1},{4,2},{5,3},{6,4},{7,5},{8,14},{9,15},{10,... | collective-permute-start | bytes 294920 | tf_op jit(solution)/shard_map/ppermute | solution.py:165
  173.3 17.5 %collective-permute-start.18 = (bf16[128,768]{0,1:T(8,128)(2,1)S(1)}, bf16[128,768]{0,1:T(8,128)(2,1)}, u32[]{:S(2)}, u32[]{:S(2)}) collective-permute-start(bf16[128,768]{0,1:T(8,128)(2,1)S(1)} %get-tuple-element.9), channel_id=1, source_target_pairs={{0,2},{1,3},{2,4},{3,5},{4,6},{5,7},{6,0},{7,1},{8,10},{9,11},{10,... | collective-permute-start | bytes 589832 | tf_op jit(solution)/shard_map/ppermute | solution.py:170
  173.4 17.4 %collective-permute-start.20 = (bf16[128,768]{0,1:T(8,128)(2,1)S(1)}, bf16[128,768]{0,1:T(8,128)(2,1)}, u32[]{:S(2)}, u32[]{:S(2)}) collective-permute-start(bf16[128,768]{0,1:T(8,128)(2,1)S(1)} %get-tuple-element.10), channel_id=1, source_target_pairs={{0,6},{1,7},{2,0},{3,1},{4,2},{5,3},{6,4},{7,5},{8,14},{9,15},{10,... | collective-permute-start | bytes 589832 | tf_op jit(solution)/shard_map/ppermute | solution.py:171
  177.0 7.1 %collective-permute-start.22 = (bf16[128,640]{1,0:T(8,128)(2,1)S(1)}, bf16[128,640]{1,0:T(8,128)(2,1)S(1)}, u32[]{:S(2)}, u32[]{:S(2)}) collective-permute-start(bf16[128,640]{1,0:T(8,128)(2,1)S(1)} %get-tuple-element.11), channel_id=1, source_target_pairs={{0,2},{1,3},{2,4},{3,5},{4,6},{5,7},{6,0},{7,1},{8,10},{9,11},{10,... | collective-permute-start | bytes 491528 | tf_op jit(solution)/shard_map/ppermute | solution.py:164
  177.1 7.0 %collective-permute-start.24 = (bf16[128,640]{1,0:T(8,128)(2,1)S(1)}, bf16[128,640]{1,0:T(8,128)(2,1)S(1)}, u32[]{:S(2)}, u32[]{:S(2)}) collective-permute-start(bf16[128,640]{1,0:T(8,128)(2,1)S(1)} %get-tuple-element.12), channel_id=1, source_target_pairs={{0,6},{1,7},{2,0},{3,1},{4,2},{5,3},{6,4},{7,5},{8,14},{9,15},{10,... | collective-permute-start | bytes 491528 | tf_op jit(solution)/shard_map/ppermute | solution.py:165
  184.9 9.8 %collective-permute-start.23 = (bf16[128,1280]{1,0:T(8,128)(2,1)S(1)}, bf16[128,1280]{1,0:T(8,128)(2,1)}, u32[]{:S(2)}, u32[]{:S(2)}) collective-permute-start(bf16[128,1280]{1,0:T(8,128)(2,1)S(1)} %get-tuple-element.5), channel_id=1, source_target_pairs={{0,2},{1,3},{2,4},{3,5},{4,6},{5,7},{6,0},{7,1},{8,10},{9,11},{10,... | collective-permute-start | bytes 983048 | tf_op jit(solution)/shard_map/ppermute | solution.py:170
  185.6 9.1 %collective-permute-start.25 = (bf16[128,1280]{1,0:T(8,128)(2,1)}, bf16[128,1280]{1,0:T(8,128)(2,1)}, u32[]{:S(2)}, u32[]{:S(2)}) collective-permute-start(bf16[128,1280]{1,0:T(8,128)(2,1)} %get-tuple-element.6), channel_id=1, source_target_pairs={{0,6},{1,7},{2,0},{3,1},{4,2},{5,3},{6,4},{7,5},{8,14},{9,15},{10,... | collective-permute-start | bytes 983048 | tf_op jit(solution)/shard_map/ppermute | solution.py:171

commit v4 on v3

--- a/solution.py
+++ b/solution.py
@@ -110,7 +110,7 @@
     moves += [(blank, 0, up_rows, 0, k, up_rows, 0, 0) for k in late]
     up_sampler = place(z, moves, up_shape, n_fs)
     down_sampler = place(z, down_moves(within(0, half - 4)), down_shape, n_fs)
-    moves = down_moves(within(half - 3, half - 2))
+    moves = down_moves(within(half - 3, half - 3))
     down_sampler = place(z, moves, down_shape, n_fs, down_sampler)
 
     tokens = prompt_rows.shape[0]
@@ -128,8 +128,12 @@
     pre_act = jnp.dot(normed, up_sampler[0], preferred_element_type=jnp.float32)
     pre_act = lax.optimization_barrier(pre_act)
 
-    rest = [up_far if k == half else held[k if k < half else k - n_fs][:up_rows] for k in late]
-    rest = jnp.concatenate(rest, axis=0)
+    rest = jnp.zeros((len(late) * up_rows, width), jnp.bfloat16)
+    for k in sorted(late, key=lambda k: k == half):
+        band = up_far if k == half else held[k if k < half else k - n_fs][:up_rows]
+        rest = lax.dynamic_update_slice(rest, band, ((k - late[0]) * up_rows, 0))
+        if k != half:
+            rest = lax.optimization_barrier(rest)
     ends = (len(late) - 1) * up_rows
     features = jnp.concatenate([normed, normed[:, :ends]], axis=1)
     features = lax.dynamic_slice_in_dim(
@@ -140,7 +144,7 @@
     pre_act = pre_act + lax.optimization_barrier(added)
     hidden = jnp.square(jax.nn.relu(pre_act)).astype(jnp.bfloat16)
 
-    moves = down_moves(within(half - 1, half - 1))
+    moves = down_moves(within(half - 2, half - 1))
     moves += [(down_far, k * span, span, 0, half, span, 0, k * width) for k in range(sides)]
     down_sampler = place(z, moves, down_shape, n_fs, down_sampler)[0]
     moves = up_moves(within(half - 2, half - 1))
@@ -171,6 +175,8 @@
         before = lax.ppermute(before, "tp", left).astype(jnp.float32)
         total = (total + after + before).astype(jnp.bfloat16)
         summed = lax.dynamic_update_slice(summed, total, (0, lo))
+        if hi < full:
+            summed = lax.optimization_barrier(summed)
     return (up_sampler[None], down_sampler[None], summed)
 
 

time: 198 us -> 205 us (1.035)
  waiting for transfers between devices: 39.3 us -> 45.4 us
    ppermute x7, waiting for transfers between devices: 28.3 us -> 36.8 us  [on_device(): held[step] = lax.ppermute(held[step - 1], 'fs', back)]
    unnamed x47, local copies, waits for them, and re-layouts: 20.9 us -> 16.4 us
    dynamic_update_slice x0 -> x6, local copies, waits for them, and re-layouts: none -> 4.48 us  [the longest x5 4.43 us: on_device(): rest = lax.dynamic_update_slice(rest, band, ((k - late[0]) * up_rows, 0))]
    ppermute x7, waiting for transfers between devices: 2.5 us -> 0.19 us  [on_device(): held[-step] = lax.ppermute(held[1 - step], 'fs', fore)]
    convert_element_type x1, other arithmetic: 2.93 us -> 5.1 us  [on_device(): normed = lax.optimization_barrier((values * scale).astype(jnp.bfloat16))]
where the time goes in v4:
time: 205 us; the launch traced here: 204 us
  starting transfers between devices  62.1 us (30%)
  waiting for transfers between devices  45.4 us (22%)
  local copies, waits for them, and re-layouts  26.7 us (13%)
  matrix products  19.7 us (10%)
  other arithmetic  17.7 us (9%)
  Pallas kernels  16.2 us (8%)
  blocking collectives  14.7 us (7%)
    ppermute x7, starting transfers between devices, on_device(): held[step] = lax.ppermute(held[step - 1], 'fs', back)  44.6 us
    ppermute x7, waiting for transfers between devices, on_device(): held[step] = lax.ppermute(held[step - 1], 'fs', back)  36.8 us
    unnamed x47, local copies, waits for them, and re-layouts  16.4 us
    pallas_call x5, Pallas kernels, place(): pl.pallas_call(body, out_shape=outs, in_specs=[pl.BlockSpec(memory_space=...  16.2 us
    all_to_all x1, blocking collectives, on_device(): parts = lax.all_to_all(parts, 'tp', split_axis=0, concat_axis=0, tiled=True)  14.7 us
    dot_general x1, matrix products, on_device(): pre_act = jnp.dot(normed, up_sampler[0], preferred_element_type=jnp.float32)  9.97 us
    dot_general x2, matrix products, on_device(): jnp.dot(hidden, weights, preferred_element_type=jnp.float32)  6.5 us
    ppermute x2, starting transfers between devices, on_device(): second = lax.ppermute(ends[1], 'tp', left).astype(jnp.float32)  5.88 us
  transfers between devices with their start and end apart: 26, of which 10 were waited for; matrix products, arithmetic and copies ran while one was open for 26% of the time, Pallas kernels for 7%

profile of v4, /device:TPU:40, one launch (start us, length us, event | category | flops | bytes accessed | tf_op | source)
XLA Modules:
  0.0 203.7 jit_solution(10476640623493733337)
XLA Ops:
  0.6 1.1 convert_element_type.82
  2.0 1.2 copy.31
  3.3 0.7 multiply_convert_fusion.1
  4.1 14.7 %all_to_all.5 = bf16[8,2,128,128]{2,3,1,0:T(8,128)(2,1)S(1)} all-to-all(bf16[8,2,128,128]{2,3,1,0:T(8,128)(2,1)S(1)} %copy.35), channel_id=1, replica_groups=mesh['grp'=2,'fs'=16,'tp'=8] {'tp'}, dimensions={0} | all-to-all | bytes 1048576 | tf_op jit(solution)/shard_map/all_to_all | solution.py:76
  19.2 0.3 copy.38
  19.7 22.5 %collective-permute-start.6 = (bf16[256,1024]{1,0:T(8,128)(2,1)S(1)}, bf16[256,1024]{1,0:T(8,128)(2,1)S(1)}, u32[]{:S(2)}, u32[]{:S(2)}) collective-permute-start(bf16[256,1024]{1,0:T(8,128)(2,1)S(1)} %pad_maximum_fusion.1.refs_0_), channel_id=1, source_target_pairs={{0,120},{8,0},{16,8},{24,16},{32,24},{40,32},{48,40},{56,48},{64,5... | collective-permute-start | bytes 1572872 | tf_op jit(solution)/shard_map/ppermute | solution.py:88
  42.2 10.8 %collective-permute-done.6.refs_2_ = bf16[256,1024]{1,0:T(8,128)(2,1)S(1)} collective-permute-done((bf16[256,1024]{1,0:T(8,128)(2,1)S(1)}, bf16[256,1024]{1,0:T(8,128)(2,1)S(1)}, u32[]{:S(2)}, u32[]{:S(2)}) %collective-permute-start.6) | collective-permute-done | bytes 524320 | tf_op jit(solution)/shard_map/ppermute | solution.py:88
  53.0 3.7 %collective-permute-start.7 = (bf16[256,1024]{1,0:T(8,128)(2,1)S(1)}, bf16[256,1024]{1,0:T(8,128)(2,1)S(1)}, u32[]{:S(2)}, u32[]{:S(2)}) collective-permute-start(bf16[256,1024]{1,0:T(8,128)(2,1)S(1)} %collective-permute-done.6.refs_2_), channel_id=1, source_target_pairs={{0,120},{8,0},{16,8},{24,16},{32,24},{40,32},{48,40},{56,48},{64,5... | collective-permute-start | bytes 1572872 | tf_op jit(solution)/shard_map/ppermute | solution.py:88
  56.8 9.8 %collective-permute-done.7.refs_4_ = bf16[256,1024]{1,0:T(8,128)(2,1)S(1)} collective-permute-done((bf16[256,1024]{1,0:T(8,128)(2,1)S(1)}, bf16[256,1024]{1,0:T(8,128)(2,1)S(1)}, u32[]{:S(2)}, u32[]{:S(2)}) %collective-permute-start.7) | collective-permute-done | bytes 524320 | tf_op jit(solution)/shard_map/ppermute | solution.py:88
  66.7 3.7 %collective-permute-start.8 = (bf16[256,1024]{1,0:T(8,128)(2,1)S(1)}, bf16[256,1024]{1,0:T(8,128)(2,1)S(1)}, u32[]{:S(2)}, u32[]{:S(2)}) collective-permute-start(bf16[256,1024]{1,0:T(8,128)(2,1)S(1)} %collective-permute-done.7.refs_4_), channel_id=1, source_target_pairs={{0,120},{8,0},{16,8},{24,16},{32,24},{40,32},{48,40},{56,48},{64,5... | collective-permute-start | bytes 1572872 | tf_op jit(solution)/shard_map/ppermute | solution.py:88
  70.5 2.0 dynamic-slice_dynamic-update-slice_fusion.7
  72.4 1.9 dynamic-slice_dynamic-update-slice_fusion.6
  74.3 5.1 %collective-permute-done.8.refs_6_ = bf16[256,1024]{1,0:T(8,128)(2,1)S(1)} collective-permute-done((bf16[256,1024]{1,0:T(8,128)(2,1)S(1)}, bf16[256,1024]{1,0:T(8,128)(2,1)S(1)}, u32[]{:S(2)}, u32[]{:S(2)}) %collective-permute-start.8) | collective-permute-done | bytes 524320 | tf_op jit(solution)/shard_map/ppermute | solution.py:88
  79.5 3.7 %collective-permute-start.9 = (bf16[256,1024]{1,0:T(8,128)(2,1)S(1)}, bf16[256,1024]{1,0:T(8,128)(2,1)S(1)}, u32[]{:S(2)}, u32[]{:S(2)}) collective-permute-start(bf16[256,1024]{1,0:T(8,128)(2,1)S(1)} %collective-permute-done.8.refs_6_), channel_id=1, source_target_pairs={{0,120},{8,0},{16,8},{24,16},{32,24},{40,32},{48,40},{56,48},{64,5... | collective-permute-start | bytes 1572872 | tf_op jit(solution)/shard_map/ppermute | solution.py:88
  83.2 2.1 %dynamic-slice_dynamic-update-slice_fusion.5 = bf16[1024,2048]{1,0:T(8,128)(2,1)} fusion(bf16[1024,2048]{1,0:T(8,128)(2,1)} %dynamic-slice_dynamic-update-slice_fusion.6, bf16[1024,2048]{1,0:T(8,128)(2,1)} %param.4, s32[]{:T(128)S(6)} %select_n.94), kind=kLoop, calls=%fused_computation.24 | loop fusion | bytes 1048580
  85.2 1.9 dynamic-slice_dynamic-update-slice_fusion.4
  87.1 1.9 dynamic-slice_dynamic-update-slice_fusion.3
  89.0 2.5 %collective-permute-done.9.refs_8_ = bf16[256,1024]{1,0:T(8,128)(2,1)S(1)} collective-permute-done((bf16[256,1024]{1,0:T(8,128)(2,1)S(1)}, bf16[256,1024]{1,0:T(8,128)(2,1)S(1)}, u32[]{:S(2)}, u32[]{:S(2)}) %collective-permute-start.9) | collective-permute-done | bytes 524320 | tf_op jit(solution)/shard_map/ppermute | solution.py:88
  91.6 3.7 %collective-permute-start.10 = (bf16[256,1024]{1,0:T(8,128)(2,1)S(1)}, bf16[256,1024]{1,0:T(8,128)(2,1)}, u32[]{:S(2)}, u32[]{:S(2)}) collective-permute-start(bf16[256,1024]{1,0:T(8,128)(2,1)S(1)} %collective-permute-done.9.refs_8_), channel_id=1, source_target_pairs={{0,120},{8,0},{16,8},{24,16},{32,24},{40,32},{48,40},{56,48},{64,5... | collective-permute-start | bytes 1572872 | tf_op jit(solution)/shard_map/ppermute | solution.py:88
  95.3 1.9 dynamic-slice_dynamic-update-slice_fusion.2
  97.1 1.9 dynamic-slice_dynamic-update-slice_fusion.1
  99.0 1.9 dynamic-slice_dynamic-update-slice_fusion
  100.9 2.4 %collective-permute-done.10.refs_10_.refs_1_ = bf16[256,1024]{1,0:T(8,128)(2,1)} collective-permute-done((bf16[256,1024]{1,0:T(8,128)(2,1)S(1)}, bf16[256,1024]{1,0:T(8,128)(2,1)}, u32[]{:S(2)}, u32[]{:S(2)}) %collective-permute-start.10) | collective-permute-done | bytes 524320 | tf_op jit(solution)/shard_map/ppermute | solution.py:88
  103.3 3.8 %collective-permute-start.11 = (bf16[256,1024]{1,0:T(8,128)(2,1)}, bf16[256,1024]{1,0:T(8,128)(2,1)S(1)}, u32[]{:S(2)}, u32[]{:S(2)}) collective-permute-start(bf16[256,1024]{1,0:T(8,128)(2,1)} %collective-permute-done.10.refs_10_.refs_1_), channel_id=1, source_target_pairs={{0,120},{8,0},{16,8},{24,16},{32,24},{40,32},{48,40},{56,48},{64,5... | collective-permute-start | bytes 1572872 | tf_op jit(solution)/shard_map/ppermute | solution.py:88
  107.2 3.1 %fusion = f32[1024]{0:T(1024)S(1)} fusion(bf16[1024,2048]{1,0:T(8,128)(2,1)} %dynamic-slice_dynamic-update-slice_fusion), kind=kLoop, calls=%fused_computation.2 | loop fusion | flops 6290432 | bytes 4198400 | tf_op jit(solution)/shard_map/reduce_sum | solution.py:126
  110.2 6.0 %collective-permute-done.11.refs_1_ = bf16[256,1024]{1,0:T(8,128)(2,1)S(1)} collective-permute-done((bf16[256,1024]{1,0:T(8,128)(2,1)}, bf16[256,1024]{1,0:T(8,128)(2,1)S(1)}, u32[]{:S(2)}, u32[]{:S(2)}) %collective-permute-start.11) | collective-permute-done | bytes 524320 | tf_op jit(solution)/shard_map/ppermute | solution.py:88
  116.3 3.6 %collective-permute-start.13 = (bf16[256,1024]{1,0:T(8,128)(2,1)S(1)}, bf16[256,1024]{1,0:T(8,128)(2,1)S(1)}, u32[]{:S(2)}, u32[]{:S(2)}) collective-permute-start(bf16[256,1024]{1,0:T(8,128)(2,1)S(1)} %collective-permute-done.11.refs_1_), channel_id=1, source_target_pairs={{0,120},{8,0},{16,8},{24,16},{32,24},{40,32},{48,40},{56,48},{64,5... | collective-permute-start | bytes 1572872 | tf_op jit(solution)/shard_map/ppermute | solution.py:88
  120.1 5.1 %fusion.1 = bf16[1024,2048]{1,0:T(8,128)(2,1)} fusion(bf16[1024,2048]{1,0:T(8,128)(2,1)} %dynamic-slice_dynamic-update-slice_fusion, f32[1024]{0:T(1024)S(1)} %add_rsqrt_fusion), kind=kLoop, calls=%fused_computation.3 | loop fusion | flops 6291456 | bytes 8392704 | tf_op jit(solution)/shard_map/convert_element_type | solution.py:127
  125.2 1.3 slice.133
  126.5 2.8 %fusion.4 = bf16[1024,640]{1,0:T(8,128)(2,1)} fusion(s32[]{:T(128)S(6)} %select_n.103, bf16[1024,2048]{1,0:T(8,128)(2,1)} %fusion.1, bf16[1024,512]{1,0:T(8,128)(2,1)S(1)} %slice.133), kind=kLoop, calls=%fused_computation.13 | loop fusion | flops 2621440 | bytes 6553604 | tf_op jit(solution)/shard_map/concatenate | solution.py:138
  129.3 3.8 %shard_map.69.refs_2_ = bf16[1024,2048]{1,0:T(8,128)(2,1)} custom-call(s32[1]{0:T(128)} %bitcast.z_ref, bf16[256,1024]{1,0:T(8,128)(2,1)} %copy-done.1, bf16[256,1024]{1,0:T(8,128)(2,1)} %copy-done.9, bf16[256,1024]{1,0:T(8,128)(2,1)} %copy-done.8, bf16[256,1024]{1,0:T(8,128)(2,1)} %copy-done.11, bf16[256,1024]{1,0:T(8,128)(2,1)} %copy-done.10, ...), custom_call_target="tpu_custom_call" | custom-call | tf_op jit(solution)/shard_map/pallas_call | solution.py:38
  133.1 0.7 broadcast_in_dim.6.refs_11_
  133.9 4.8 %shard_map.67.refs_5_ = bf16[2048,1024]{1,0:T(8,128)(2,1)} custom-call(s32[1]{0:T(128)} %bitcast.z_ref, bf16[256,1024]{1,0:T(8,128)(2,1)} %copy-done.1, bf16[256,1024]{1,0:T(8,128)(2,1)} %copy-done.9, bf16[256,1024]{1,0:T(8,128)(2,1)} %copy-done.8, bf16[256,1024]{1,0:T(8,128)(2,1)} %copy-done.11, bf16[256,1024]{1,0:T(8,128)(2,1)} %copy-done.10, ...), custom_call_target="tpu_custom_call" | custom-call | tf_op jit(solution)/shard_map/pallas_call | solution.py:38
  138.7 1.2 dynamic_update_slice.33
  139.9 0.9 slice_dynamic-update-slice_fusion.1
  140.8 0.9 constant_dynamic-update-slice_fusion.1
  141.7 10.0 %fusion.25 = f32[1024,1024]{1,0:T(8,128)} fusion(bf16[1024,2048]{1,0:T(8,128)(2,1)} %fusion.1, bf16[2048,1024]{1,0:T(8,128)(2,1)} %shard_map.67.refs_5_), kind=kOutput, calls=%fused_computation.56 | convolution fusion | flops 4294967296 | bytes 12582912 | tf_op jit(solution)/shard_map/dot_general | solution.py:128
  151.7 2.1 %shard_map.70.refs_5_ = bf16[1024,2048]{1,0:T(8,128)(2,1)} custom-call(s32[1]{0:T(128)} %bitcast.z_ref, bf16[256,1024]{1,0:T(8,128)(2,1)} %collective-permute-done.4.refs_9_.refs_0_, bf16[256,1024]{1,0:T(8,128)(2,1)} %collective-permute-done.10.refs_10_.refs_1_, bf16[1024,2048]{1,0:T(8,128)(2,1)} %shard_map.69.refs_2_), custom_call_target="tpu_custom_call", output_to_operand_aliasing={{}: (3, {})} | custom-call | tf_op jit(solution)/shard_map/pallas_call | solution.py:38
  153.8 0.7 slice_dynamic-update-slice_fusion
  154.5 3.2 %collective-permute-start.15 = (bf16[128,1024]{1,0:T(8,128)(2,1)}, bf16[128,1024]{1,0:T(8,128)(2,1)S(1)}, u32[]{:S(2)}, u32[]{:S(2)}) collective-permute-start(bf16[128,1024]{1,0:T(8,128)(2,1)} %get-tuple-element.22), channel_id=1, source_target_pairs={{0,120},{8,0},{16,8},{24,16},{32,24},{40,32},{48,40},{56,48},{64,5... | collective-permute-start | bytes 786440 | tf_op jit(solution)/shard_map/ppermute | solution.py:90
  157.8 0.8 constant_dynamic-update-slice_fusion
  158.5 3.3 %fusion.26 = f32[1024,1024]{1,0:T(8,128)S(1)} fusion(bf16[1024,640]{1,0:T(8,128)(2,1)S(1)} %copy-done.15, bf16[640,1024]{1,0:T(8,128)(2,1)} %constant_dynamic-update-slice_fusion), kind=kOutput, calls=%fused_computation.57 | convolution fusion | flops 1342177280 | bytes 6815744 | tf_op jit(solution)/shard_map/dot_general | solution.py:143
  161.8 1.1 multiply_convert_fusion
  163.0 0.7 copy-done.18
  163.7 2.7 %shard_map.71 = bf16[1024,2048]{1,0:T(8,128)(2,1)} custom-call(s32[1]{0:T(128)} %bitcast.z_ref, bf16[256,1024]{1,0:T(8,128)(2,1)} %copy-done.6, bf16[256,1024]{1,0:T(8,128)(2,1)} %copy-done.5, bf16[256,1024]{1,0:T(8,128)(2,1)} %copy-done.7, bf16[256,1024]{1,0:T(8,128)(2,1)} %copy-done.2, ...), custom_call_target="tpu_custom_call", output_to_operand_aliasing={{}: (6, {})} | custom-call | tf_op jit(solution)/shard_map/pallas_call | solution.py:38
  166.4 3.3 %convolution_convert_fusion.1 = bf16[1024,768]{1,0:T(8,128)(2,1)S(1)} fusion(bf16[1024,1024]{1,0:T(8,128)(2,1)S(1)} %multiply_convert_fusion, bf16[1024,2048]{1,0:T(8,128)(2,1)} %shard_map.71), kind=kOutput, calls=%fused_computation.10 | convolution fusion | flops 1611399168 | bytes 5242880 | tf_op jit(solution)/shard_map/dot_general | solution.py:161
  170.0 3.2 %convolution_convert_fusion = bf16[1024,1280]{1,0:T(8,128)(2,1)S(1)} fusion(bf16[1024,1024]{1,0:T(8,128)(2,1)S(1)} %multiply_convert_fusion, bf16[1024,2048]{1,0:T(8,128)(2,1)S(1)} %copy-done), kind=kOutput, calls=%fused_computation.7 | convolution fusion | flops 2685665280 | bytes 7340032 | tf_op jit(solution)/shard_map/dot_general | solution.py:161
  173.2 0.6 collective-permute-start.21
  174.0 0.7 collective-permute-start.17
  174.7 2.7 %collective-permute-start.19 = (bf16[128,384]{1,0:T(8,128)(2,1)S(1)}, bf16[128,384]{1,0:T(8,128)(2,1)S(1)}, u32[]{:S(2)}, u32[]{:S(2)}) collective-permute-start(bf16[128,384]{1,0:T(8,128)(2,1)S(1)} %get-tuple-element.16), channel_id=1, source_target_pairs={{0,6},{1,7},{2,0},{3,1},{4,2},{5,3},{6,4},{7,5},{8,14},{9,15},{10,... | collective-permute-start | bytes 294920 | tf_op jit(solution)/shard_map/ppermute | solution.py:169
  177.4 0.7 fusion.23
  178.1 2.0 collective-permute-done.17
  180.1 0.7 fusion.16
  180.9 3.1 %collective-permute-start.20 = (bf16[128,768]{1,0:T(8,128)(2,1)}, bf16[128,768]{1,0:T(8,128)(2,1)}, u32[]{:S(2)}, u32[]{:S(2)}) collective-permute-start(bf16[128,768]{1,0:T(8,128)(2,1)} %get-tuple-element.10), channel_id=1, source_target_pairs={{0,6},{1,7},{2,0},{3,1},{4,2},{5,3},{6,4},{7,5},{8,14},{9,15},{10,... | collective-permute-start | bytes 589832 | tf_op jit(solution)/shard_map/ppermute | solution.py:175
  184.1 0.3 convert_add_fusion
  184.6 3.2 %collective-permute-start.24 = (bf16[128,640]{1,0:T(8,128)(2,1)S(1)}, bf16[128,640]{1,0:T(8,128)(2,1)S(1)}, u32[]{:S(2)}, u32[]{:S(2)}) collective-permute-start(bf16[128,640]{1,0:T(8,128)(2,1)S(1)} %get-tuple-element.12), channel_id=1, source_target_pairs={{0,6},{1,7},{2,0},{3,1},{4,2},{5,3},{6,4},{7,5},{8,14},{9,15},{10,... | collective-permute-start | bytes 491528 | tf_op jit(solution)/shard_map/ppermute | solution.py:169
  187.8 3.7 %collective-permute-done.22 = bf16[128,640]{1,0:T(8,128)(2,1)S(1)} collective-permute-done((bf16[128,640]{1,0:T(8,128)(2,1)S(1)}, bf16[128,640]{1,0:T(8,128)(2,1)S(1)}, u32[]{:S(2)}, u32[]{:S(2)}) %collective-permute-start.22) | collective-permute-done | bytes 163872 | tf_op jit(solution)/shard_map/ppermute | solution.py:168
  191.6 1.0 collective-permute-start.23
  192.7 2.4 %collective-permute-start.25 = (bf16[128,1280]{1,0:T(8,128)(2,1)S(1)}, bf16[128,1280]{1,0:T(8,128)(2,1)}, u32[]{:S(2)}, u32[]{:S(2)}) collective-permute-start(bf16[128,1280]{1,0:T(8,128)(2,1)S(1)} %get-tuple-element.6), channel_id=1, source_target_pairs={{0,6},{1,7},{2,0},{3,1},{4,2},{5,3},{6,4},{7,5},{8,14},{9,15},{10,... | collective-permute-start | bytes 983048 | tf_op jit(solution)/shard_map/ppermute | solution.py:175
  195.1 2.7 %shard_map.68 = bf16[2048,1024]{1,0:T(8,128)(2,1)} custom-call(s32[1]{0:T(128)} %bitcast.z_ref, bf16[256,1024]{1,0:T(8,128)(2,1)} %copy-done.6, bf16[256,1024]{1,0:T(8,128)(2,1)} %copy-done.5, bf16[256,1024]{1,0:T(8,128)(2,1)} %copy-done.7, bf16[256,1024]{1,0:T(8,128)(2,1)} %copy-done.2, ...), custom_call_target="tpu_custom_call", output_to_operand_aliasing={{}: (6, {})} | custom-call | tf_op jit(solution)/shard_map/pallas_call | solution.py:38
  197.8 1.2 fusion.8
  199.0 2.7 %collective-permute-done.23 = bf16[128,1280]{1,0:T(8,128)(2,1)} collective-permute-done((bf16[128,1280]{1,0:T(8,128)(2,1)S(1)}, bf16[128,1280]{1,0:T(8,128)(2,1)}, u32[]{:S(2)}, u32[]{:S(2)}) %collective-permute-start.23) | collective-permute-done | bytes 327712 | tf_op jit(solution)/shard_map/ppermute | solution.py:174
  201.7 1.2 fusion.9
  202.9 0.8 copy-done.17
  (85 shorter events, 2.4 us)
Async XLA Ops:
  19.7 81.2 %copy-start.1 = (bf16[256,1024]{1,0:T(8,128)(2,1)}, bf16[256,1024]{1,0:T(8,128)(2,1)S(1)}, u32[]{:S(2)}) copy-start(bf16[256,1024]{1,0:T(8,128)(2,1)S(1)} %pad_maximum_fusion.1.refs_0_) | copy-start | bytes 1572868
  19.7 33.3 %collective-permute-start.6 = (bf16[256,1024]{1,0:T(8,128)(2,1)S(1)}, bf16[256,1024]{1,0:T(8,128)(2,1)S(1)}, u32[]{:S(2)}, u32[]{:S(2)}) collective-permute-start(bf16[256,1024]{1,0:T(8,128)(2,1)S(1)} %pad_maximum_fusion.1.refs_0_), channel_id=1, source_target_pairs={{0,120},{8,0},{16,8},{24,16},{32,24},{40,32},{48,40},{56,48},{64,5... | collective-permute-start | bytes 1572872 | tf_op jit(solution)/shard_map/ppermute | solution.py:88
  42.2 14.5 %collective-permute-start = (bf16[256,1024]{1,0:T(8,128)(2,1)S(1)}, bf16[256,1024]{1,0:T(8,128)(2,1)S(1)}, u32[]{:S(2)}, u32[]{:S(2)}) collective-permute-start(bf16[256,1024]{1,0:T(8,128)(2,1)S(1)} %pad_maximum_fusion.1.refs_0_), channel_id=1, source_target_pairs={{0,8},{8,16},{16,24},{24,32},{32,40},{40,48},{48,56},{56,64},{64,7... | collective-permute-start | bytes 1572872 | tf_op jit(solution)/shard_map/ppermute | solution.py:87
  53.0 3.7 %copy-start.8 = (bf16[256,1024]{1,0:T(8,128)(2,1)}, bf16[256,1024]{1,0:T(8,128)(2,1)S(1)}, u32[]{:S(2)}) copy-start(bf16[256,1024]{1,0:T(8,128)(2,1)S(1)} %collective-permute-done.6.refs_2_) | copy-start | bytes 1572868
  53.0 13.7 %collective-permute-start.7 = (bf16[256,1024]{1,0:T(8,128)(2,1)S(1)}, bf16[256,1024]{1,0:T(8,128)(2,1)S(1)}, u32[]{:S(2)}, u32[]{:S(2)}) collective-permute-start(bf16[256,1024]{1,0:T(8,128)(2,1)S(1)} %collective-permute-done.6.refs_2_), channel_id=1, source_target_pairs={{0,120},{8,0},{16,8},{24,16},{32,24},{40,32},{48,40},{56,48},{64,5... | collective-permute-start | bytes 1572872 | tf_op jit(solution)/shard_map/ppermute | solution.py:88
  56.7 10.0 %copy-start.9 = (bf16[256,1024]{1,0:T(8,128)(2,1)}, bf16[256,1024]{1,0:T(8,128)(2,1)S(1)}, u32[]{:S(2)}) copy-start(bf16[256,1024]{1,0:T(8,128)(2,1)S(1)} %collective-permute-done.refs_1_) | copy-start | bytes 1572868
  56.7 13.7 %collective-permute-start.1 = (bf16[256,1024]{1,0:T(8,128)(2,1)S(1)}, bf16[256,1024]{1,0:T(8,128)(2,1)S(1)}, u32[]{:S(2)}, u32[]{:S(2)}) collective-permute-start(bf16[256,1024]{1,0:T(8,128)(2,1)S(1)} %collective-permute-done.refs_1_), channel_id=1, source_target_pairs={{0,8},{8,16},{16,24},{24,32},{32,40},{40,48},{48,56},{56,64},{64,7... | collective-permute-start | bytes 1572872 | tf_op jit(solution)/shard_map/ppermute | solution.py:87
  66.7 34.2 %copy-start.10 = (bf16[256,1024]{1,0:T(8,128)(2,1)}, bf16[256,1024]{1,0:T(8,128)(2,1)S(1)}, u32[]{:S(2)}) copy-start(bf16[256,1024]{1,0:T(8,128)(2,1)S(1)} %collective-permute-done.7.refs_4_) | copy-start | bytes 1572868
  66.7 12.8 %collective-permute-start.8 = (bf16[256,1024]{1,0:T(8,128)(2,1)S(1)}, bf16[256,1024]{1,0:T(8,128)(2,1)S(1)}, u32[]{:S(2)}, u32[]{:S(2)}) collective-permute-start(bf16[256,1024]{1,0:T(8,128)(2,1)S(1)} %collective-permute-done.7.refs_4_), channel_id=1, source_target_pairs={{0,120},{8,0},{16,8},{24,16},{32,24},{40,32},{48,40},{56,48},{64,5... | collective-permute-start | bytes 1572872 | tf_op jit(solution)/shard_map/ppermute | solution.py:88
  70.4 30.5 %copy-start.11 = (bf16[256,1024]{1,0:T(8,128)(2,1)}, bf16[256,1024]{1,0:T(8,128)(2,1)S(1)}, u32[]{:S(2)}) copy-start(bf16[256,1024]{1,0:T(8,128)(2,1)S(1)} %collective-permute-done.1.refs_3_) | copy-start | bytes 1572868
  70.4 12.8 %collective-permute-start.2 = (bf16[256,1024]{1,0:T(8,128)(2,1)S(1)}, bf16[256,1024]{1,0:T(8,128)(2,1)S(1)}, u32[]{:S(2)}, u32[]{:S(2)}) collective-permute-start(bf16[256,1024]{1,0:T(8,128)(2,1)S(1)} %collective-permute-done.1.refs_3_), channel_id=1, source_target_pairs={{0,8},{8,16},{16,24},{24,32},{32,40},{40,48},{48,56},{56,64},{64,7... | collective-permute-start | bytes 1572872 | tf_op jit(solution)/shard_map/ppermute | solution.py:87
  79.5 21.4 %copy-start.12 = (bf16[256,1024]{1,0:T(8,128)(2,1)}, bf16[256,1024]{1,0:T(8,128)(2,1)S(1)}, u32[]{:S(2)}) copy-start(bf16[256,1024]{1,0:T(8,128)(2,1)S(1)} %collective-permute-done.8.refs_6_) | copy-start | bytes 1572868
  79.5 12.1 %collective-permute-start.9 = (bf16[256,1024]{1,0:T(8,128)(2,1)S(1)}, bf16[256,1024]{1,0:T(8,128)(2,1)S(1)}, u32[]{:S(2)}, u32[]{:S(2)}) collective-permute-start(bf16[256,1024]{1,0:T(8,128)(2,1)S(1)} %collective-permute-done.8.refs_6_), channel_id=1, source_target_pairs={{0,120},{8,0},{16,8},{24,16},{32,24},{40,32},{48,40},{56,48},{64,5... | collective-permute-start | bytes 1572872 | tf_op jit(solution)/shard_map/ppermute | solution.py:88
  83.2 24.0 %copy-start.13 = (bf16[256,1024]{1,0:T(8,128)(2,1)}, bf16[256,1024]{1,0:T(8,128)(2,1)S(1)}, u32[]{:S(2)}) copy-start(bf16[256,1024]{1,0:T(8,128)(2,1)S(1)} %collective-permute-done.2.refs_5_) | copy-start | bytes 1572868
  83.2 12.1 %collective-permute-start.3 = (bf16[256,1024]{1,0:T(8,128)(2,1)S(1)}, bf16[256,1024]{1,0:T(8,128)(2,1)}, u32[]{:S(2)}, u32[]{:S(2)}) collective-permute-start(bf16[256,1024]{1,0:T(8,128)(2,1)S(1)} %collective-permute-done.2.refs_5_), channel_id=1, source_target_pairs={{0,8},{8,16},{16,24},{24,32},{32,40},{40,48},{48,56},{56,64},{64,7... | collective-permute-start | bytes 1572872 | tf_op jit(solution)/shard_map/ppermute | solution.py:87
  91.6 28.3 %copy-start.14 = (bf16[256,1024]{1,0:T(8,128)(2,1)}, bf16[256,1024]{1,0:T(8,128)(2,1)S(1)}, u32[]{:S(2)}) copy-start(bf16[256,1024]{1,0:T(8,128)(2,1)S(1)} %collective-permute-done.9.refs_8_) | copy-start | bytes 1572868
  91.6 11.8 %collective-permute-start.10 = (bf16[256,1024]{1,0:T(8,128)(2,1)S(1)}, bf16[256,1024]{1,0:T(8,128)(2,1)}, u32[]{:S(2)}, u32[]{:S(2)}) collective-permute-start(bf16[256,1024]{1,0:T(8,128)(2,1)S(1)} %collective-permute-done.9.refs_8_), channel_id=1, source_target_pairs={{0,120},{8,0},{16,8},{24,16},{32,24},{40,32},{48,40},{56,48},{64,5... | collective-permute-start | bytes 1572872 | tf_op jit(solution)/shard_map/ppermute | solution.py:88
  95.3 11.9 %collective-permute-start.4 = (bf16[256,1024]{1,0:T(8,128)(2,1)}, bf16[256,1024]{1,0:T(8,128)(2,1)}, u32[]{:S(2)}, u32[]{:S(2)}) collective-permute-start(bf16[256,1024]{1,0:T(8,128)(2,1)} %collective-permute-done.3.refs_7_), channel_id=1, source_target_pairs={{0,8},{8,16},{16,24},{24,32},{32,40},{40,48},{48,56},{56,64},{64,7... | collective-permute-start | bytes 1572872 | tf_op jit(solution)/shard_map/ppermute | solution.py:87
  103.3 13.0 %collective-permute-start.11 = (bf16[256,1024]{1,0:T(8,128)(2,1)}, bf16[256,1024]{1,0:T(8,128)(2,1)S(1)}, u32[]{:S(2)}, u32[]{:S(2)}) collective-permute-start(bf16[256,1024]{1,0:T(8,128)(2,1)} %collective-permute-done.10.refs_10_.refs_1_), channel_id=1, source_target_pairs={{0,120},{8,0},{16,8},{24,16},{32,24},{40,32},{48,40},{56,48},{64,5... | collective-permute-start | bytes 1572872 | tf_op jit(solution)/shard_map/ppermute | solution.py:88
  107.1 12.9 %collective-permute-start.5 = (bf16[256,1024]{1,0:T(8,128)(2,1)}, bf16[256,1024]{1,0:T(8,128)(2,1)S(1)}, u32[]{:S(2)}, u32[]{:S(2)}) collective-permute-start(bf16[256,1024]{1,0:T(8,128)(2,1)} %collective-permute-done.4.refs_9_.refs_0_), channel_id=1, source_target_pairs={{0,8},{8,16},{16,24},{24,32},{32,40},{40,48},{48,56},{56,64},{64,7... | collective-permute-start | bytes 1572872 | tf_op jit(solution)/shard_map/ppermute | solution.py:87
  116.3 22.4 %copy-start.5 = (bf16[256,1024]{1,0:T(8,128)(2,1)}, bf16[256,1024]{1,0:T(8,128)(2,1)S(1)}, u32[]{:S(2)}) copy-start(bf16[256,1024]{1,0:T(8,128)(2,1)S(1)} %collective-permute-done.11.refs_1_) | copy-start | bytes 1572868
  116.3 23.7 %collective-permute-start.13 = (bf16[256,1024]{1,0:T(8,128)(2,1)S(1)}, bf16[256,1024]{1,0:T(8,128)(2,1)S(1)}, u32[]{:S(2)}, u32[]{:S(2)}) collective-permute-start(bf16[256,1024]{1,0:T(8,128)(2,1)S(1)} %collective-permute-done.11.refs_1_), channel_id=1, source_target_pairs={{0,120},{8,0},{16,8},{24,16},{32,24},{40,32},{48,40},{56,48},{64,5... | collective-permute-start | bytes 1572872 | tf_op jit(solution)/shard_map/ppermute | solution.py:88
  120.0 33.7 %copy-start.6 = (bf16[256,1024]{1,0:T(8,128)(2,1)}, bf16[256,1024]{1,0:T(8,128)(2,1)S(1)}, u32[]{:S(2)}) copy-start(bf16[256,1024]{1,0:T(8,128)(2,1)S(1)} %collective-permute-done.5.refs_0_) | copy-start | bytes 1572868
  120.1 20.8 %collective-permute-start.12 = (bf16[256,1024]{1,0:T(8,128)(2,1)S(1)}, bf16[256,1024]{1,0:T(8,128)(2,1)S(1)}, u32[]{:S(2)}, u32[]{:S(2)}) collective-permute-start(bf16[256,1024]{1,0:T(8,128)(2,1)S(1)} %collective-permute-done.5.refs_0_), channel_id=1, source_target_pairs={{0,8},{8,16},{16,24},{24,32},{32,40},{40,48},{48,56},{56,64},{64,7... | collective-permute-start | bytes 1572872 | tf_op jit(solution)/shard_map/ppermute | solution.py:87
  139.9 11.7 %copy-start.2 = (bf16[256,1024]{1,0:T(8,128)(2,1)}, bf16[256,1024]{1,0:T(8,128)(2,1)S(1)}, u32[]{:S(2)}) copy-start(bf16[256,1024]{1,0:T(8,128)(2,1)S(1)} %collective-permute-done.13.refs_3_) | copy-start | bytes 1572868
  140.8 10.8 %copy-start.7 = (bf16[256,1024]{1,0:T(8,128)(2,1)}, bf16[256,1024]{1,0:T(8,128)(2,1)S(1)}, u32[]{:S(2)}) copy-start(bf16[256,1024]{1,0:T(8,128)(2,1)S(1)} %collective-permute-done.12.refs_2_) | copy-start | bytes 1572868
  141.7 16.1 %collective-permute-start.14 = (bf16[128,1024]{1,0:T(8,128)(2,1)S(1)}, bf16[128,1024]{1,0:T(8,128)(2,1)S(1)}, u32[]{:S(2)}, u32[]{:S(2)}) collective-permute-start(bf16[128,1024]{1,0:T(8,128)(2,1)S(1)} %get-tuple-element.20), channel_id=1, source_target_pairs={{0,8},{8,16},{16,24},{24,32},{32,40},{40,48},{48,56},{56,64},{64,7... | collective-permute-start | bytes 786440 | tf_op jit(solution)/shard_map/ppermute | solution.py:89
  151.7 6.9 %copy-start.15 = (bf16[1024,640]{1,0:T(8,128)(2,1)S(1)}, bf16[1024,640]{1,0:T(8,128)(2,1)}, u32[]{:S(2)}) copy-start(bf16[1024,640]{1,0:T(8,128)(2,1)} %fusion.4) | copy-start | bytes 3932164
  154.5 8.4 %collective-permute-start.15 = (bf16[128,1024]{1,0:T(8,128)(2,1)}, bf16[128,1024]{1,0:T(8,128)(2,1)S(1)}, u32[]{:S(2)}, u32[]{:S(2)}) collective-permute-start(bf16[128,1024]{1,0:T(8,128)(2,1)} %get-tuple-element.22), channel_id=1, source_target_pairs={{0,120},{8,0},{16,8},{24,16},{32,24},{40,32},{48,40},{56,48},{64,5... | collective-permute-start | bytes 786440 | tf_op jit(solution)/shard_map/ppermute | solution.py:90
  157.8 4.0 %copy-start.16 = (bf16[128,1024]{1,0:T(8,128)(2,1)}, bf16[128,1024]{1,0:T(8,128)(2,1)S(1)}, u32[]{:S(2)}) copy-start(bf16[128,1024]{1,0:T(8,128)(2,1)S(1)} %collective-permute-done.14.refs_4_) | copy-start | bytes 786436
  158.5 3.3 %copy-start.3 = (f32[1024,1024]{1,0:T(8,128)S(1)}, f32[1024,1024]{1,0:T(8,128)}, u32[]{:S(2)}) copy-start(f32[1024,1024]{1,0:T(8,128)} %fusion.25) | copy-start | bytes 12582916
  163.0 0.7 copy-start.18
  166.4 3.6 %copy-start = (bf16[1024,2048]{1,0:T(8,128)(2,1)S(1)}, bf16[1024,2048]{1,0:T(8,128)(2,1)}, u32[]{:S(2)}) copy-start(bf16[1024,2048]{1,0:T(8,128)(2,1)} %shard_map.71) | copy-start | bytes 12582916
  169.8 4.0 %collective-permute-start.16 = (bf16[512,768]{1,0:T(8,128)(2,1)S(1)}, bf16[512,768]{1,0:T(8,128)(2,1)S(1)}, u32[]{:S(2)}, u32[]{:S(2)}) collective-permute-start(bf16[512,768]{1,0:T(8,128)(2,1)S(1)} %slice.139), channel_id=1, source_target_pairs={{0,1},{1,0},{2,3},{3,2},{4,5},{5,4},{6,7},{7,6},{8,9},{9,8},{10,11... | collective-permute-start | bytes 2359304 | tf_op jit(solution)/shard_map/ppermute | solution.py:162
  173.2 10.8 %collective-permute-start.21 = (bf16[512,1280]{1,0:T(8,128)(2,1)S(1)}, bf16[512,1280]{1,0:T(8,128)(2,1)S(1)}, u32[]{:S(2)}, u32[]{:S(2)}) collective-permute-start(bf16[512,1280]{1,0:T(8,128)(2,1)S(1)} %slice.149), channel_id=1, source_target_pairs={{0,1},{1,0},{2,3},{3,2},{4,5},{5,4},{6,7},{7,6},{8,9},{9,8},{10,11... | collective-permute-start | bytes 3932168 | tf_op jit(solution)/shard_map/ppermute | solution.py:162
  174.0 10.1 %copy-start.4 = (f32[512,768]{1,0:T(8,128)}, f32[512,768]{1,0:T(8,128)S(1)}, u32[]{:S(2)}) copy-start(f32[512,768]{1,0:T(8,128)S(1)} %get-tuple-element.8) | copy-start | bytes 4718596
  174.0 6.1 %collective-permute-start.17 = (bf16[128,384]{1,0:T(8,128)(2,1)S(1)}, bf16[128,384]{1,0:T(8,128)(2,1)S(1)}, u32[]{:S(2)}, u32[]{:S(2)}) collective-permute-start(bf16[128,384]{1,0:T(8,128)(2,1)S(1)} %get-tuple-element.15), channel_id=1, source_target_pairs={{0,2},{1,3},{2,4},{3,5},{4,6},{5,7},{6,0},{7,1},{8,10},{9,11},{10,... | collective-permute-start | bytes 294920 | tf_op jit(solution)/shard_map/ppermute | solution.py:168
  174.7 5.4 %collective-permute-start.19 = (bf16[128,384]{1,0:T(8,128)(2,1)S(1)}, bf16[128,384]{1,0:T(8,128)(2,1)S(1)}, u32[]{:S(2)}, u32[]{:S(2)}) collective-permute-start(bf16[128,384]{1,0:T(8,128)(2,1)S(1)} %get-tuple-element.16), channel_id=1, source_target_pairs={{0,6},{1,7},{2,0},{3,1},{4,2},{5,3},{6,4},{7,5},{8,14},{9,15},{10,... | collective-permute-start | bytes 294920 | tf_op jit(solution)/shard_map/ppermute | solution.py:169
  180.8 16.9 %collective-permute-start.18 = (bf16[128,768]{1,0:T(8,128)(2,1)S(1)}, bf16[128,768]{1,0:T(8,128)(2,1)}, u32[]{:S(2)}, u32[]{:S(2)}) collective-permute-start(bf16[128,768]{1,0:T(8,128)(2,1)S(1)} %get-tuple-element.9), channel_id=1, source_target_pairs={{0,2},{1,3},{2,4},{3,5},{4,6},{5,7},{6,0},{7,1},{8,10},{9,11},{10,... | collective-permute-start | bytes 589832 | tf_op jit(solution)/shard_map/ppermute | solution.py:174
  180.9 16.8 %collective-permute-start.20 = (bf16[128,768]{1,0:T(8,128)(2,1)}, bf16[128,768]{1,0:T(8,128)(2,1)}, u32[]{:S(2)}, u32[]{:S(2)}) collective-permute-start(bf16[128,768]{1,0:T(8,128)(2,1)} %get-tuple-element.10), channel_id=1, source_target_pairs={{0,6},{1,7},{2,0},{3,1},{4,2},{5,3},{6,4},{7,5},{8,14},{9,15},{10,... | collective-permute-start | bytes 589832 | tf_op jit(solution)/shard_map/ppermute | solution.py:175
  184.4 7.1 %collective-permute-start.22 = (bf16[128,640]{1,0:T(8,128)(2,1)S(1)}, bf16[128,640]{1,0:T(8,128)(2,1)S(1)}, u32[]{:S(2)}, u32[]{:S(2)}) collective-permute-start(bf16[128,640]{1,0:T(8,128)(2,1)S(1)} %get-tuple-element.11), channel_id=1, source_target_pairs={{0,2},{1,3},{2,4},{3,5},{4,6},{5,7},{6,0},{7,1},{8,10},{9,11},{10,... | collective-permute-start | bytes 491528 | tf_op jit(solution)/shard_map/ppermute | solution.py:168
  184.6 7.0 %collective-permute-start.24 = (bf16[128,640]{1,0:T(8,128)(2,1)S(1)}, bf16[128,640]{1,0:T(8,128)(2,1)S(1)}, u32[]{:S(2)}, u32[]{:S(2)}) collective-permute-start(bf16[128,640]{1,0:T(8,128)(2,1)S(1)} %get-tuple-element.12), channel_id=1, source_target_pairs={{0,6},{1,7},{2,0},{3,1},{4,2},{5,3},{6,4},{7,5},{8,14},{9,15},{10,... | collective-permute-start | bytes 491528 | tf_op jit(solution)/shard_map/ppermute | solution.py:169
  191.6 10.0 %collective-permute-start.23 = (bf16[128,1280]{1,0:T(8,128)(2,1)S(1)}, bf16[128,1280]{1,0:T(8,128)(2,1)}, u32[]{:S(2)}, u32[]{:S(2)}) collective-permute-start(bf16[128,1280]{1,0:T(8,128)(2,1)S(1)} %get-tuple-element.5), channel_id=1, source_target_pairs={{0,2},{1,3},{2,4},{3,5},{4,6},{5,7},{6,0},{7,1},{8,10},{9,11},{10,... | collective-permute-start | bytes 983048 | tf_op jit(solution)/shard_map/ppermute | solution.py:174
  192.7 9.0 %collective-permute-start.25 = (bf16[128,1280]{1,0:T(8,128)(2,1)S(1)}, bf16[128,1280]{1,0:T(8,128)(2,1)}, u32[]{:S(2)}, u32[]{:S(2)}) collective-permute-start(bf16[128,1280]{1,0:T(8,128)(2,1)S(1)} %get-tuple-element.6), channel_id=1, source_target_pairs={{0,6},{1,7},{2,0},{3,1},{4,2},{5,3},{6,4},{7,5},{8,14},{9,15},{10,... | collective-permute-start | bytes 983048 | tf_op jit(solution)/shard_map/ppermute | solution.py:175
  202.9 0.8 copy-start.17

commit v5 on v4

--- a/solution.py
+++ b/solution.py
@@ -43,6 +43,7 @@
         + [anywhere] * n_old,
         out_specs=[anywhere] * len(outs),
         scratch_shapes=[pltpu.SemaphoreType.DMA((len(moves),))],
+        compiler_params=pltpu.CompilerParams(vmem_limit_bytes=12 * 2**20),
         input_output_aliases={1 + len(pieces) + k: k for k in range(n_old)},
     )(z.reshape(1), *pieces, *old)
 
@@ -140,12 +141,12 @@
         features, (z + late[0]) % n_fs * up_rows, len(late) * up_rows, axis=1
     )
     features = lax.optimization_barrier(features)
-    added = jnp.dot(features, rest, preferred_element_type=jnp.float32)
-    pre_act = pre_act + lax.optimization_barrier(added)
+    pre_act = pre_act + jnp.dot(features, rest, preferred_element_type=jnp.float32)
     hidden = jnp.square(jax.nn.relu(pre_act)).astype(jnp.bfloat16)
 
     moves = down_moves(within(half - 2, half - 1))
-    moves += [(down_far, k * span, span, 0, half, span, 0, k * width) for k in range(sides)]
+    down_sampler = place(z, moves, down_shape, n_fs, down_sampler)
+    moves = [(down_far, k * span, span, 0, half, span, 0, k * width) for k in range(sides)]
     down_sampler = place(z, moves, down_shape, n_fs, down_sampler)[0]
     moves = up_moves(within(half - 2, half - 1))
     moves += [(up_far, 0, up_rows, 0, half, up_rows, 0, 0)]
@@ -154,7 +155,7 @@
     pair = [(k, k ^ 1) for k in range(n_tp)]
     right = [(j, (j + 2) % n_tp) for j in range(n_tp)]
     left = [(j, (j - 2) % n_tp) for j in range(n_tp)]
-    bounds = [0, 3 * full // 8, full]
+    bounds = [0, 5 * full // 8, full]
     summed = jnp.zeros((block, full), jnp.bfloat16)
     for lo, hi in zip(bounds[:-1], bounds[1:]):
         weights = lax.slice_in_dim(down_sampler, lo, hi, axis=1)

time: 205 us -> 188 us (0.917)
  local copies, waits for them, and re-layouts: 26.7 us -> 21.2 us
  matrix products: 19.7 us -> 14.6 us
  Pallas kernels: 16.2 us -> 11.7 us
  other arithmetic: 17.7 us -> 13.7 us
  waiting for transfers between devices: 45.4 us -> 47.9 us
    pallas_call x5 -> x6, Pallas kernels: 16.2 us -> 11.7 us  [place(): pl.pallas_call(body, out_shape=outs, in_specs=[pl.BlockSpec(memory_space=...]
    ppermute x2, waiting for transfers between devices: 2.66 us -> 6.82 us  [on_device(): after = lax.ppermute(after, 'tp', right).astype(jnp.float32)]
    dynamic_update_slice x5, local copies, waits for them, and re-layouts: 4.43 us -> 0.28 us  [on_device(): rest = lax.dynamic_update_slice(rest, band, ((k - late[0]) * up_rows, 0))]
    dot_general x1, matrix products: 9.97 us -> 6.3 us  [on_device(): pre_act = jnp.dot(normed, up_sampler[0], preferred_element_type=jnp.float32)]
    ppermute x2, waiting for transfers between devices: 5.76 us -> 3.53 us  [on_device(): first = lax.ppermute(ends[0], 'tp', right).astype(jnp.float32)]
    unnamed x47 -> x31, local copies, waits for them, and re-layouts: 16.4 us -> 15.5 us
  transfers between devices with their start and end apart: 26 -> 26, of which waited for: 10 -> 10; matrix products, arithmetic and copies ran while one was open for 26% -> 22% of each run, Pallas kernels for 7% -> 6%
where the time goes in v5:
time: 188 us
  starting transfers between devices  62.4 us (33%)
  waiting for transfers between devices  47.9 us (25%)
  local copies, waits for them, and re-layouts  21.2 us (11%)
  blocking collectives  14.7 us (8%)
  matrix products  14.6 us (8%)
  other arithmetic  13.7 us (7%)
  Pallas kernels  11.7 us (6%)
    ppermute x7, starting transfers between devices, on_device(): held[step] = lax.ppermute(held[step - 1], 'fs', back)  44.6 us
    ppermute x7, waiting for transfers between devices, on_device(): held[step] = lax.ppermute(held[step - 1], 'fs', back)  37.3 us
    unnamed x31, local copies, waits for them, and re-layouts  15.5 us
    all_to_all x1, blocking collectives, on_device(): parts = lax.all_to_all(parts, 'tp', split_axis=0, concat_axis=0, tiled=True)  14.7 us
    pallas_call x6, Pallas kernels, place(): pl.pallas_call(body, out_shape=outs, in_specs=[pl.BlockSpec(memory_space=...  11.7 us
    ppermute x2, waiting for transfers between devices, on_device(): after = lax.ppermute(after, 'tp', right).astype(jnp.float32)  6.82 us
    dot_general x2, matrix products, on_device(): jnp.dot(hidden, weights, preferred_element_type=jnp.float32)  6.52 us
    ppermute x2, starting transfers between devices, on_device(): before = lax.ppermute(before, 'tp', left).astype(jnp.float32)  6.42 us
  transfers between devices with their start and end apart: 26, of which 10 were waited for; matrix products, arithmetic and copies ran while one was open for 22% of the time, Pallas kernels for 6%

profile of v5, /device:TPU:40, one launch (start us, length us, event | category | flops | bytes accessed | tf_op | source)
XLA Modules:
  0.0 187.6 jit_solution(15040948792185794902)
XLA Ops:
  0.6 1.1 convert_element_type.82
  1.8 0.2 copy.35
  2.0 1.2 copy.32
  3.3 0.7 multiply_convert_fusion.1
  4.1 14.7 %all_to_all.5 = bf16[8,2,128,128]{2,3,1,0:T(8,128)(2,1)S(1)} all-to-all(bf16[8,2,128,128]{2,3,1,0:T(8,128)(2,1)S(1)} %copy.36), channel_id=1, replica_groups=mesh['grp'=2,'fs'=16,'tp'=8] {'tp'}, dimensions={0} | all-to-all | bytes 1048576 | tf_op jit(solution)/shard_map/all_to_all | solution.py:77
  18.9 0.1 copy.40
  19.0 0.2 copy.41
  19.2 0.3 copy.39
  19.5 0.2 reshape.47
  19.7 22.5 %collective-permute-start.6 = (bf16[256,1024]{1,0:T(8,128)(2,1)S(1)}, bf16[256,1024]{1,0:T(8,128)(2,1)S(1)}, u32[]{:S(2)}, u32[]{:S(2)}) collective-permute-start(bf16[256,1024]{1,0:T(8,128)(2,1)S(1)} %pad_maximum_fusion.1.refs_0_), channel_id=1, source_target_pairs={{0,120},{8,0},{16,8},{24,16},{32,24},{40,32},{48,40},{56,48},{64,5... | collective-permute-start | bytes 1572872 | tf_op jit(solution)/shard_map/ppermute | solution.py:89
  42.2 10.8 %collective-permute-done.6.refs_2_ = bf16[256,1024]{1,0:T(8,128)(2,1)S(1)} collective-permute-done((bf16[256,1024]{1,0:T(8,128)(2,1)S(1)}, bf16[256,1024]{1,0:T(8,128)(2,1)S(1)}, u32[]{:S(2)}, u32[]{:S(2)}) %collective-permute-start.6) | collective-permute-done | bytes 524320 | tf_op jit(solution)/shard_map/ppermute | solution.py:89
  53.0 3.7 %collective-permute-start.7 = (bf16[256,1024]{1,0:T(8,128)(2,1)S(1)}, bf16[256,1024]{1,0:T(8,128)(2,1)S(1)}, u32[]{:S(2)}, u32[]{:S(2)}) collective-permute-start(bf16[256,1024]{1,0:T(8,128)(2,1)S(1)} %collective-permute-done.6.refs_2_), channel_id=1, source_target_pairs={{0,120},{8,0},{16,8},{24,16},{32,24},{40,32},{48,40},{56,48},{64,5... | collective-permute-start | bytes 1572872 | tf_op jit(solution)/shard_map/ppermute | solution.py:89
  56.7 9.9 %collective-permute-done.7.refs_4_ = bf16[256,1024]{1,0:T(8,128)(2,1)S(1)} collective-permute-done((bf16[256,1024]{1,0:T(8,128)(2,1)S(1)}, bf16[256,1024]{1,0:T(8,128)(2,1)S(1)}, u32[]{:S(2)}, u32[]{:S(2)}) %collective-permute-start.7) | collective-permute-done | bytes 524320 | tf_op jit(solution)/shard_map/ppermute | solution.py:89
  66.7 3.7 %collective-permute-start.8 = (bf16[256,1024]{1,0:T(8,128)(2,1)S(1)}, bf16[256,1024]{1,0:T(8,128)(2,1)S(1)}, u32[]{:S(2)}, u32[]{:S(2)}) collective-permute-start(bf16[256,1024]{1,0:T(8,128)(2,1)S(1)} %collective-permute-done.7.refs_4_), channel_id=1, source_target_pairs={{0,120},{8,0},{16,8},{24,16},{32,24},{40,32},{48,40},{56,48},{64,5... | collective-permute-start | bytes 1572872 | tf_op jit(solution)/shard_map/ppermute | solution.py:89
  70.5 2.0 %dynamic-slice_dynamic-update-slice_fusion.7 = bf16[1024,2048]{1,0:T(8,128)(2,1)} fusion(bf16[1024,2048]{1,0:T(8,128)(2,1)} %param.4, s32[]{:T(128)S(6)} %select_n.90), kind=kLoop, calls=%fused_computation.26 | loop fusion | bytes 1048580
  72.4 1.9 %dynamic-slice_dynamic-update-slice_fusion.6 = bf16[1024,2048]{1,0:T(8,128)(2,1)} fusion(bf16[1024,2048]{1,0:T(8,128)(2,1)} %dynamic-slice_dynamic-update-slice_fusion.7, bf16[1024,2048]{1,0:T(8,128)(2,1)} %param.4, s32[]{:T(128)S(6)} %select_n.92), kind=kLoop, calls=%fused_computation.25 | loop fusion | bytes 1048580
  74.3 5.1 %collective-permute-done.8.refs_6_ = bf16[256,1024]{1,0:T(8,128)(2,1)S(1)} collective-permute-done((bf16[256,1024]{1,0:T(8,128)(2,1)S(1)}, bf16[256,1024]{1,0:T(8,128)(2,1)S(1)}, u32[]{:S(2)}, u32[]{:S(2)}) %collective-permute-start.8) | collective-permute-done | bytes 524320 | tf_op jit(solution)/shard_map/ppermute | solution.py:89
  79.5 3.7 %collective-permute-start.9 = (bf16[256,1024]{1,0:T(8,128)(2,1)S(1)}, bf16[256,1024]{1,0:T(8,128)(2,1)}, u32[]{:S(2)}, u32[]{:S(2)}) collective-permute-start(bf16[256,1024]{1,0:T(8,128)(2,1)S(1)} %collective-permute-done.8.refs_6_), channel_id=1, source_target_pairs={{0,120},{8,0},{16,8},{24,16},{32,24},{40,32},{48,40},{56,48},{64,5... | collective-permute-start | bytes 1572872 | tf_op jit(solution)/shard_map/ppermute | solution.py:89
  83.2 1.9 %dynamic-slice_dynamic-update-slice_fusion.5 = bf16[1024,2048]{1,0:T(8,128)(2,1)} fusion(bf16[1024,2048]{1,0:T(8,128)(2,1)} %dynamic-slice_dynamic-update-slice_fusion.6, bf16[1024,2048]{1,0:T(8,128)(2,1)} %param.4, s32[]{:T(128)S(6)} %select_n.94), kind=kLoop, calls=%fused_computation.24 | loop fusion | bytes 1048580
  85.0 1.9 %dynamic-slice_dynamic-update-slice_fusion.4 = bf16[1024,2048]{1,0:T(8,128)(2,1)} fusion(bf16[1024,2048]{1,0:T(8,128)(2,1)} %dynamic-slice_dynamic-update-slice_fusion.5, bf16[1024,2048]{1,0:T(8,128)(2,1)} %param.4, s32[]{:T(128)S(6)} %select_n.96), kind=kLoop, calls=%fused_computation.23 | loop fusion | bytes 1048580
  86.9 1.9 %dynamic-slice_dynamic-update-slice_fusion.3 = bf16[1024,2048]{1,0:T(8,128)(2,1)} fusion(bf16[1024,2048]{1,0:T(8,128)(2,1)} %dynamic-slice_dynamic-update-slice_fusion.4, bf16[1024,2048]{1,0:T(8,128)(2,1)} %param.4, s32[]{:T(128)S(6)} %select_n.98), kind=kLoop, calls=%fused_computation.22 | loop fusion | bytes 1048580
  88.8 2.6 %collective-permute-done.9.refs_8_ = bf16[256,1024]{1,0:T(8,128)(2,1)} collective-permute-done((bf16[256,1024]{1,0:T(8,128)(2,1)S(1)}, bf16[256,1024]{1,0:T(8,128)(2,1)}, u32[]{:S(2)}, u32[]{:S(2)}) %collective-permute-start.9) | collective-permute-done | bytes 524320 | tf_op jit(solution)/shard_map/ppermute | solution.py:89
  91.4 3.8 %collective-permute-start.10 = (bf16[256,1024]{1,0:T(8,128)(2,1)}, bf16[256,1024]{1,0:T(8,128)(2,1)}, u32[]{:S(2)}, u32[]{:S(2)}) collective-permute-start(bf16[256,1024]{1,0:T(8,128)(2,1)} %collective-permute-done.9.refs_8_), channel_id=1, source_target_pairs={{0,120},{8,0},{16,8},{24,16},{32,24},{40,32},{48,40},{56,48},{64,5... | collective-permute-start | bytes 1572872 | tf_op jit(solution)/shard_map/ppermute | solution.py:89
  95.2 1.9 %dynamic-slice_dynamic-update-slice_fusion.2 = bf16[1024,2048]{1,0:T(8,128)(2,1)} fusion(bf16[1024,2048]{1,0:T(8,128)(2,1)} %dynamic-slice_dynamic-update-slice_fusion.3, bf16[1024,2048]{1,0:T(8,128)(2,1)} %param.4, s32[]{:T(128)S(6)} %select_n.99), kind=kLoop, calls=%fused_computation.21 | loop fusion | bytes 1048580
  97.1 1.9 %dynamic-slice_dynamic-update-slice_fusion.1 = bf16[1024,2048]{1,0:T(8,128)(2,1)} fusion(bf16[1024,2048]{1,0:T(8,128)(2,1)} %dynamic-slice_dynamic-update-slice_fusion.2, bf16[1024,2048]{1,0:T(8,128)(2,1)} %param.4, s32[]{:T(128)S(6)} %select_n.100), kind=kLoop, calls=%fused_computation.20 | loop fusion | bytes 1048580
  99.0 1.9 %dynamic-slice_dynamic-update-slice_fusion = bf16[1024,2048]{1,0:T(8,128)(2,1)} fusion(bf16[1024,2048]{1,0:T(8,128)(2,1)} %dynamic-slice_dynamic-update-slice_fusion.1, bf16[1024,2048]{1,0:T(8,128)(2,1)} %param.4, s32[]{:T(128)S(6)} %select_n.101), kind=kLoop, calls=%fused_computation.19 | loop fusion | bytes 1048580 | tf_op jit(solution)/shard_map/concatenate | solution.py:126
  100.9 2.7 %collective-permute-done.10.refs_10_.refs_1_ = bf16[256,1024]{1,0:T(8,128)(2,1)} collective-permute-done((bf16[256,1024]{1,0:T(8,128)(2,1)}, bf16[256,1024]{1,0:T(8,128)(2,1)}, u32[]{:S(2)}, u32[]{:S(2)}) %collective-permute-start.10) | collective-permute-done | bytes 524320 | tf_op jit(solution)/shard_map/ppermute | solution.py:89
  103.6 3.7 %collective-permute-start.11 = (bf16[256,1024]{1,0:T(8,128)(2,1)}, bf16[256,1024]{1,0:T(8,128)(2,1)S(1)}, u32[]{:S(2)}, u32[]{:S(2)}) collective-permute-start(bf16[256,1024]{1,0:T(8,128)(2,1)} %collective-permute-done.10.refs_10_.refs_1_), channel_id=1, source_target_pairs={{0,120},{8,0},{16,8},{24,16},{32,24},{40,32},{48,40},{56,48},{64,5... | collective-permute-start | bytes 1572872 | tf_op jit(solution)/shard_map/ppermute | solution.py:89
  107.3 3.1 %fusion = f32[1024]{0:T(1024)S(1)} fusion(bf16[1024,2048]{1,0:T(8,128)(2,1)} %dynamic-slice_dynamic-update-slice_fusion), kind=kLoop, calls=%fused_computation.2 | loop fusion | flops 6290432 | bytes 4198400 | tf_op jit(solution)/shard_map/reduce_sum | solution.py:127
  110.4 6.1 %collective-permute-done.11.refs_1_ = bf16[256,1024]{1,0:T(8,128)(2,1)S(1)} collective-permute-done((bf16[256,1024]{1,0:T(8,128)(2,1)}, bf16[256,1024]{1,0:T(8,128)(2,1)S(1)}, u32[]{:S(2)}, u32[]{:S(2)}) %collective-permute-start.11) | collective-permute-done | bytes 524320 | tf_op jit(solution)/shard_map/ppermute | solution.py:89
  116.5 3.6 %collective-permute-start.13 = (bf16[256,1024]{1,0:T(8,128)(2,1)S(1)}, bf16[256,1024]{1,0:T(8,128)(2,1)S(1)}, u32[]{:S(2)}, u32[]{:S(2)}) collective-permute-start(bf16[256,1024]{1,0:T(8,128)(2,1)S(1)} %collective-permute-done.11.refs_1_), channel_id=1, source_target_pairs={{0,120},{8,0},{16,8},{24,16},{32,24},{40,32},{48,40},{56,48},{64,5... | collective-permute-start | bytes 1572872 | tf_op jit(solution)/shard_map/ppermute | solution.py:89
  120.0 0.2 collective-permute-done.5.refs_0_
  120.3 4.9 %fusion.1 = bf16[1024,2048]{1,0:T(8,128)(2,1)} fusion(bf16[1024,2048]{1,0:T(8,128)(2,1)} %dynamic-slice_dynamic-update-slice_fusion, f32[1024]{0:T(1024)S(1)} %add_rsqrt_fusion), kind=kLoop, calls=%fused_computation.3 | loop fusion | flops 6291456 | bytes 8392704 | tf_op jit(solution)/shard_map/convert_element_type | solution.py:128
  125.2 2.3 %slice.133 = bf16[1024,512]{1,0:T(8,128)(2,1)} slice(bf16[1024,2048]{1,0:T(8,128)(2,1)} %fusion.1), slice={[0:1024], [0:512]} | slice | bytes 2097152 | tf_op jit(solution)/shard_map/slice | solution.py:139
  127.5 1.9 %fusion.4 = bf16[1024,640]{1,0:T(8,128)(2,1)S(1)} fusion(s32[]{:T(128)S(6)} %select_n.103, bf16[1024,2048]{1,0:T(8,128)(2,1)} %fusion.1, bf16[1024,512]{1,0:T(8,128)(2,1)} %slice.133), kind=kLoop, calls=%fused_computation.13 | loop fusion | flops 2621440 | bytes 6553604 | tf_op jit(solution)/shard_map/concatenate | solution.py:139
  129.4 2.9 %shard_map.69.refs_2_ = bf16[1024,2048]{1,0:T(8,128)(2,1)} custom-call(s32[1]{0:T(128)} %bitcast.z_ref, bf16[256,1024]{1,0:T(8,128)(2,1)S(1)} %pad_maximum_fusion.1.refs_0_, bf16[256,1024]{1,0:T(8,128)(2,1)S(1)} %copy-done.1, bf16[256,1024]{1,0:T(8,128)(2,1)S(1)} %collective-permute-done.6.refs_2_, bf16[256,1024]{1,0:T(8,128)(2,1)S(1)} %copy-done.5, ...), custom_call_target="tpu_custom_call" | custom-call | tf_op jit(solution)/shard_map/pallas_call | solution.py:38
  132.4 4.0 %shard_map.67.refs_5_ = bf16[2048,1024]{1,0:T(8,128)(2,1)} custom-call(s32[1]{0:T(128)} %bitcast.z_ref, bf16[256,1024]{1,0:T(8,128)(2,1)S(1)} %pad_maximum_fusion.1.refs_0_, bf16[256,1024]{1,0:T(8,128)(2,1)S(1)} %copy-done.1, bf16[256,1024]{1,0:T(8,128)(2,1)S(1)} %collective-permute-done.6.refs_2_, bf16[256,1024]{1,0:T(8,128)(2,1)S(1)} %copy-done.5, ...), custom_call_target="tpu_custom_call" | custom-call | tf_op jit(solution)/shard_map/pallas_call | solution.py:38
  136.4 0.1 dynamic_update_slice.33
  136.7 0.1 collective-permute-start.14
  136.8 6.3 %fusion.25 = f32[1024,1024]{1,0:T(8,128)S(1)} fusion(bf16[1024,2048]{1,0:T(8,128)(2,1)S(1)} %copy-done.9, bf16[2048,1024]{1,0:T(8,128)(2,1)} %shard_map.67.refs_5_), kind=kOutput, calls=%fused_computation.56 | convolution fusion | flops 4294967296 | bytes 12582912 | tf_op jit(solution)/shard_map/dot_general | solution.py:129
  143.1 2.0 %shard_map.70.refs_4_ = bf16[1024,2048]{1,0:T(8,128)(2,1)} custom-call(s32[1]{0:T(128)} %bitcast.z_ref, bf16[256,1024]{1,0:T(8,128)(2,1)} %collective-permute-done.4.refs_9_.refs_0_, bf16[256,1024]{1,0:T(8,128)(2,1)} %collective-permute-done.10.refs_10_.refs_1_, bf16[1024,2048]{1,0:T(8,128)(2,1)} %shard_map.69.refs_2_), custom_call_target="tpu_custom_call", output_to_operand_aliasing={{}: (3, {})} | custom-call | tf_op jit(solution)/shard_map/pallas_call | solution.py:38
  145.2 3.3 %collective-permute-start.15 = (bf16[128,1024]{1,0:T(8,128)(2,1)S(1)}, bf16[128,1024]{1,0:T(8,128)(2,1)S(1)}, u32[]{:S(2)}, u32[]{:S(2)}) collective-permute-start(bf16[128,1024]{1,0:T(8,128)(2,1)S(1)} %get-tuple-element.22), channel_id=1, source_target_pairs={{0,120},{8,0},{16,8},{24,16},{32,24},{40,32},{48,40},{56,48},{64,5... | collective-permute-start | bytes 786440 | tf_op jit(solution)/shard_map/ppermute | solution.py:91
  148.5 1.0 shard_map.71.refs_1_
  149.6 1.8 fusion.26
  151.4 1.1 multiply_convert_fusion
  152.5 0.7 shard_map.72
  153.3 3.4 %convolution_convert_fusion.1 = bf16[1024,768]{1,0:T(8,128)(2,1)S(1)} fusion(bf16[1024,1024]{1,0:T(8,128)(2,1)S(1)} %multiply_convert_fusion, bf16[1024,2048]{1,0:T(8,128)(2,1)} %shard_map.72), kind=kOutput, calls=%fused_computation.10 | convolution fusion | flops 1611399168 | bytes 5242880 | tf_op jit(solution)/shard_map/dot_general | solution.py:162
  156.7 0.4 collective-permute-start.21
  157.1 3.2 %convolution_convert_fusion = bf16[1024,1280]{1,0:T(8,128)(2,1)S(1)} fusion(bf16[1024,1024]{1,0:T(8,128)(2,1)S(1)} %multiply_convert_fusion, bf16[1024,2048]{1,0:T(8,128)(2,1)S(1)} %copy-done.8), kind=kOutput, calls=%fused_computation.7 | convolution fusion | flops 2685665280 | bytes 7340032 | tf_op jit(solution)/shard_map/dot_general | solution.py:162
  160.3 0.6 collective-permute-start.16
  160.9 1.1 shard_map.68
  162.0 0.2 convert_add_fusion.1
  162.3 0.7 collective-permute-start.22
  162.9 2.7 %collective-permute-start.24 = (bf16[128,384]{1,0:T(8,128)(2,1)S(1)}, bf16[128,384]{1,0:T(8,128)(2,1)S(1)}, u32[]{:S(2)}, u32[]{:S(2)}) collective-permute-start(bf16[128,384]{1,0:T(8,128)(2,1)S(1)} %get-tuple-element.16), channel_id=1, source_target_pairs={{0,6},{1,7},{2,0},{3,1},{4,2},{5,3},{6,4},{7,5},{8,14},{9,15},{10,... | collective-permute-start | bytes 294920 | tf_op jit(solution)/shard_map/ppermute | solution.py:170
  165.6 0.3 fusion.19
  166.0 0.1 collective-permute-start.17
  166.1 3.2 %collective-permute-start.19 = (bf16[128,640]{1,0:T(8,128)(2,1)S(1)}, bf16[128,640]{1,0:T(8,128)(2,1)S(1)}, u32[]{:S(2)}, u32[]{:S(2)}) collective-permute-start(bf16[128,640]{1,0:T(8,128)(2,1)S(1)} %get-tuple-element.12), channel_id=1, source_target_pairs={{0,6},{1,7},{2,0},{3,1},{4,2},{5,3},{6,4},{7,5},{8,14},{9,15},{10,... | collective-permute-start | bytes 491528 | tf_op jit(solution)/shard_map/ppermute | solution.py:170
  169.4 3.5 %collective-permute-done.17 = bf16[128,640]{1,0:T(8,128)(2,1)S(1)} collective-permute-done((bf16[128,640]{1,0:T(8,128)(2,1)S(1)}, bf16[128,640]{1,0:T(8,128)(2,1)S(1)}, u32[]{:S(2)}, u32[]{:S(2)}) %collective-permute-start.17) | collective-permute-done | bytes 163872 | tf_op jit(solution)/shard_map/ppermute | solution.py:169
  173.1 3.2 %collective-permute-start.20 = (bf16[128,1280]{1,0:T(8,128)(2,1)S(1)}, bf16[128,1280]{1,0:T(8,128)(2,1)S(1)}, u32[]{:S(2)}, u32[]{:S(2)}) collective-permute-start(bf16[128,1280]{1,0:T(8,128)(2,1)S(1)} %get-tuple-element.6), channel_id=1, source_target_pairs={{0,6},{1,7},{2,0},{3,1},{4,2},{5,3},{6,4},{7,5},{8,14},{9,15},{10,... | collective-permute-start | bytes 983048 | tf_op jit(solution)/shard_map/ppermute | solution.py:176
  176.4 0.1 collective-permute-start.23
  176.6 3.2 %collective-permute-start.25 = (bf16[128,768]{1,0:T(8,128)(2,1)S(1)}, bf16[128,768]{1,0:T(8,128)(2,1)S(1)}, u32[]{:S(2)}, u32[]{:S(2)}) collective-permute-start(bf16[128,768]{1,0:T(8,128)(2,1)S(1)} %get-tuple-element.10), channel_id=1, source_target_pairs={{0,6},{1,7},{2,0},{3,1},{4,2},{5,3},{6,4},{7,5},{8,14},{9,15},{10,... | collective-permute-start | bytes 589832 | tf_op jit(solution)/shard_map/ppermute | solution.py:176
  179.8 4.9 %collective-permute-done.18 = bf16[128,1280]{1,0:T(8,128)(2,1)S(1)} collective-permute-done((bf16[128,1280]{1,0:T(8,128)(2,1)S(1)}, bf16[128,1280]{1,0:T(8,128)(2,1)S(1)}, u32[]{:S(2)}, u32[]{:S(2)}) %collective-permute-start.18) | collective-permute-done | bytes 327712 | tf_op jit(solution)/shard_map/ppermute | solution.py:175
  184.8 1.9 %collective-permute-done.23 = bf16[128,768]{1,0:T(8,128)(2,1)S(1)} collective-permute-done((bf16[128,768]{1,0:T(8,128)(2,1)S(1)}, bf16[128,768]{1,0:T(8,128)(2,1)S(1)}, u32[]{:S(2)}, u32[]{:S(2)}) %collective-permute-start.23) | collective-permute-done | bytes 196640 | tf_op jit(solution)/shard_map/ppermute | solution.py:175
  186.9 0.8 copy-done.10
  (70 shorter events, 1.3 us)
Async XLA Ops:
  19.7 33.3 %collective-permute-start.6 = (bf16[256,1024]{1,0:T(8,128)(2,1)S(1)}, bf16[256,1024]{1,0:T(8,128)(2,1)S(1)}, u32[]{:S(2)}, u32[]{:S(2)}) collective-permute-start(bf16[256,1024]{1,0:T(8,128)(2,1)S(1)} %pad_maximum_fusion.1.refs_0_), channel_id=1, source_target_pairs={{0,120},{8,0},{16,8},{24,16},{32,24},{40,32},{48,40},{56,48},{64,5... | collective-permute-start | bytes 1572872 | tf_op jit(solution)/shard_map/ppermute | solution.py:89
  42.2 14.5 %collective-permute-start = (bf16[256,1024]{1,0:T(8,128)(2,1)S(1)}, bf16[256,1024]{1,0:T(8,128)(2,1)S(1)}, u32[]{:S(2)}, u32[]{:S(2)}) collective-permute-start(bf16[256,1024]{1,0:T(8,128)(2,1)S(1)} %pad_maximum_fusion.1.refs_0_), channel_id=1, source_target_pairs={{0,8},{8,16},{16,24},{24,32},{32,40},{40,48},{48,56},{56,64},{64,7... | collective-permute-start | bytes 1572872 | tf_op jit(solution)/shard_map/ppermute | solution.py:88
  53.0 13.7 %collective-permute-start.7 = (bf16[256,1024]{1,0:T(8,128)(2,1)S(1)}, bf16[256,1024]{1,0:T(8,128)(2,1)S(1)}, u32[]{:S(2)}, u32[]{:S(2)}) collective-permute-start(bf16[256,1024]{1,0:T(8,128)(2,1)S(1)} %collective-permute-done.6.refs_2_), channel_id=1, source_target_pairs={{0,120},{8,0},{16,8},{24,16},{32,24},{40,32},{48,40},{56,48},{64,5... | collective-permute-start | bytes 1572872 | tf_op jit(solution)/shard_map/ppermute | solution.py:89
  56.7 44.1 %copy-start = (bf16[256,1024]{1,0:T(8,128)(2,1)}, bf16[256,1024]{1,0:T(8,128)(2,1)S(1)}, u32[]{:S(2)}) copy-start(bf16[256,1024]{1,0:T(8,128)(2,1)S(1)} %collective-permute-done.refs_1_) | copy-start | bytes 1572868
  56.7 13.7 %collective-permute-start.1 = (bf16[256,1024]{1,0:T(8,128)(2,1)S(1)}, bf16[256,1024]{1,0:T(8,128)(2,1)S(1)}, u32[]{:S(2)}, u32[]{:S(2)}) collective-permute-start(bf16[256,1024]{1,0:T(8,128)(2,1)S(1)} %collective-permute-done.refs_1_), channel_id=1, source_target_pairs={{0,8},{8,16},{16,24},{24,32},{32,40},{40,48},{48,56},{56,64},{64,7... | collective-permute-start | bytes 1572872 | tf_op jit(solution)/shard_map/ppermute | solution.py:88
  66.7 34.2 %copy-start.2 = (bf16[256,1024]{1,0:T(8,128)(2,1)}, bf16[256,1024]{1,0:T(8,128)(2,1)S(1)}, u32[]{:S(2)}) copy-start(bf16[256,1024]{1,0:T(8,128)(2,1)S(1)} %collective-permute-done.7.refs_4_) | copy-start | bytes 1572868
  66.7 12.8 %collective-permute-start.8 = (bf16[256,1024]{1,0:T(8,128)(2,1)S(1)}, bf16[256,1024]{1,0:T(8,128)(2,1)S(1)}, u32[]{:S(2)}, u32[]{:S(2)}) collective-permute-start(bf16[256,1024]{1,0:T(8,128)(2,1)S(1)} %collective-permute-done.7.refs_4_), channel_id=1, source_target_pairs={{0,120},{8,0},{16,8},{24,16},{32,24},{40,32},{48,40},{56,48},{64,5... | collective-permute-start | bytes 1572872 | tf_op jit(solution)/shard_map/ppermute | solution.py:89
  70.4 30.5 %copy-start.4 = (bf16[256,1024]{1,0:T(8,128)(2,1)}, bf16[256,1024]{1,0:T(8,128)(2,1)S(1)}, u32[]{:S(2)}) copy-start(bf16[256,1024]{1,0:T(8,128)(2,1)S(1)} %collective-permute-done.1.refs_3_) | copy-start | bytes 1572868
  70.4 12.8 %collective-permute-start.2 = (bf16[256,1024]{1,0:T(8,128)(2,1)S(1)}, bf16[256,1024]{1,0:T(8,128)(2,1)}, u32[]{:S(2)}, u32[]{:S(2)}) collective-permute-start(bf16[256,1024]{1,0:T(8,128)(2,1)S(1)} %collective-permute-done.1.refs_3_), channel_id=1, source_target_pairs={{0,8},{8,16},{16,24},{24,32},{32,40},{40,48},{48,56},{56,64},{64,7... | collective-permute-start | bytes 1572872 | tf_op jit(solution)/shard_map/ppermute | solution.py:88
  79.5 30.9 %copy-start.6 = (bf16[256,1024]{1,0:T(8,128)(2,1)}, bf16[256,1024]{1,0:T(8,128)(2,1)S(1)}, u32[]{:S(2)}) copy-start(bf16[256,1024]{1,0:T(8,128)(2,1)S(1)} %collective-permute-done.8.refs_6_) | copy-start | bytes 1572868
  79.5 11.9 %collective-permute-start.9 = (bf16[256,1024]{1,0:T(8,128)(2,1)S(1)}, bf16[256,1024]{1,0:T(8,128)(2,1)}, u32[]{:S(2)}, u32[]{:S(2)}) collective-permute-start(bf16[256,1024]{1,0:T(8,128)(2,1)S(1)} %collective-permute-done.8.refs_6_), channel_id=1, source_target_pairs={{0,120},{8,0},{16,8},{24,16},{32,24},{40,32},{48,40},{56,48},{64,5... | collective-permute-start | bytes 1572872 | tf_op jit(solution)/shard_map/ppermute | solution.py:89
  83.2 12.0 %collective-permute-start.3 = (bf16[256,1024]{1,0:T(8,128)(2,1)}, bf16[256,1024]{1,0:T(8,128)(2,1)}, u32[]{:S(2)}, u32[]{:S(2)}) collective-permute-start(bf16[256,1024]{1,0:T(8,128)(2,1)} %collective-permute-done.2.refs_5_), channel_id=1, source_target_pairs={{0,8},{8,16},{16,24},{24,32},{32,40},{40,48},{48,56},{56,64},{64,7... | collective-permute-start | bytes 1572872 | tf_op jit(solution)/shard_map/ppermute | solution.py:88
  91.4 12.2 %collective-permute-start.10 = (bf16[256,1024]{1,0:T(8,128)(2,1)}, bf16[256,1024]{1,0:T(8,128)(2,1)}, u32[]{:S(2)}, u32[]{:S(2)}) collective-permute-start(bf16[256,1024]{1,0:T(8,128)(2,1)} %collective-permute-done.9.refs_8_), channel_id=1, source_target_pairs={{0,120},{8,0},{16,8},{24,16},{32,24},{40,32},{48,40},{56,48},{64,5... | collective-permute-start | bytes 1572872 | tf_op jit(solution)/shard_map/ppermute | solution.py:89
  95.2 12.1 %collective-permute-start.4 = (bf16[256,1024]{1,0:T(8,128)(2,1)}, bf16[256,1024]{1,0:T(8,128)(2,1)}, u32[]{:S(2)}, u32[]{:S(2)}) collective-permute-start(bf16[256,1024]{1,0:T(8,128)(2,1)} %collective-permute-done.3.refs_7_), channel_id=1, source_target_pairs={{0,8},{8,16},{16,24},{24,32},{32,40},{40,48},{48,56},{56,64},{64,7... | collective-permute-start | bytes 1572872 | tf_op jit(solution)/shard_map/ppermute | solution.py:88
  103.6 12.9 %collective-permute-start.11 = (bf16[256,1024]{1,0:T(8,128)(2,1)}, bf16[256,1024]{1,0:T(8,128)(2,1)S(1)}, u32[]{:S(2)}, u32[]{:S(2)}) collective-permute-start(bf16[256,1024]{1,0:T(8,128)(2,1)} %collective-permute-done.10.refs_10_.refs_1_), channel_id=1, source_target_pairs={{0,120},{8,0},{16,8},{24,16},{32,24},{40,32},{48,40},{56,48},{64,5... | collective-permute-start | bytes 1572872 | tf_op jit(solution)/shard_map/ppermute | solution.py:89
  107.3 13.0 %collective-permute-start.5 = (bf16[256,1024]{1,0:T(8,128)(2,1)}, bf16[256,1024]{1,0:T(8,128)(2,1)S(1)}, u32[]{:S(2)}, u32[]{:S(2)}) collective-permute-start(bf16[256,1024]{1,0:T(8,128)(2,1)} %collective-permute-done.4.refs_9_.refs_0_), channel_id=1, source_target_pairs={{0,8},{8,16},{16,24},{24,32},{32,40},{40,48},{48,56},{56,64},{64,7... | collective-permute-start | bytes 1572872 | tf_op jit(solution)/shard_map/ppermute | solution.py:88
  116.5 20.1 %collective-permute-start.13 = (bf16[256,1024]{1,0:T(8,128)(2,1)S(1)}, bf16[256,1024]{1,0:T(8,128)(2,1)S(1)}, u32[]{:S(2)}, u32[]{:S(2)}) collective-permute-start(bf16[256,1024]{1,0:T(8,128)(2,1)S(1)} %collective-permute-done.11.refs_1_), channel_id=1, source_target_pairs={{0,120},{8,0},{16,8},{24,16},{32,24},{40,32},{48,40},{56,48},{64,5... | collective-permute-start | bytes 1572872 | tf_op jit(solution)/shard_map/ppermute | solution.py:89
  120.3 16.3 %collective-permute-start.12 = (bf16[256,1024]{1,0:T(8,128)(2,1)S(1)}, bf16[256,1024]{1,0:T(8,128)(2,1)S(1)}, u32[]{:S(2)}, u32[]{:S(2)}) collective-permute-start(bf16[256,1024]{1,0:T(8,128)(2,1)S(1)} %collective-permute-done.5.refs_0_), channel_id=1, source_target_pairs={{0,8},{8,16},{16,24},{24,32},{32,40},{40,48},{48,56},{56,64},{64,7... | collective-permute-start | bytes 1572872 | tf_op jit(solution)/shard_map/ppermute | solution.py:88
  127.4 2.0 %copy-start.1 = (bf16[256,1024]{1,0:T(8,128)(2,1)S(1)}, bf16[256,1024]{1,0:T(8,128)(2,1)}, u32[]{:S(2)}) copy-start(bf16[256,1024]{1,0:T(8,128)(2,1)} %copy-done) | copy-start | bytes 1572868
  127.4 2.0 %copy-start.3 = (bf16[256,1024]{1,0:T(8,128)(2,1)S(1)}, bf16[256,1024]{1,0:T(8,128)(2,1)}, u32[]{:S(2)}) copy-start(bf16[256,1024]{1,0:T(8,128)(2,1)} %copy-done.2) | copy-start | bytes 1572868
  127.4 2.0 %copy-start.5 = (bf16[256,1024]{1,0:T(8,128)(2,1)S(1)}, bf16[256,1024]{1,0:T(8,128)(2,1)}, u32[]{:S(2)}) copy-start(bf16[256,1024]{1,0:T(8,128)(2,1)} %copy-done.4) | copy-start | bytes 1572868
  127.4 2.0 %copy-start.7 = (bf16[256,1024]{1,0:T(8,128)(2,1)S(1)}, bf16[256,1024]{1,0:T(8,128)(2,1)}, u32[]{:S(2)}) copy-start(bf16[256,1024]{1,0:T(8,128)(2,1)} %copy-done.6) | copy-start | bytes 1572868
  132.4 4.4 %copy-start.9 = (bf16[1024,2048]{1,0:T(8,128)(2,1)S(1)}, bf16[1024,2048]{1,0:T(8,128)(2,1)}, u32[]{:S(2)}) copy-start(bf16[1024,2048]{1,0:T(8,128)(2,1)} %fusion.1) | copy-start | bytes 12582916
  136.7 12.9 %collective-permute-start.14 = (bf16[128,1024]{1,0:T(8,128)(2,1)S(1)}, bf16[128,1024]{1,0:T(8,128)(2,1)S(1)}, u32[]{:S(2)}, u32[]{:S(2)}) collective-permute-start(bf16[128,1024]{1,0:T(8,128)(2,1)S(1)} %get-tuple-element.20), channel_id=1, source_target_pairs={{0,8},{8,16},{16,24},{24,32},{32,40},{40,48},{48,56},{56,64},{64,7... | collective-permute-start | bytes 786440 | tf_op jit(solution)/shard_map/ppermute | solution.py:90
  145.2 7.3 %collective-permute-start.15 = (bf16[128,1024]{1,0:T(8,128)(2,1)S(1)}, bf16[128,1024]{1,0:T(8,128)(2,1)S(1)}, u32[]{:S(2)}, u32[]{:S(2)}) collective-permute-start(bf16[128,1024]{1,0:T(8,128)(2,1)S(1)} %get-tuple-element.22), channel_id=1, source_target_pairs={{0,120},{8,0},{16,8},{24,16},{32,24},{40,32},{48,40},{56,48},{64,5... | collective-permute-start | bytes 786440 | tf_op jit(solution)/shard_map/ppermute | solution.py:91
  153.3 3.8 %copy-start.8 = (bf16[1024,2048]{1,0:T(8,128)(2,1)S(1)}, bf16[1024,2048]{1,0:T(8,128)(2,1)}, u32[]{:S(2)}) copy-start(bf16[1024,2048]{1,0:T(8,128)(2,1)} %shard_map.72) | copy-start | bytes 12582916
  156.7 5.3 %collective-permute-start.21 = (bf16[512,768]{1,0:T(8,128)(2,1)S(1)}, bf16[512,768]{1,0:T(8,128)(2,1)S(1)}, u32[]{:S(2)}, u32[]{:S(2)}) collective-permute-start(bf16[512,768]{1,0:T(8,128)(2,1)S(1)} %slice.149), channel_id=1, source_target_pairs={{0,1},{1,0},{2,3},{3,2},{4,5},{5,4},{6,7},{7,6},{8,9},{9,8},{10,11... | collective-permute-start | bytes 2359304 | tf_op jit(solution)/shard_map/ppermute | solution.py:163
  160.3 5.3 %collective-permute-start.16 = (bf16[512,1280]{1,0:T(8,128)(2,1)S(1)}, bf16[512,1280]{1,0:T(8,128)(2,1)S(1)}, u32[]{:S(2)}, u32[]{:S(2)}) collective-permute-start(bf16[512,1280]{1,0:T(8,128)(2,1)S(1)} %slice.139), channel_id=1, source_target_pairs={{0,1},{1,0},{2,3},{3,2},{4,5},{5,4},{6,7},{7,6},{8,9},{9,8},{10,11... | collective-permute-start | bytes 3932168 | tf_op jit(solution)/shard_map/ppermute | solution.py:163
  162.3 14.1 %collective-permute-start.22 = (bf16[128,384]{1,0:T(8,128)(2,1)S(1)}, bf16[128,384]{1,0:T(8,128)(2,1)S(1)}, u32[]{:S(2)}, u32[]{:S(2)}) collective-permute-start(bf16[128,384]{1,0:T(8,128)(2,1)S(1)} %get-tuple-element.15), channel_id=1, source_target_pairs={{0,2},{1,3},{2,4},{3,5},{4,6},{5,7},{6,0},{7,1},{8,10},{9,11},{10,... | collective-permute-start | bytes 294920 | tf_op jit(solution)/shard_map/ppermute | solution.py:169
  162.9 13.4 %collective-permute-start.24 = (bf16[128,384]{1,0:T(8,128)(2,1)S(1)}, bf16[128,384]{1,0:T(8,128)(2,1)S(1)}, u32[]{:S(2)}, u32[]{:S(2)}) collective-permute-start(bf16[128,384]{1,0:T(8,128)(2,1)S(1)} %get-tuple-element.16), channel_id=1, source_target_pairs={{0,6},{1,7},{2,0},{3,1},{4,2},{5,3},{6,4},{7,5},{8,14},{9,15},{10,... | collective-permute-start | bytes 294920 | tf_op jit(solution)/shard_map/ppermute | solution.py:170
  166.0 6.9 %collective-permute-start.17 = (bf16[128,640]{1,0:T(8,128)(2,1)S(1)}, bf16[128,640]{1,0:T(8,128)(2,1)S(1)}, u32[]{:S(2)}, u32[]{:S(2)}) collective-permute-start(bf16[128,640]{1,0:T(8,128)(2,1)S(1)} %get-tuple-element.11), channel_id=1, source_target_pairs={{0,2},{1,3},{2,4},{3,5},{4,6},{5,7},{6,0},{7,1},{8,10},{9,11},{10,... | collective-permute-start | bytes 491528 | tf_op jit(solution)/shard_map/ppermute | solution.py:169
  166.1 6.8 %collective-permute-start.19 = (bf16[128,640]{1,0:T(8,128)(2,1)S(1)}, bf16[128,640]{1,0:T(8,128)(2,1)S(1)}, u32[]{:S(2)}, u32[]{:S(2)}) collective-permute-start(bf16[128,640]{1,0:T(8,128)(2,1)S(1)} %get-tuple-element.12), channel_id=1, source_target_pairs={{0,6},{1,7},{2,0},{3,1},{4,2},{5,3},{6,4},{7,5},{8,14},{9,15},{10,... | collective-permute-start | bytes 491528 | tf_op jit(solution)/shard_map/ppermute | solution.py:170
  173.0 11.7 %collective-permute-start.18 = (bf16[128,1280]{1,0:T(8,128)(2,1)S(1)}, bf16[128,1280]{1,0:T(8,128)(2,1)S(1)}, u32[]{:S(2)}, u32[]{:S(2)}) collective-permute-start(bf16[128,1280]{1,0:T(8,128)(2,1)S(1)} %get-tuple-element.5), channel_id=1, source_target_pairs={{0,2},{1,3},{2,4},{3,5},{4,6},{5,7},{6,0},{7,1},{8,10},{9,11},{10,... | collective-permute-start | bytes 983048 | tf_op jit(solution)/shard_map/ppermute | solution.py:175
  173.1 11.5 %collective-permute-start.20 = (bf16[128,1280]{1,0:T(8,128)(2,1)S(1)}, bf16[128,1280]{1,0:T(8,128)(2,1)S(1)}, u32[]{:S(2)}, u32[]{:S(2)}) collective-permute-start(bf16[128,1280]{1,0:T(8,128)(2,1)S(1)} %get-tuple-element.6), channel_id=1, source_target_pairs={{0,6},{1,7},{2,0},{3,1},{4,2},{5,3},{6,4},{7,5},{8,14},{9,15},{10,... | collective-permute-start | bytes 983048 | tf_op jit(solution)/shard_map/ppermute | solution.py:176
  176.4 10.3 %collective-permute-start.23 = (bf16[128,768]{1,0:T(8,128)(2,1)S(1)}, bf16[128,768]{1,0:T(8,128)(2,1)S(1)}, u32[]{:S(2)}, u32[]{:S(2)}) collective-permute-start(bf16[128,768]{1,0:T(8,128)(2,1)S(1)} %get-tuple-element.9), channel_id=1, source_target_pairs={{0,2},{1,3},{2,4},{3,5},{4,6},{5,7},{6,0},{7,1},{8,10},{9,11},{10,... | collective-permute-start | bytes 589832 | tf_op jit(solution)/shard_map/ppermute | solution.py:175
  176.6 10.2 %collective-permute-start.25 = (bf16[128,768]{1,0:T(8,128)(2,1)S(1)}, bf16[128,768]{1,0:T(8,128)(2,1)S(1)}, u32[]{:S(2)}, u32[]{:S(2)}) collective-permute-start(bf16[128,768]{1,0:T(8,128)(2,1)S(1)} %get-tuple-element.10), channel_id=1, source_target_pairs={{0,6},{1,7},{2,0},{3,1},{4,2},{5,3},{6,4},{7,5},{8,14},{9,15},{10,... | collective-permute-start | bytes 589832 | tf_op jit(solution)/shard_map/ppermute | solution.py:176
  186.8 0.8 copy-start.10

commit v6 on v5

--- a/solution.py
+++ b/solution.py
@@ -155,13 +155,16 @@
     pair = [(k, k ^ 1) for k in range(n_tp)]
     right = [(j, (j + 2) % n_tp) for j in range(n_tp)]
     left = [(j, (j - 2) % n_tp) for j in range(n_tp)]
-    bounds = [0, 5 * full // 8, full]
+    bounds = [0, 3 * full // 8, full]
     summed = jnp.zeros((block, full), jnp.bfloat16)
     for lo, hi in zip(bounds[:-1], bounds[1:]):
         weights = lax.slice_in_dim(down_sampler, lo, hi, axis=1)
-        partial = jnp.dot(hidden, weights, preferred_element_type=jnp.float32).astype(jnp.bfloat16)
-        theirs = lax.ppermute(partial[: tokens // 2], "tp", pair)
-        chip = partial[tokens // 2 :].astype(jnp.float32) + theirs.astype(jnp.float32)
+        theirs = jnp.dot(hidden[: tokens // 2], weights, preferred_element_type=jnp.float32)
+        theirs = theirs.astype(jnp.bfloat16)
+        theirs = lax.ppermute(theirs, "tp", pair)
+        mine = jnp.dot(hidden[tokens // 2 :], weights, preferred_element_type=jnp.float32)
+        mine = lax.optimization_barrier(mine.astype(jnp.bfloat16))
+        chip = mine.astype(jnp.float32) + theirs.astype(jnp.float32)
         after, across, before, total = [chip[j * block : (j + 1) * block] for j in range(n_x)]
         across = across.astype(jnp.bfloat16)
         mid = (hi - lo) // 2

time: 188 us -> 190 us (1.011)
    ppermute x2, waiting for transfers between devices: 3.53 us -> 6.36 us  [on_device(): first = lax.ppermute(ends[0], 'tp', right).astype(jnp.float32)]
    dot_general x2 -> x4, matrix products: 6.52 us -> 6.63 us  [the longest x2 4.1 us: on_device(): jnp.dot(hidden[:tokens // 2], weights, preferred_element_type=jnp.float32)]
where the time goes in v6:
time: 190 us; the launch traced here: 189 us
  starting transfers between devices  62.5 us (33%)
  waiting for transfers between devices  49.1 us (26%)
  local copies, waits for them, and re-layouts  21.2 us (11%)
  blocking collectives  14.7 us (8%)
  matrix products  14.7 us (8%)
  other arithmetic  13.7 us (7%)
  Pallas kernels  11.7 us (6%)
    ppermute x7, starting transfers between devices, on_device(): held[step] = lax.ppermute(held[step - 1], 'fs', back)  44.6 us
    ppermute x7, waiting for transfers between devices, on_device(): held[step] = lax.ppermute(held[step - 1], 'fs', back)  37.3 us
    unnamed x31, local copies, waits for them, and re-layouts  15.6 us
    all_to_all x1, blocking collectives, on_device(): parts = lax.all_to_all(parts, 'tp', split_axis=0, concat_axis=0, tiled=True)  14.7 us
    pallas_call x6, Pallas kernels, place(): pl.pallas_call(body, out_shape=outs, in_specs=[pl.BlockSpec(memory_space=...  11.7 us
    ppermute x2, waiting for transfers between devices, on_device(): first = lax.ppermute(ends[0], 'tp', right).astype(jnp.float32)  6.36 us
    dot_general x1, matrix products, on_device(): pre_act = jnp.dot(normed, up_sampler[0], preferred_element_type=jnp.float32)  6.3 us
    ppermute x2, starting transfers between devices, on_device(): second = lax.ppermute(ends[1], 'tp', left).astype(jnp.float32)  5.88 us
  transfers between devices with their start and end apart: 26, of which 10 were waited for; matrix products, arithmetic and copies ran while one was open for 22% of the time, Pallas kernels for 6%

profile of v6, /device:TPU:40, one launch (start us, length us, event | category | flops | bytes accessed | tf_op | source)
XLA Modules:
  0.0 188.9 jit_solution(9039457978749532800)
XLA Ops:
  0.6 1.1 convert_element_type.88
  1.8 0.2 copy.35
  2.0 1.2 copy.32
  3.3 0.7 multiply_convert_fusion.1
  4.1 14.7 %all_to_all.5 = bf16[8,2,128,128]{2,3,1,0:T(8,128)(2,1)S(1)} all-to-all(bf16[8,2,128,128]{2,3,1,0:T(8,128)(2,1)S(1)} %copy.36), channel_id=1, replica_groups=mesh['grp'=2,'fs'=16,'tp'=8] {'tp'}, dimensions={0} | all-to-all | bytes 1048576 | tf_op jit(solution)/shard_map/all_to_all | solution.py:77
  19.0 0.2 copy.41
  19.2 0.3 copy.39
  19.5 0.2 reshape.47
  19.7 22.5 %collective-permute-start.6 = (bf16[256,1024]{1,0:T(8,128)(2,1)S(1)}, bf16[256,1024]{1,0:T(8,128)(2,1)S(1)}, u32[]{:S(2)}, u32[]{:S(2)}) collective-permute-start(bf16[256,1024]{1,0:T(8,128)(2,1)S(1)} %pad_maximum_fusion.1.refs_0_), channel_id=1, source_target_pairs={{0,120},{8,0},{16,8},{24,16},{32,24},{40,32},{48,40},{56,48},{64,5... | collective-permute-start | bytes 1572872 | tf_op jit(solution)/shard_map/ppermute | solution.py:89
  42.2 10.8 %collective-permute-done.6.refs_2_ = bf16[256,1024]{1,0:T(8,128)(2,1)S(1)} collective-permute-done((bf16[256,1024]{1,0:T(8,128)(2,1)S(1)}, bf16[256,1024]{1,0:T(8,128)(2,1)S(1)}, u32[]{:S(2)}, u32[]{:S(2)}) %collective-permute-start.6) | collective-permute-done | bytes 524320 | tf_op jit(solution)/shard_map/ppermute | solution.py:89
  53.0 3.7 %collective-permute-start.7 = (bf16[256,1024]{1,0:T(8,128)(2,1)S(1)}, bf16[256,1024]{1,0:T(8,128)(2,1)S(1)}, u32[]{:S(2)}, u32[]{:S(2)}) collective-permute-start(bf16[256,1024]{1,0:T(8,128)(2,1)S(1)} %collective-permute-done.6.refs_2_), channel_id=1, source_target_pairs={{0,120},{8,0},{16,8},{24,16},{32,24},{40,32},{48,40},{56,48},{64,5... | collective-permute-start | bytes 1572872 | tf_op jit(solution)/shard_map/ppermute | solution.py:89
  56.7 9.9 %collective-permute-done.7.refs_4_ = bf16[256,1024]{1,0:T(8,128)(2,1)S(1)} collective-permute-done((bf16[256,1024]{1,0:T(8,128)(2,1)S(1)}, bf16[256,1024]{1,0:T(8,128)(2,1)S(1)}, u32[]{:S(2)}, u32[]{:S(2)}) %collective-permute-start.7) | collective-permute-done | bytes 524320 | tf_op jit(solution)/shard_map/ppermute | solution.py:89
  66.7 3.7 %collective-permute-start.8 = (bf16[256,1024]{1,0:T(8,128)(2,1)S(1)}, bf16[256,1024]{1,0:T(8,128)(2,1)S(1)}, u32[]{:S(2)}, u32[]{:S(2)}) collective-permute-start(bf16[256,1024]{1,0:T(8,128)(2,1)S(1)} %collective-permute-done.7.refs_4_), channel_id=1, source_target_pairs={{0,120},{8,0},{16,8},{24,16},{32,24},{40,32},{48,40},{56,48},{64,5... | collective-permute-start | bytes 1572872 | tf_op jit(solution)/shard_map/ppermute | solution.py:89
  70.5 2.0 %dynamic-slice_dynamic-update-slice_fusion.7 = bf16[1024,2048]{1,0:T(8,128)(2,1)} fusion(bf16[1024,2048]{1,0:T(8,128)(2,1)} %param.4, s32[]{:T(128)S(6)} %select_n.90), kind=kLoop, calls=%fused_computation.34 | loop fusion | bytes 1048580
  72.4 1.9 dynamic-slice_dynamic-update-slice_fusion.6
  74.3 5.1 %collective-permute-done.8.refs_6_ = bf16[256,1024]{1,0:T(8,128)(2,1)S(1)} collective-permute-done((bf16[256,1024]{1,0:T(8,128)(2,1)S(1)}, bf16[256,1024]{1,0:T(8,128)(2,1)S(1)}, u32[]{:S(2)}, u32[]{:S(2)}) %collective-permute-start.8) | collective-permute-done | bytes 524320 | tf_op jit(solution)/shard_map/ppermute | solution.py:89
  79.5 3.7 %collective-permute-start.9 = (bf16[256,1024]{1,0:T(8,128)(2,1)S(1)}, bf16[256,1024]{1,0:T(8,128)(2,1)}, u32[]{:S(2)}, u32[]{:S(2)}) collective-permute-start(bf16[256,1024]{1,0:T(8,128)(2,1)S(1)} %collective-permute-done.8.refs_6_), channel_id=1, source_target_pairs={{0,120},{8,0},{16,8},{24,16},{32,24},{40,32},{48,40},{56,48},{64,5... | collective-permute-start | bytes 1572872 | tf_op jit(solution)/shard_map/ppermute | solution.py:89
  83.2 1.9 dynamic-slice_dynamic-update-slice_fusion.5
  85.0 1.9 dynamic-slice_dynamic-update-slice_fusion.4
  86.9 1.9 dynamic-slice_dynamic-update-slice_fusion.3
  88.8 2.6 %collective-permute-done.9.refs_8_ = bf16[256,1024]{1,0:T(8,128)(2,1)} collective-permute-done((bf16[256,1024]{1,0:T(8,128)(2,1)S(1)}, bf16[256,1024]{1,0:T(8,128)(2,1)}, u32[]{:S(2)}, u32[]{:S(2)}) %collective-permute-start.9) | collective-permute-done | bytes 524320 | tf_op jit(solution)/shard_map/ppermute | solution.py:89
  91.4 3.8 %collective-permute-start.10 = (bf16[256,1024]{1,0:T(8,128)(2,1)}, bf16[256,1024]{1,0:T(8,128)(2,1)}, u32[]{:S(2)}, u32[]{:S(2)}) collective-permute-start(bf16[256,1024]{1,0:T(8,128)(2,1)} %collective-permute-done.9.refs_8_), channel_id=1, source_target_pairs={{0,120},{8,0},{16,8},{24,16},{32,24},{40,32},{48,40},{56,48},{64,5... | collective-permute-start | bytes 1572872 | tf_op jit(solution)/shard_map/ppermute | solution.py:89
  95.2 1.9 dynamic-slice_dynamic-update-slice_fusion.2
  97.1 1.9 dynamic-slice_dynamic-update-slice_fusion.1
  99.0 1.9 dynamic-slice_dynamic-update-slice_fusion
  100.9 2.7 %collective-permute-done.10.refs_10_.refs_1_ = bf16[256,1024]{1,0:T(8,128)(2,1)} collective-permute-done((bf16[256,1024]{1,0:T(8,128)(2,1)}, bf16[256,1024]{1,0:T(8,128)(2,1)}, u32[]{:S(2)}, u32[]{:S(2)}) %collective-permute-start.10) | collective-permute-done | bytes 524320 | tf_op jit(solution)/shard_map/ppermute | solution.py:89
  103.6 3.7 %collective-permute-start.11 = (bf16[256,1024]{1,0:T(8,128)(2,1)}, bf16[256,1024]{1,0:T(8,128)(2,1)S(1)}, u32[]{:S(2)}, u32[]{:S(2)}) collective-permute-start(bf16[256,1024]{1,0:T(8,128)(2,1)} %collective-permute-done.10.refs_10_.refs_1_), channel_id=1, source_target_pairs={{0,120},{8,0},{16,8},{24,16},{32,24},{40,32},{48,40},{56,48},{64,5... | collective-permute-start | bytes 1572872 | tf_op jit(solution)/shard_map/ppermute | solution.py:89
  107.3 3.1 %fusion = f32[1024]{0:T(1024)S(1)} fusion(bf16[1024,2048]{1,0:T(8,128)(2,1)} %dynamic-slice_dynamic-update-slice_fusion), kind=kLoop, calls=%fused_computation.2 | loop fusion | flops 6290432 | bytes 4198400 | tf_op jit(solution)/shard_map/reduce_sum | solution.py:127
  110.4 6.1 %collective-permute-done.11.refs_1_ = bf16[256,1024]{1,0:T(8,128)(2,1)S(1)} collective-permute-done((bf16[256,1024]{1,0:T(8,128)(2,1)}, bf16[256,1024]{1,0:T(8,128)(2,1)S(1)}, u32[]{:S(2)}, u32[]{:S(2)}) %collective-permute-start.11) | collective-permute-done | bytes 524320 | tf_op jit(solution)/shard_map/ppermute | solution.py:89
  116.5 3.6 %collective-permute-start.13 = (bf16[256,1024]{1,0:T(8,128)(2,1)S(1)}, bf16[256,1024]{1,0:T(8,128)(2,1)S(1)}, u32[]{:S(2)}, u32[]{:S(2)}) collective-permute-start(bf16[256,1024]{1,0:T(8,128)(2,1)S(1)} %collective-permute-done.11.refs_1_), channel_id=1, source_target_pairs={{0,120},{8,0},{16,8},{24,16},{32,24},{40,32},{48,40},{56,48},{64,5... | collective-permute-start | bytes 1572872 | tf_op jit(solution)/shard_map/ppermute | solution.py:89
  120.0 0.2 collective-permute-done.5.refs_0_
  120.3 4.9 %fusion.1 = bf16[1024,2048]{1,0:T(8,128)(2,1)} fusion(bf16[1024,2048]{1,0:T(8,128)(2,1)} %dynamic-slice_dynamic-update-slice_fusion, f32[1024]{0:T(1024)S(1)} %add_rsqrt_fusion), kind=kLoop, calls=%fused_computation.3 | loop fusion | flops 6291456 | bytes 8392704 | tf_op jit(solution)/shard_map/convert_element_type | solution.py:128
  125.2 2.3 %slice.127 = bf16[1024,512]{1,0:T(8,128)(2,1)} slice(bf16[1024,2048]{1,0:T(8,128)(2,1)} %fusion.1), slice={[0:1024], [0:512]} | slice | bytes 2097152 | tf_op jit(solution)/shard_map/slice | solution.py:139
  127.5 1.9 %fusion.6 = bf16[1024,640]{1,0:T(8,128)(2,1)S(1)} fusion(s32[]{:T(128)S(6)} %select_n.103, bf16[1024,2048]{1,0:T(8,128)(2,1)} %fusion.1, bf16[1024,512]{1,0:T(8,128)(2,1)} %slice.127), kind=kLoop, calls=%fused_computation.17 | loop fusion | flops 2621440 | bytes 6553604 | tf_op jit(solution)/shard_map/concatenate | solution.py:139
  129.4 2.9 %shard_map.69.refs_2_ = bf16[1024,2048]{1,0:T(8,128)(2,1)} custom-call(s32[1]{0:T(128)} %bitcast.z_ref, bf16[256,1024]{1,0:T(8,128)(2,1)S(1)} %pad_maximum_fusion.1.refs_0_, bf16[256,1024]{1,0:T(8,128)(2,1)S(1)} %copy-done.1, bf16[256,1024]{1,0:T(8,128)(2,1)S(1)} %collective-permute-done.6.refs_2_, bf16[256,1024]{1,0:T(8,128)(2,1)S(1)} %copy-done.5, ...), custom_call_target="tpu_custom_call" | custom-call | tf_op jit(solution)/shard_map/pallas_call | solution.py:38
  132.4 4.0 %shard_map.67.refs_5_ = bf16[2048,1024]{1,0:T(8,128)(2,1)} custom-call(s32[1]{0:T(128)} %bitcast.z_ref, bf16[256,1024]{1,0:T(8,128)(2,1)S(1)} %pad_maximum_fusion.1.refs_0_, bf16[256,1024]{1,0:T(8,128)(2,1)S(1)} %copy-done.1, bf16[256,1024]{1,0:T(8,128)(2,1)S(1)} %collective-permute-done.6.refs_2_, bf16[256,1024]{1,0:T(8,128)(2,1)S(1)} %copy-done.5, ...), custom_call_target="tpu_custom_call" | custom-call | tf_op jit(solution)/shard_map/pallas_call | solution.py:38
  136.4 0.1 dynamic_update_slice.33
  136.8 6.3 %fusion.31 = f32[1024,1024]{1,0:T(8,128)S(1)} fusion(bf16[1024,2048]{1,0:T(8,128)(2,1)S(1)} %copy-done.9, bf16[2048,1024]{1,0:T(8,128)(2,1)} %shard_map.67.refs_5_), kind=kOutput, calls=%fused_computation.64 | convolution fusion | flops 4294967296 | bytes 12582912 | tf_op jit(solution)/shard_map/dot_general | solution.py:129
  143.1 2.0 %shard_map.70.refs_4_ = bf16[1024,2048]{1,0:T(8,128)(2,1)} custom-call(s32[1]{0:T(128)} %bitcast.z_ref, bf16[256,1024]{1,0:T(8,128)(2,1)} %collective-permute-done.4.refs_9_.refs_0_, bf16[256,1024]{1,0:T(8,128)(2,1)} %collective-permute-done.10.refs_10_.refs_1_, bf16[1024,2048]{1,0:T(8,128)(2,1)} %shard_map.69.refs_2_), custom_call_target="tpu_custom_call", output_to_operand_aliasing={{}: (3, {})} | custom-call | tf_op jit(solution)/shard_map/pallas_call | solution.py:38
  145.2 3.3 %collective-permute-start.15 = (bf16[128,1024]{1,0:T(8,128)(2,1)S(1)}, bf16[128,1024]{1,0:T(8,128)(2,1)S(1)}, u32[]{:S(2)}, u32[]{:S(2)}) collective-permute-start(bf16[128,1024]{1,0:T(8,128)(2,1)S(1)} %get-tuple-element.22), channel_id=1, source_target_pairs={{0,120},{8,0},{16,8},{24,16},{32,24},{40,32},{48,40},{56,48},{64,5... | collective-permute-start | bytes 786440 | tf_op jit(solution)/shard_map/ppermute | solution.py:91
  148.5 1.0 shard_map.71.refs_1_
  149.6 1.8 fusion.32
  151.4 1.1 multiply_convert_fusion
  152.5 0.7 shard_map.72
  153.3 2.6 %convolution_convert_fusion.2 = bf16[512,768]{1,0:T(8,128)(2,1)S(1)} fusion(bf16[1024,2048]{1,0:T(8,128)(2,1)} %shard_map.72, bf16[1024,1024]{1,0:T(8,128)(2,1)S(1)} %multiply_convert_fusion), kind=kOutput, calls=%fused_computation.13 | convolution fusion | flops 805699584 | bytes 3407872 | tf_op jit(solution)/shard_map/dot_general | solution.py:162
  155.9 1.0 convolution_convert_fusion.3
  156.9 0.4 collective-permute-start.16
  157.3 1.5 convolution_convert_fusion
  158.9 0.6 collective-permute-start.21
  159.5 1.5 convolution_convert_fusion.1
  161.0 0.2 fusion.24
  161.3 0.7 collective-permute-start.17
  162.0 2.7 %collective-permute-start.19 = (bf16[128,384]{1,0:T(8,128)(2,1)S(1)}, bf16[128,384]{1,0:T(8,128)(2,1)S(1)}, u32[]{:S(2)}, u32[]{:S(2)}) collective-permute-start(bf16[128,384]{1,0:T(8,128)(2,1)S(1)} %get-tuple-element.16), channel_id=1, source_target_pairs={{0,6},{1,7},{2,0},{3,1},{4,2},{5,3},{6,4},{7,5},{8,14},{9,15},{10,... | collective-permute-start | bytes 294920 | tf_op jit(solution)/shard_map/ppermute | solution.py:173
  164.7 2.7 %collective-permute-done.17 = bf16[128,384]{1,0:T(8,128)(2,1)S(1)} collective-permute-done((bf16[128,384]{1,0:T(8,128)(2,1)S(1)}, bf16[128,384]{1,0:T(8,128)(2,1)S(1)}, u32[]{:S(2)}, u32[]{:S(2)}) %collective-permute-start.17) | collective-permute-done | bytes 98336 | tf_op jit(solution)/shard_map/ppermute | solution.py:172
  167.4 0.3 collective-permute-start.18
  167.7 3.1 %collective-permute-start.20 = (bf16[128,768]{1,0:T(8,128)(2,1)S(1)}, bf16[128,768]{1,0:T(8,128)(2,1)S(1)}, u32[]{:S(2)}, u32[]{:S(2)}) collective-permute-start(bf16[128,768]{1,0:T(8,128)(2,1)S(1)} %get-tuple-element.8), channel_id=1, source_target_pairs={{0,6},{1,7},{2,0},{3,1},{4,2},{5,3},{6,4},{7,5},{8,14},{9,15},{10,... | collective-permute-start | bytes 589832 | tf_op jit(solution)/shard_map/ppermute | solution.py:179
  170.8 0.3 convert_add_fusion
  171.3 3.2 %collective-permute-start.24 = (bf16[128,640]{1,0:T(8,128)(2,1)S(1)}, bf16[128,640]{1,0:T(8,128)(2,1)S(1)}, u32[]{:S(2)}, u32[]{:S(2)}) collective-permute-start(bf16[128,640]{1,0:T(8,128)(2,1)S(1)} %get-tuple-element.12), channel_id=1, source_target_pairs={{0,6},{1,7},{2,0},{3,1},{4,2},{5,3},{6,4},{7,5},{8,14},{9,15},{10,... | collective-permute-start | bytes 491528 | tf_op jit(solution)/shard_map/ppermute | solution.py:173
  174.5 3.7 %collective-permute-done.22 = bf16[128,640]{1,0:T(8,128)(2,1)S(1)} collective-permute-done((bf16[128,640]{1,0:T(8,128)(2,1)S(1)}, bf16[128,640]{1,0:T(8,128)(2,1)S(1)}, u32[]{:S(2)}, u32[]{:S(2)}) %collective-permute-start.22) | collective-permute-done | bytes 163872 | tf_op jit(solution)/shard_map/ppermute | solution.py:172
  178.3 0.8 collective-permute-start.23
  179.1 2.5 %collective-permute-start.25 = (bf16[128,1280]{1,0:T(8,128)(2,1)S(1)}, bf16[128,1280]{1,0:T(8,128)(2,1)S(1)}, u32[]{:S(2)}, u32[]{:S(2)}) collective-permute-start(bf16[128,1280]{1,0:T(8,128)(2,1)S(1)} %get-tuple-element.4), channel_id=1, source_target_pairs={{0,6},{1,7},{2,0},{3,1},{4,2},{5,3},{6,4},{7,5},{8,14},{9,15},{10,... | collective-permute-start | bytes 983048 | tf_op jit(solution)/shard_map/ppermute | solution.py:179
  181.6 1.1 shard_map.68
  182.9 5.1 %collective-permute-done.23 = bf16[128,1280]{1,0:T(8,128)(2,1)S(1)} collective-permute-done((bf16[128,1280]{1,0:T(8,128)(2,1)S(1)}, bf16[128,1280]{1,0:T(8,128)(2,1)S(1)}, u32[]{:S(2)}, u32[]{:S(2)}) %collective-permute-start.23) | collective-permute-done | bytes 327712 | tf_op jit(solution)/shard_map/ppermute | solution.py:178
  188.1 0.8 copy-done.10
  (70 shorter events, 1.6 us)
Async XLA Ops:
  19.7 33.3 %collective-permute-start.6 = (bf16[256,1024]{1,0:T(8,128)(2,1)S(1)}, bf16[256,1024]{1,0:T(8,128)(2,1)S(1)}, u32[]{:S(2)}, u32[]{:S(2)}) collective-permute-start(bf16[256,1024]{1,0:T(8,128)(2,1)S(1)} %pad_maximum_fusion.1.refs_0_), channel_id=1, source_target_pairs={{0,120},{8,0},{16,8},{24,16},{32,24},{40,32},{48,40},{56,48},{64,5... | collective-permute-start | bytes 1572872 | tf_op jit(solution)/shard_map/ppermute | solution.py:89
  42.2 14.5 %collective-permute-start = (bf16[256,1024]{1,0:T(8,128)(2,1)S(1)}, bf16[256,1024]{1,0:T(8,128)(2,1)S(1)}, u32[]{:S(2)}, u32[]{:S(2)}) collective-permute-start(bf16[256,1024]{1,0:T(8,128)(2,1)S(1)} %pad_maximum_fusion.1.refs_0_), channel_id=1, source_target_pairs={{0,8},{8,16},{16,24},{24,32},{32,40},{40,48},{48,56},{56,64},{64,7... | collective-permute-start | bytes 1572872 | tf_op jit(solution)/shard_map/ppermute | solution.py:88
  53.0 13.7 %collective-permute-start.7 = (bf16[256,1024]{1,0:T(8,128)(2,1)S(1)}, bf16[256,1024]{1,0:T(8,128)(2,1)S(1)}, u32[]{:S(2)}, u32[]{:S(2)}) collective-permute-start(bf16[256,1024]{1,0:T(8,128)(2,1)S(1)} %collective-permute-done.6.refs_2_), channel_id=1, source_target_pairs={{0,120},{8,0},{16,8},{24,16},{32,24},{40,32},{48,40},{56,48},{64,5... | collective-permute-start | bytes 1572872 | tf_op jit(solution)/shard_map/ppermute | solution.py:89
  56.7 44.1 %copy-start = (bf16[256,1024]{1,0:T(8,128)(2,1)}, bf16[256,1024]{1,0:T(8,128)(2,1)S(1)}, u32[]{:S(2)}) copy-start(bf16[256,1024]{1,0:T(8,128)(2,1)S(1)} %collective-permute-done.refs_1_) | copy-start | bytes 1572868
  56.7 13.7 %collective-permute-start.1 = (bf16[256,1024]{1,0:T(8,128)(2,1)S(1)}, bf16[256,1024]{1,0:T(8,128)(2,1)S(1)}, u32[]{:S(2)}, u32[]{:S(2)}) collective-permute-start(bf16[256,1024]{1,0:T(8,128)(2,1)S(1)} %collective-permute-done.refs_1_), channel_id=1, source_target_pairs={{0,8},{8,16},{16,24},{24,32},{32,40},{40,48},{48,56},{56,64},{64,7... | collective-permute-start | bytes 1572872 | tf_op jit(solution)/shard_map/ppermute | solution.py:88
  66.7 34.2 %copy-start.2 = (bf16[256,1024]{1,0:T(8,128)(2,1)}, bf16[256,1024]{1,0:T(8,128)(2,1)S(1)}, u32[]{:S(2)}) copy-start(bf16[256,1024]{1,0:T(8,128)(2,1)S(1)} %collective-permute-done.7.refs_4_) | copy-start | bytes 1572868
  66.7 12.8 %collective-permute-start.8 = (bf16[256,1024]{1,0:T(8,128)(2,1)S(1)}, bf16[256,1024]{1,0:T(8,128)(2,1)S(1)}, u32[]{:S(2)}, u32[]{:S(2)}) collective-permute-start(bf16[256,1024]{1,0:T(8,128)(2,1)S(1)} %collective-permute-done.7.refs_4_), channel_id=1, source_target_pairs={{0,120},{8,0},{16,8},{24,16},{32,24},{40,32},{48,40},{56,48},{64,5... | collective-permute-start | bytes 1572872 | tf_op jit(solution)/shard_map/ppermute | solution.py:89
  70.4 30.5 %copy-start.4 = (bf16[256,1024]{1,0:T(8,128)(2,1)}, bf16[256,1024]{1,0:T(8,128)(2,1)S(1)}, u32[]{:S(2)}) copy-start(bf16[256,1024]{1,0:T(8,128)(2,1)S(1)} %collective-permute-done.1.refs_3_) | copy-start | bytes 1572868
  70.4 12.8 %collective-permute-start.2 = (bf16[256,1024]{1,0:T(8,128)(2,1)S(1)}, bf16[256,1024]{1,0:T(8,128)(2,1)}, u32[]{:S(2)}, u32[]{:S(2)}) collective-permute-start(bf16[256,1024]{1,0:T(8,128)(2,1)S(1)} %collective-permute-done.1.refs_3_), channel_id=1, source_target_pairs={{0,8},{8,16},{16,24},{24,32},{32,40},{40,48},{48,56},{56,64},{64,7... | collective-permute-start | bytes 1572872 | tf_op jit(solution)/shard_map/ppermute | solution.py:88
  79.5 30.9 %copy-start.6 = (bf16[256,1024]{1,0:T(8,128)(2,1)}, bf16[256,1024]{1,0:T(8,128)(2,1)S(1)}, u32[]{:S(2)}) copy-start(bf16[256,1024]{1,0:T(8,128)(2,1)S(1)} %collective-permute-done.8.refs_6_) | copy-start | bytes 1572868
  79.5 11.9 %collective-permute-start.9 = (bf16[256,1024]{1,0:T(8,128)(2,1)S(1)}, bf16[256,1024]{1,0:T(8,128)(2,1)}, u32[]{:S(2)}, u32[]{:S(2)}) collective-permute-start(bf16[256,1024]{1,0:T(8,128)(2,1)S(1)} %collective-permute-done.8.refs_6_), channel_id=1, source_target_pairs={{0,120},{8,0},{16,8},{24,16},{32,24},{40,32},{48,40},{56,48},{64,5... | collective-permute-start | bytes 1572872 | tf_op jit(solution)/shard_map/ppermute | solution.py:89
  83.2 12.0 %collective-permute-start.3 = (bf16[256,1024]{1,0:T(8,128)(2,1)}, bf16[256,1024]{1,0:T(8,128)(2,1)}, u32[]{:S(2)}, u32[]{:S(2)}) collective-permute-start(bf16[256,1024]{1,0:T(8,128)(2,1)} %collective-permute-done.2.refs_5_), channel_id=1, source_target_pairs={{0,8},{8,16},{16,24},{24,32},{32,40},{40,48},{48,56},{56,64},{64,7... | collective-permute-start | bytes 1572872 | tf_op jit(solution)/shard_map/ppermute | solution.py:88
  91.4 12.2 %collective-permute-start.10 = (bf16[256,1024]{1,0:T(8,128)(2,1)}, bf16[256,1024]{1,0:T(8,128)(2,1)}, u32[]{:S(2)}, u32[]{:S(2)}) collective-permute-start(bf16[256,1024]{1,0:T(8,128)(2,1)} %collective-permute-done.9.refs_8_), channel_id=1, source_target_pairs={{0,120},{8,0},{16,8},{24,16},{32,24},{40,32},{48,40},{56,48},{64,5... | collective-permute-start | bytes 1572872 | tf_op jit(solution)/shard_map/ppermute | solution.py:89
  95.2 12.1 %collective-permute-start.4 = (bf16[256,1024]{1,0:T(8,128)(2,1)}, bf16[256,1024]{1,0:T(8,128)(2,1)}, u32[]{:S(2)}, u32[]{:S(2)}) collective-permute-start(bf16[256,1024]{1,0:T(8,128)(2,1)} %collective-permute-done.3.refs_7_), channel_id=1, source_target_pairs={{0,8},{8,16},{16,24},{24,32},{32,40},{40,48},{48,56},{56,64},{64,7... | collective-permute-start | bytes 1572872 | tf_op jit(solution)/shard_map/ppermute | solution.py:88
  103.6 12.9 %collective-permute-start.11 = (bf16[256,1024]{1,0:T(8,128)(2,1)}, bf16[256,1024]{1,0:T(8,128)(2,1)S(1)}, u32[]{:S(2)}, u32[]{:S(2)}) collective-permute-start(bf16[256,1024]{1,0:T(8,128)(2,1)} %collective-permute-done.10.refs_10_.refs_1_), channel_id=1, source_target_pairs={{0,120},{8,0},{16,8},{24,16},{32,24},{40,32},{48,40},{56,48},{64,5... | collective-permute-start | bytes 1572872 | tf_op jit(solution)/shard_map/ppermute | solution.py:89
  107.3 13.0 %collective-permute-start.5 = (bf16[256,1024]{1,0:T(8,128)(2,1)}, bf16[256,1024]{1,0:T(8,128)(2,1)S(1)}, u32[]{:S(2)}, u32[]{:S(2)}) collective-permute-start(bf16[256,1024]{1,0:T(8,128)(2,1)} %collective-permute-done.4.refs_9_.refs_0_), channel_id=1, source_target_pairs={{0,8},{8,16},{16,24},{24,32},{32,40},{40,48},{48,56},{56,64},{64,7... | collective-permute-start | bytes 1572872 | tf_op jit(solution)/shard_map/ppermute | solution.py:88
  116.5 20.1 %collective-permute-start.13 = (bf16[256,1024]{1,0:T(8,128)(2,1)S(1)}, bf16[256,1024]{1,0:T(8,128)(2,1)S(1)}, u32[]{:S(2)}, u32[]{:S(2)}) collective-permute-start(bf16[256,1024]{1,0:T(8,128)(2,1)S(1)} %collective-permute-done.11.refs_1_), channel_id=1, source_target_pairs={{0,120},{8,0},{16,8},{24,16},{32,24},{40,32},{48,40},{56,48},{64,5... | collective-permute-start | bytes 1572872 | tf_op jit(solution)/shard_map/ppermute | solution.py:89
  120.3 16.3 %collective-permute-start.12 = (bf16[256,1024]{1,0:T(8,128)(2,1)S(1)}, bf16[256,1024]{1,0:T(8,128)(2,1)S(1)}, u32[]{:S(2)}, u32[]{:S(2)}) collective-permute-start(bf16[256,1024]{1,0:T(8,128)(2,1)S(1)} %collective-permute-done.5.refs_0_), channel_id=1, source_target_pairs={{0,8},{8,16},{16,24},{24,32},{32,40},{40,48},{48,56},{56,64},{64,7... | collective-permute-start | bytes 1572872 | tf_op jit(solution)/shard_map/ppermute | solution.py:88
  127.4 2.0 %copy-start.1 = (bf16[256,1024]{1,0:T(8,128)(2,1)S(1)}, bf16[256,1024]{1,0:T(8,128)(2,1)}, u32[]{:S(2)}) copy-start(bf16[256,1024]{1,0:T(8,128)(2,1)} %copy-done) | copy-start | bytes 1572868
  127.4 2.0 %copy-start.3 = (bf16[256,1024]{1,0:T(8,128)(2,1)S(1)}, bf16[256,1024]{1,0:T(8,128)(2,1)}, u32[]{:S(2)}) copy-start(bf16[256,1024]{1,0:T(8,128)(2,1)} %copy-done.2) | copy-start | bytes 1572868
  127.4 2.0 %copy-start.5 = (bf16[256,1024]{1,0:T(8,128)(2,1)S(1)}, bf16[256,1024]{1,0:T(8,128)(2,1)}, u32[]{:S(2)}) copy-start(bf16[256,1024]{1,0:T(8,128)(2,1)} %copy-done.4) | copy-start | bytes 1572868
  127.4 2.0 %copy-start.7 = (bf16[256,1024]{1,0:T(8,128)(2,1)S(1)}, bf16[256,1024]{1,0:T(8,128)(2,1)}, u32[]{:S(2)}) copy-start(bf16[256,1024]{1,0:T(8,128)(2,1)} %copy-done.6) | copy-start | bytes 1572868
  132.4 4.4 %copy-start.9 = (bf16[1024,2048]{1,0:T(8,128)(2,1)S(1)}, bf16[1024,2048]{1,0:T(8,128)(2,1)}, u32[]{:S(2)}) copy-start(bf16[1024,2048]{1,0:T(8,128)(2,1)} %fusion.1) | copy-start | bytes 12582916
  136.7 12.9 %collective-permute-start.14 = (bf16[128,1024]{1,0:T(8,128)(2,1)S(1)}, bf16[128,1024]{1,0:T(8,128)(2,1)S(1)}, u32[]{:S(2)}, u32[]{:S(2)}) collective-permute-start(bf16[128,1024]{1,0:T(8,128)(2,1)S(1)} %get-tuple-element.20), channel_id=1, source_target_pairs={{0,8},{8,16},{16,24},{24,32},{32,40},{40,48},{48,56},{56,64},{64,7... | collective-permute-start | bytes 786440 | tf_op jit(solution)/shard_map/ppermute | solution.py:90
  145.2 7.3 %collective-permute-start.15 = (bf16[128,1024]{1,0:T(8,128)(2,1)S(1)}, bf16[128,1024]{1,0:T(8,128)(2,1)S(1)}, u32[]{:S(2)}, u32[]{:S(2)}) collective-permute-start(bf16[128,1024]{1,0:T(8,128)(2,1)S(1)} %get-tuple-element.22), channel_id=1, source_target_pairs={{0,120},{8,0},{16,8},{24,16},{32,24},{40,32},{48,40},{56,48},{64,5... | collective-permute-start | bytes 786440 | tf_op jit(solution)/shard_map/ppermute | solution.py:91
  153.3 2.7 %copy-start.8 = (bf16[1024,2048]{1,0:T(8,128)(2,1)S(1)}, bf16[1024,2048]{1,0:T(8,128)(2,1)}, u32[]{:S(2)}) copy-start(bf16[1024,2048]{1,0:T(8,128)(2,1)} %shard_map.72) | copy-start | bytes 12582916
  156.9 4.1 %collective-permute-start.16 = (bf16[512,768]{1,0:T(8,128)(2,1)S(1)}, bf16[512,768]{1,0:T(8,128)(2,1)S(1)}, u32[]{:S(2)}, u32[]{:S(2)}) collective-permute-start(bf16[512,768]{1,0:T(8,128)(2,1)S(1)} %convolution_convert_fusion.2), channel_id=1, source_target_pairs={{0,1},{1,0},{2,3},{3,2},{4,5},{5,4},{6,7},{7,6},{8,9},{9,8},{10,11... | collective-permute-start | bytes 2359304 | tf_op jit(solution)/shard_map/ppermute | solution.py:164
  158.9 11.9 %collective-permute-start.21 = (bf16[512,1280]{1,0:T(8,128)(2,1)S(1)}, bf16[512,1280]{1,0:T(8,128)(2,1)S(1)}, u32[]{:S(2)}, u32[]{:S(2)}) collective-permute-start(bf16[512,1280]{1,0:T(8,128)(2,1)S(1)} %convolution_convert_fusion), channel_id=1, source_target_pairs={{0,1},{1,0},{2,3},{3,2},{4,5},{5,4},{6,7},{7,6},{8,9},{9,8},{10,11... | collective-permute-start | bytes 3932168 | tf_op jit(solution)/shard_map/ppermute | solution.py:164
  161.3 6.1 %collective-permute-start.17 = (bf16[128,384]{1,0:T(8,128)(2,1)S(1)}, bf16[128,384]{1,0:T(8,128)(2,1)S(1)}, u32[]{:S(2)}, u32[]{:S(2)}) collective-permute-start(bf16[128,384]{1,0:T(8,128)(2,1)S(1)} %get-tuple-element.15), channel_id=1, source_target_pairs={{0,2},{1,3},{2,4},{3,5},{4,6},{5,7},{6,0},{7,1},{8,10},{9,11},{10,... | collective-permute-start | bytes 294920 | tf_op jit(solution)/shard_map/ppermute | solution.py:172
  162.0 5.4 %collective-permute-start.19 = (bf16[128,384]{1,0:T(8,128)(2,1)S(1)}, bf16[128,384]{1,0:T(8,128)(2,1)S(1)}, u32[]{:S(2)}, u32[]{:S(2)}) collective-permute-start(bf16[128,384]{1,0:T(8,128)(2,1)S(1)} %get-tuple-element.16), channel_id=1, source_target_pairs={{0,6},{1,7},{2,0},{3,1},{4,2},{5,3},{6,4},{7,5},{8,14},{9,15},{10,... | collective-permute-start | bytes 294920 | tf_op jit(solution)/shard_map/ppermute | solution.py:173
  167.4 15.4 %collective-permute-start.18 = (bf16[128,768]{1,0:T(8,128)(2,1)S(1)}, bf16[128,768]{1,0:T(8,128)(2,1)S(1)}, u32[]{:S(2)}, u32[]{:S(2)}) collective-permute-start(bf16[128,768]{1,0:T(8,128)(2,1)S(1)} %get-tuple-element.7), channel_id=1, source_target_pairs={{0,2},{1,3},{2,4},{3,5},{4,6},{5,7},{6,0},{7,1},{8,10},{9,11},{10,... | collective-permute-start | bytes 589832 | tf_op jit(solution)/shard_map/ppermute | solution.py:178
  167.7 15.1 %collective-permute-start.20 = (bf16[128,768]{1,0:T(8,128)(2,1)S(1)}, bf16[128,768]{1,0:T(8,128)(2,1)S(1)}, u32[]{:S(2)}, u32[]{:S(2)}) collective-permute-start(bf16[128,768]{1,0:T(8,128)(2,1)S(1)} %get-tuple-element.8), channel_id=1, source_target_pairs={{0,6},{1,7},{2,0},{3,1},{4,2},{5,3},{6,4},{7,5},{8,14},{9,15},{10,... | collective-permute-start | bytes 589832 | tf_op jit(solution)/shard_map/ppermute | solution.py:179
  171.1 7.1 %collective-permute-start.22 = (bf16[128,640]{1,0:T(8,128)(2,1)S(1)}, bf16[128,640]{1,0:T(8,128)(2,1)S(1)}, u32[]{:S(2)}, u32[]{:S(2)}) collective-permute-start(bf16[128,640]{1,0:T(8,128)(2,1)S(1)} %get-tuple-element.11), channel_id=1, source_target_pairs={{0,2},{1,3},{2,4},{3,5},{4,6},{5,7},{6,0},{7,1},{8,10},{9,11},{10,... | collective-permute-start | bytes 491528 | tf_op jit(solution)/shard_map/ppermute | solution.py:172
  171.3 6.9 %collective-permute-start.24 = (bf16[128,640]{1,0:T(8,128)(2,1)S(1)}, bf16[128,640]{1,0:T(8,128)(2,1)S(1)}, u32[]{:S(2)}, u32[]{:S(2)}) collective-permute-start(bf16[128,640]{1,0:T(8,128)(2,1)S(1)} %get-tuple-element.12), channel_id=1, source_target_pairs={{0,6},{1,7},{2,0},{3,1},{4,2},{5,3},{6,4},{7,5},{8,14},{9,15},{10,... | collective-permute-start | bytes 491528 | tf_op jit(solution)/shard_map/ppermute | solution.py:173
  178.3 9.7 %collective-permute-start.23 = (bf16[128,1280]{1,0:T(8,128)(2,1)S(1)}, bf16[128,1280]{1,0:T(8,128)(2,1)S(1)}, u32[]{:S(2)}, u32[]{:S(2)}) collective-permute-start(bf16[128,1280]{1,0:T(8,128)(2,1)S(1)} %get-tuple-element.3), channel_id=1, source_target_pairs={{0,2},{1,3},{2,4},{3,5},{4,6},{5,7},{6,0},{7,1},{8,10},{9,11},{10,... | collective-permute-start | bytes 983048 | tf_op jit(solution)/shard_map/ppermute | solution.py:178
  179.1 8.9 %collective-permute-start.25 = (bf16[128,1280]{1,0:T(8,128)(2,1)S(1)}, bf16[128,1280]{1,0:T(8,128)(2,1)S(1)}, u32[]{:S(2)}, u32[]{:S(2)}) collective-permute-start(bf16[128,1280]{1,0:T(8,128)(2,1)S(1)} %get-tuple-element.4), channel_id=1, source_target_pairs={{0,6},{1,7},{2,0},{3,1},{4,2},{5,3},{6,4},{7,5},{8,14},{9,15},{10,... | collective-permute-start | bytes 983048 | tf_op jit(solution)/shard_map/ppermute | solution.py:179
  188.1 0.8 copy-start.10
